TPU v7x, 32 devices: a whole 2x2x4 slice. The times are simulated.
32 devices in a mesh: dp: 4 (over y, x), kv: 4 (over z), tp: 2 (over core).
Axes of the slice: x: 2, y: 2, z: 4, core: 2. Of those that a mesh axis runs over, the one named last changes fastest.
Arguments:
- tokens: bfloat16 [32, 2048], P('dp', ('kv', 'tp')), as said below
- first_gain: float32 [2048], replicated, may hold values from 0.1 to 1.9
- first_gate: bfloat16 [2048, 5632], P(None, ('kv', 'tp')), may hold values from -0.125 to 0.125
- first_up: bfloat16 [2048, 5632], P(None, ('kv', 'tp')), may hold values from -0.125 to 0.125
- first_down: bfloat16 [5632, 2048], P(('kv', 'tp')), may hold values from -0.109375 to 0.109375
- mix_gain: float32 [2048], P(('kv', 'tp')), may hold values from 0.1 to 1.9
- w_input: bfloat16 [2048, 2048], P(('kv', 'tp')), may hold values from -0.125 to 0.125
- w_outgate: bfloat16 [2048, 2048], P(('kv', 'tp')), may hold values from -0.125 to 0.125
- w_write: bfloat16 [2048, 512], P(('kv', 'tp')), may hold values from -0.125 to 0.125
- w_read: bfloat16 [2048, 512], P(('kv', 'tp')), may hold values from -0.125 to 0.125
- w_step: bfloat16 [2048, 32], P(('kv', 'tp')), may hold values from -0.125 to 0.125
- conv_taps: bfloat16 [4, 3072], replicated, may hold values from -3 to 3
- conv_history: bfloat16 [32, 3, 3072], P(('dp', 'kv', 'tp')), may hold values from -6 to 6
- step_bias: float32 [32], replicated, may hold values from -6 to -1
- rate_log: float32 [32], replicated, may hold values from 0 to 2.77
- mixer_state: float32 [32, 32, 64, 128], P(('dp', 'kv', 'tp')), may hold values from -4 to 4
- group_gain: float32 [2048], replicated, may hold values from 0.1 to 1.9
- w_output: bfloat16 [2048, 2048], P(None, ('kv', 'tp')), may hold values from -0.125 to 0.125
- second_gain: float32 [2048], replicated, may hold values from 0.1 to 1.9
- second_gate: bfloat16 [2048, 5632], P(None, ('kv', 'tp')), may hold values from -0.125 to 0.125
- second_up: bfloat16 [2048, 5632], P(None, ('kv', 'tp')), may hold values from -0.125 to 0.125
- second_down: bfloat16 [5632, 2048], P(('kv', 'tp')), may hold values from -0.109375 to 0.109375
Outputs:
- layer_out: bfloat16 [32, 2048], P('dp', ('kv', 'tp'))
- state_out: float32 [32, 32, 64, 128], P(('dp', 'kv', 'tp'))
- history_out: bfloat16 [32, 3, 3072], P(('dp', 'kv', 'tp'))
Inputs may be any that keep to these rules, and one draw needn't show every extreme that they name: `tokens`: channel scales rise along the width.
All inputs are finite; a program needn't handle non-finite values.
Results may differ from a plain program's by a relative error of at most 0.014.
Values may be sent and summed in bfloat16 or wider, within the bound.
No kernel may reach another device: no remote copies, remote signals or barrier semaphores. Data moves between devices by JAX's collectives and lax.ppermute only.
A program may use at most 64 MiB of HBM per device.

v0:
```python
import jax
import jax.numpy as jnp
from jax import lax
from jax.sharding import PartitionSpec as P

EPS = 1e-06


def half_block(resid, gain, w_gate, w_up, w_down):
    whole = lax.all_gather(resid, ("kv", "tp"), axis=1, tiled=True)
    whole_f = whole.astype(jnp.float32)
    scale = lax.rsqrt(jnp.mean(whole_f * whole_f, axis=-1, keepdims=True) + EPS)
    normed = (whole_f * scale * gain).astype(jnp.bfloat16)
    gate = jnp.dot(normed, w_gate, preferred_element_type=jnp.float32)
    upper = jnp.dot(normed, w_up, preferred_element_type=jnp.float32)
    hidden = (jax.nn.silu(gate) * upper).astype(jnp.bfloat16)
    down = jnp.dot(hidden, w_down, preferred_element_type=jnp.float32)
    share = lax.psum_scatter(down, ("kv", "tp"), scatter_dimension=1, tiled=True)
    return (resid.astype(jnp.float32) + 0.5 * share).astype(jnp.bfloat16)


def body(
    tokens,
    first_gain,
    first_gate,
    first_up,
    first_down,
    mix_gain,
    w_input,
    w_outgate,
    w_write,
    w_read,
    w_step,
    conv_taps,
    conv_history,
    step_bias,
    rate_log,
    mixer_state,
    group_gain,
    w_output,
    second_gain,
    second_gate,
    second_up,
    second_down,
):
    width = first_gate.shape[0]
    count = mixer_state.shape[0]
    heads = mixer_state.shape[1]
    head_dim = mixer_state.shape[2]
    state_dim = mixer_state.shape[3]
    ssd_width = heads * head_dim
    groups = w_write.shape[1] // state_dim
    per_group = heads // groups
    first = half_block(tokens, first_gain, first_gate, first_up, first_down)
    first_f = first.astype(jnp.float32)
    squares = jnp.sum(first_f * first_f, axis=1)
    premix = (first_f * mix_gain).astype(jnp.bfloat16)
    part_input = jnp.dot(premix, w_input, preferred_element_type=jnp.float32)
    part_write = jnp.dot(premix, w_write, preferred_element_type=jnp.float32)
    part_read = jnp.dot(premix, w_read, preferred_element_type=jnp.float32)
    part_step = jnp.dot(premix, w_step, preferred_element_type=jnp.float32)
    part_gate = jnp.dot(premix, w_outgate, preferred_element_type=jnp.float32)
    totals = lax.psum(squares, ("kv", "tp"))
    head_terms = (part_input, part_write, part_read, part_step)
    extra_terms = ()
    summed = lax.psum_scatter(
        head_terms + extra_terms + (part_gate,), ("kv", "tp"), scatter_dimension=0, tiled=True
    )
    gate_sum = summed[-1]
    summed = summed[:-1]
    own_squares = lax.dynamic_slice_in_dim(totals, lax.axis_index(("kv", "tp")) * count, count, 0)
    scale = lax.rsqrt(own_squares / width + EPS)[:, None]
    inputs = (scale * summed[0]).astype(jnp.bfloat16)
    writes = (scale * summed[1]).astype(jnp.bfloat16)
    reads = (scale * summed[2]).astype(jnp.bfloat16)
    steps_raw = (scale * summed[3]).astype(jnp.bfloat16)
    fresh = jnp.concatenate([inputs, writes, reads], axis=1)
    window = jnp.concatenate([conv_history, fresh[:, None, :]], axis=1)
    history_out = window[:, 1:]
    conv = jax.nn.silu(
        jnp.sum(window.astype(jnp.float32) * conv_taps.astype(jnp.float32)[None], axis=1)
    )
    conv_in = conv[:, :ssd_width].reshape(count, groups, per_group, head_dim)
    conv_write = conv[:, ssd_width : ssd_width + groups * state_dim].reshape(
        count, groups, state_dim
    )
    conv_read = conv[:, ssd_width + groups * state_dim :].reshape(count, groups, state_dim)
    step = jax.nn.softplus(steps_raw.astype(jnp.float32) + step_bias)
    decay = jnp.exp(-step * jnp.exp(rate_log))
    state = mixer_state.reshape(count, groups, per_group, head_dim, state_dim)
    decay_g = decay.reshape(count, groups, per_group)
    step_g = step.reshape(count, groups, per_group)
    written = (step_g[..., None] * conv_in)[..., None] * conv_write[:, :, None, None, :]
    new_state = decay_g[..., None, None] * state + written
    read_out = jnp.einsum("sgjpn,sgn->sgjp", new_state, conv_read, precision=lax.Precision.HIGHEST)
    outgate = (scale * gate_sum).astype(jnp.bfloat16)
    gated = read_out.reshape(count, ssd_width) * jax.nn.silu(outgate.astype(jnp.float32))
    blocks = gated.reshape(count, groups, ssd_width // groups)
    block_scale = lax.rsqrt(jnp.mean(blocks * blocks, axis=-1, keepdims=True) + EPS)
    normed = ((blocks * block_scale).reshape(count, ssd_width) * group_gain).astype(jnp.bfloat16)
    mixed = jnp.dot(
        lax.all_gather(normed, ("kv", "tp"), axis=0, tiled=True),
        w_output,
        preferred_element_type=jnp.float32,
    )
    second = (first_f + mixed).astype(jnp.bfloat16)
    layer_out = half_block(second, second_gain, second_gate, second_up, second_down)
    state_out = new_state.reshape(count, heads, head_dim, state_dim)
    return (layer_out, state_out, history_out)


def solution(mesh):
    return jax.shard_map(
        body,
        mesh=mesh,
        in_specs=(
            P("dp", ("kv", "tp")),
            P(),
            P(None, ("kv", "tp")),
            P(None, ("kv", "tp")),
            P(("kv", "tp"), None),
            P(("kv", "tp")),
            P(("kv", "tp"), None),
            P(("kv", "tp"), None),
            P(("kv", "tp"), None),
            P(("kv", "tp"), None),
            P(("kv", "tp"), None),
            P(),
            P(("dp", "kv", "tp"), None, None),
            P(),
            P(),
            P(("dp", "kv", "tp"), None, None, None),
            P(),
            P(None, ("kv", "tp")),
            P(),
            P(None, ("kv", "tp")),
            P(None, ("kv", "tp")),
            P(("kv", "tp"), None),
        ),
        out_specs=(
            P("dp", ("kv", "tp")),
            P(("dp", "kv", "tp"), None, None, None),
            P(("dp", "kv", "tp"), None, None),
        ),
        check_vma=False,
    )
```

profile of v0, /device:TPU:0, one launch (start us, length us, event | category | flops | bytes accessed | tf_op | source)
XLA Modules:
  0.0 234.0 jit_solution(7709291567706687449)
XLA Ops:
  7.2 0.0 reduce-scatter.3.cloned.1.call-start
  7.2 16.1 %all_gather.9 = bf16[8,2048]{1,0:T(8,128)(2,1)S(1)} all-gather(bf16[8,256]{1,0:T(8,128)(2,1)} %param.22), channel_id=1, replica_groups=mesh['dp'=4,'kv'=4,'tp'=2] {'kv','tp'}, dimensions={1}, use_global_device_ids=true | all-gather | bytes 36864 | tf_op jit(solution)/shard_map/all_gather | solution.py:10
  23.3 0.1 fusion.12
  23.4 2.7 %fusion.42 = f32[8,704]{1,0:T(8,128)S(1)} fusion(bf16[2048,704]{0,1:T(8,128)(2,1)} %param.24, bf16[8,2048]{1,0:T(8,128)(2,1)S(1)} %all_gather.9, f32[2048]{0:T(1024)} %param.23, f32[8]{0:T(128)S(1)} %add_rsqrt_fusion.2), kind=kOutput, calls=%fused_computation.61 | convolution fusion | flops 23134208 | bytes 2947104 | tf_op jit(solution)/shard_map/dot_general | solution.py:14
  26.1 0.0 copy-start.13
  26.2 4.2 %fusion.3 = f32[8,2048]{1,0:T(8,128)} fusion(bf16[704,2048]{1,0:T(8,128)(2,1)S(1)} %copy-done, bf16[2048,704]{0,1:T(8,128)(2,1)} %param.25, f32[8,704]{1,0:T(8,128)S(1)} %fusion.42, bf16[8,2048]{1,0:T(8,128)(2,1)S(1)} %all_gather.9, f32[2048]{0:T(1024)S(1)} %copy-done.4, f32[8]{0:T(128)S(1)} %add_rsqrt_fusion.2), kind=kOutput, calls=%fused_computation.5 | convolution fusion | flops 46236672 | bytes 5896224 | tf_op jit(solution)/shard_map/dot_general | solution.py:17
  30.4 0.0 reduce-scatter.3.cloned.1.call-update
  30.4 0.0 all-reduce.9.cloned.1.call-start
  30.5 0.6 dynamic-slice
  31.1 31.0 %reduce-scatter.3.cloned.1.call-done = f32[8,256]{1,0:T(8,128)} async-done(((f32[8,2048]{1,0:T(8,128)}), f32[8,256]{1,0:T(8,128)}) %reduce-scatter.3.cloned.1.call-update) | async-done | bytes 8208 | tf_op jit(solution)/shard_map/reduce_scatter | solution.py:18
  62.0 0.8 fusion.31
  62.9 0.1 fusion.53
  63.0 0.1 fusion.55
  63.2 0.1 fusion.59
  63.3 26.4 %all-reduce.5 = (f32[8,512]{1,0:T(8,128)S(1)}, f32[8]{0:T(128)S(1)}, f32[8,512]{1,0:T(8,128)S(1)}, f32[8,32]{1,0:T(8,128)S(1)}) all-reduce(f32[8,512]{1,0:T(8,128)S(1)} %fusion.53, f32[8]{0:T(128)S(1)} %get-tuple-element.14, f32[8,512]{1,0:T(8,128)S(1)} %fusion.55, ...), channel_id=7, replica_groups=mesh['dp'=4,'kv'=4,'tp'=2] {'kv','tp'}, use_global_device_ids=true, to_apply=%region_7.8.clone | all-reduce | flops 8456 | bytes 67648
  89.7 0.6 dynamic_slice.3
  91.0 2.1 fusion.57
  93.1 2.1 fusion.51
  95.2 0.5 broadcast.146
  95.7 1.3 fusion.64
  97.0 0.6 reduce.20
  97.7 0.1 mul.266
  97.7 0.1 mul.263
  97.8 0.0 all-reduce.9.cloned.1.call-update
  97.9 0.0 reduce-scatter.5.cloned.1.call-start
  97.9 0.7 fusion.44
  98.6 52.9 %all-reduce.9.cloned.1.call-done = (f32[8,2048]{1,0:T(8,128)}, f32[8,2048]{1,0:T(8,128)}) async-done(((f32[8,2048]{1,0:T(8,128)}, f32[8,2048]{1,0:T(8,128)}), (f32[8,2048]{1,0:T(8,128)}, f32[8,2048]{1,0:T(8,128)})) %all-reduce.9.cloned.1.call-update) | async-done | bytes 131088
  151.5 1.5 fusion.35
  153.0 0.1 multiply_reduce_fusion
  153.2 0.1 reshape.166
  153.2 0.1 broadcast_multiply_fusion.1
  153.3 3.8 %fusion.5 = f32[4,1,8,64]{3,1,2,0:T(1,128)S(1)} fusion(f32[4,8,64,128]{3,2,1,0:T(8,128)} %bitcast.47, f32[4,128]{1,0:T(4,128)S(1)} %bitcast.55, f32[4,8,64]{2,1,0:T(8,128)S(1)} %broadcast_multiply_fusion.1, f32[4,8]{1,0:T(4,128)S(1)} %mul.263, f32[1,3072]{1,0:T(1,128)S(1)} %divide_multiply_fusion), kind=kOutput, calls=%fused_computation.9 | convolution fusion | flops 3932160 | bytes 1079296 | tf_op jit(solution)/shard_map/sgjpn,sgn->sgjp/dot_general | solution.py:95
  157.2 0.1 reshape.168
  157.2 1.6 multiply_reduce_fusion.1
  158.8 0.1 reduce_sum.51
  158.9 0.1 mul.285
  159.0 14.1 %all-gather = bf16[16384]{0:T(1024)(128)(2,1)S(1)} all-gather(bf16[2048]{0:T(1024)(128)(2,1)S(1)} %multiply_convert_fusion), channel_id=2, replica_groups=mesh['dp'=4,'kv'=4,'tp'=2] {'kv','tp'}, dimensions={0}, use_global_device_ids=true | all-gather | bytes 36864 | tf_op jit(solution)/shard_map/all_gather | solution.py:102
  173.1 1.5 fusion.4
  174.6 14.1 %all_gather.11 = bf16[8,2048]{1,0:T(8,128)(2,1)S(1)} all-gather(bf16[8,256]{1,0:T(8,128)(2,1)S(1)} %fusion.4), channel_id=1, replica_groups=mesh['dp'=4,'kv'=4,'tp'=2] {'kv','tp'}, dimensions={1}, use_global_device_ids=true | all-gather | bytes 36864 | tf_op jit(solution)/shard_map/all_gather | solution.py:10
  188.7 0.1 fusion.15
  188.8 2.7 %fusion.38 = f32[8,704]{1,0:T(8,128)S(1)} fusion(bf16[2048,704]{0,1:T(8,128)(2,1)} %param.41, bf16[8,2048]{1,0:T(8,128)(2,1)S(1)} %all_gather.11, f32[2048]{0:T(1024)S(1)} %copy-done.5, f32[8]{0:T(128)S(1)} %add_rsqrt_fusion), kind=kOutput, calls=%fused_computation.60 | convolution fusion | flops 23134208 | bytes 2947104 | tf_op jit(solution)/shard_map/dot_general | solution.py:14
  191.5 5.0 %fusion.2 = f32[8,2048]{1,0:T(8,128)} fusion(bf16[704,2048]{1,0:T(8,128)(2,1)} %param.43, bf16[2048,704]{0,1:T(8,128)(2,1)} %param.42, f32[8,704]{1,0:T(8,128)S(1)} %fusion.38, bf16[8,2048]{1,0:T(8,128)(2,1)S(1)} %all_gather.11, f32[2048]{0:T(1024)S(1)} %copy-done.5, f32[8]{0:T(128)S(1)} %add_rsqrt_fusion), kind=kOutput, calls=%fused_computation.4 | convolution fusion | flops 46236672 | bytes 5896224 | tf_op jit(solution)/shard_map/dot_general | solution.py:17
  196.5 0.1 reshape.170
  196.6 0.6 pad_maximum_fusion
  197.2 0.1 broadcast_multiply_fusion
  197.3 2.6 %multiply_add_fusion = f32[1,32,64,128]{3,2,1,0:T(8,128)} fusion(f32[1,32,64,128]{3,2,1,0:T(8,128)} %param.37, f32[32,128]{1,0:T(8,128)S(1)} %broadcast_bitcast_fusion, f32[32,64]{1,0:T(8,128)S(1)} %broadcast_multiply_fusion, f32[32]{0:T(128)S(1)} %bitcast.56), kind=kLoop, calls=%fused_computation.8 | loop fusion | flops 786432 | bytes 2121856 | tf_op jit(solution)/shard_map/add | solution.py:94
  199.9 26.3 %reduce-scatter.5.cloned.1.call-done = f32[8,256]{1,0:T(8,128)} async-done(((f32[8,2048]{1,0:T(8,128)}), f32[8,256]{1,0:T(8,128)}) %reduce-scatter.5.cloned.1.call-update) | async-done | bytes 8208 | tf_op jit(solution)/shard_map/reduce_scatter | solution.py:18
  226.2 1.3 add_convert_fusion
  (39 shorter events, 0.2 us)
Async XLA Ops:
  7.2 19.0 %copy-start = (bf16[704,2048]{1,0:T(8,128)(2,1)S(1)}, bf16[704,2048]{1,0:T(8,128)(2,1)}, u32[]{:S(2)}) copy-start(bf16[704,2048]{1,0:T(8,128)(2,1)} %param.26) | copy-start | bytes 8650756
  7.2 18.9 %copy-start.4 = (f32[2048]{0:T(1024)S(1)}, f32[2048]{0:T(1024)}, u32[]{:S(2)}) copy-start(f32[2048]{0:T(1024)} %param.23) | copy-start | bytes 24580
  7.2 54.9 %reduce-scatter.3.cloned.1.call-start = ((), (), s32[]{:S(2)}) async-start(), calls=%async_computation.2 | async-start | bytes 73728 | tf_op jit(solution)/shard_map/reduce_scatter | solution.py:18
  26.1 4.4 %copy-start.13 = (u32[32]{0:T(128)S(1)}, u32[32]{0:T(128)}, u32[]{:S(2)}) copy-start(u32[32]{0:T(128)} %constant.47) | copy-start | bytes 388
  26.1 35.9 %copy-start.9 = (bf16[8,256]{1,0:T(8,128)(2,1)S(1)}, bf16[8,256]{1,0:T(8,128)(2,1)}, u32[]{:S(2)}) copy-start(bf16[8,256]{1,0:T(8,128)(2,1)} %param.22) | copy-start | bytes 12292
  26.2 36.7 %copy-start.1 = (bf16[256,512]{1,0:T(8,128)(2,1)S(1)}, bf16[256,512]{1,0:T(8,128)(2,1)}, u32[]{:S(2)}) copy-start(bf16[256,512]{1,0:T(8,128)(2,1)} %param.31) | copy-start | bytes 786436
  26.2 36.7 %copy-start.6 = (f32[256]{0:T(256)S(1)}, f32[256]{0:T(256)}, u32[]{:S(2)}) copy-start(f32[256]{0:T(256)} %param.27) | copy-start | bytes 3076
  26.2 36.8 %copy-start.2 = (bf16[256,512]{1,0:T(8,128)(2,1)S(1)}, bf16[256,512]{1,0:T(8,128)(2,1)}, u32[]{:S(2)}) copy-start(bf16[256,512]{1,0:T(8,128)(2,1)} %param.30) | copy-start | bytes 786436
  26.2 37.0 %copy-start.8 = (bf16[256,32]{0,1:T(8,128)(2,1)S(1)}, bf16[256,32]{0,1:T(8,128)(2,1)}, u32[]{:S(2)}) copy-start(bf16[256,32]{0,1:T(8,128)(2,1)} %param.32) | copy-start | bytes 49156
  30.4 65.4 %copy-start.11 = (f32[32]{0:T(128)S(1)}, f32[32]{0:T(128)}, u32[]{:S(2)}) copy-start(f32[32]{0:T(128)} %param.36) | copy-start | bytes 388
  30.4 65.4 %copy-start.12 = (f32[32]{0:T(128)S(1)}, f32[32]{0:T(128)}, u32[]{:S(2)}) copy-start(f32[32]{0:T(128)} %param.35) | copy-start | bytes 388
  30.4 122.6 %copy-start.3 = (bf16[1,3,3072]{2,1,0:T(4,128)(2,1)S(1)}, bf16[1,3,3072]{2,1,0:T(4,128)(2,1)}, u32[]{:S(2)}) copy-start(bf16[1,3,3072]{2,1,0:T(4,128)(2,1)} %param.34) | copy-start | bytes 55300
  30.4 122.6 %copy-start.7 = (bf16[4,3072]{1,0:T(4,128)(2,1)S(1)}, bf16[4,3072]{1,0:T(4,128)(2,1)}, u32[]{:S(2)}) copy-start(bf16[4,3072]{1,0:T(4,128)(2,1)} %param.33) | copy-start | bytes 73732
  30.4 128.6 %copy-start.10 = (f32[2048]{0:T(1024)S(1)}, f32[2048]{0:T(1024)}, u32[]{:S(2)}) copy-start(f32[2048]{0:T(1024)} %param.38) | copy-start | bytes 24580
  30.4 121.1 %all-reduce.9.cloned.1.call-start = ((), (), s32[]{:S(2)}) async-start(), calls=%async_computation.4 | async-start | bytes 262144
  62.9 126.0 %copy-start.5 = (f32[2048]{0:T(1024)S(1)}, f32[2048]{0:T(1024)}, u32[]{:S(2)}) copy-start(f32[2048]{0:T(1024)} %param.40) | copy-start | bytes 24580
  97.9 128.3 %reduce-scatter.5.cloned.1.call-start = ((), (), s32[]{:S(2)}) async-start(), calls=%async_computation.3 | async-start | bytes 73728 | tf_op jit(solution)/shard_map/reduce_scatter | solution.py:18
Sparse Core Ops, SparseCore 0:
  30.5 31.4 reduce-scatter.2
  98.0 53.4 all-reduce.8
  196.6 29.4 reduce-scatter.4
where the time goes:
time: 235 us; the launch traced here: 234 us
  waiting for transfers between devices  110 us (47%)
  blocking collectives  70.6 us (30%)
  matrix products  24.4 us (10%)
  between operations  14.7 us (6%)
  other arithmetic  11.7 us (5%)
    reduce_scatter x2, waiting for transfers between devices, half_block(): lax.psum_scatter(down, ('kv', 'tp'), scatter_dimension=1, tiled=True)  57.2 us
    unnamed x4, waiting for transfers between devices  53 us
    all_gather x2, blocking collectives, half_block(): whole = lax.all_gather(resid, ('kv', 'tp'), axis=1, tiled=True)  30.1 us
    unnamed x1, blocking collectives  26.4 us
    all_gather x1, blocking collectives, body(): lax.all_gather(normed, ('kv', 'tp'), axis=0, tiled=True)  14.1 us
    dot_general x2, matrix products, half_block(): down = jnp.dot(hidden, w_down, preferred_element_type=jnp.float32)  9.15 us
    dot_general x2, matrix products, half_block(): gate = jnp.dot(normed, w_gate, preferred_element_type=jnp.float32)  5.33 us
  transfers between devices with their start and end apart: 3, of which 3 were waited for; matrix products, arithmetic and copies ran while one was open for 2% of the time, Pallas kernels for 0%

commit v1 on v0

v1 whole, which is shorter than its diff:
```python
import jax
import jax.numpy as jnp
from jax import lax
from jax.sharding import PartitionSpec as P

EPS = 1e-06
AXES = ("kv", "tp")


def exchange(blocks):
    return lax.all_to_all(blocks, AXES, split_axis=0, concat_axis=0, tiled=True)


def gather(block, ways):
    return exchange(jnp.broadcast_to(block[None], (ways,) + block.shape))


def scatter_sum(partial, ways):
    rows, width = partial.shape
    blocks = partial.reshape(rows, ways, width // ways).transpose(1, 0, 2)
    return jnp.sum(exchange(blocks), axis=0)


def half_block(resid, gain, w_gate, w_up, w_down, ways):
    rows = resid.shape[0]
    whole = gather(resid, ways).transpose(1, 0, 2).reshape(rows, -1)
    whole_f = whole.astype(jnp.float32)
    scale = lax.rsqrt(jnp.mean(whole_f * whole_f, axis=-1, keepdims=True) + EPS)
    normed = (whole_f * scale * gain).astype(jnp.bfloat16)
    gate = jnp.dot(normed, w_gate, preferred_element_type=jnp.float32)
    upper = jnp.dot(normed, w_up, preferred_element_type=jnp.float32)
    hidden = (jax.nn.silu(gate) * upper).astype(jnp.bfloat16)
    down = jnp.dot(hidden, w_down, preferred_element_type=jnp.float32)
    share = scatter_sum(down, ways)
    return (resid.astype(jnp.float32) + 0.5 * share).astype(jnp.bfloat16)


def make_body(ways):
    def body(
        tokens,
        first_gain,
        first_gate,
        first_up,
        first_down,
        mix_gain,
        w_input,
        w_outgate,
        w_write,
        w_read,
        w_step,
        conv_taps,
        conv_history,
        step_bias,
        rate_log,
        mixer_state,
        group_gain,
        w_output,
        second_gain,
        second_gate,
        second_up,
        second_down,
    ):
        width = first_gate.shape[0]
        count = mixer_state.shape[0]
        heads = mixer_state.shape[1]
        head_dim = mixer_state.shape[2]
        state_dim = mixer_state.shape[3]
        ssd_width = heads * head_dim
        groups = w_write.shape[1] // state_dim
        per_group = heads // groups
        rows = tokens.shape[0]
        first = half_block(tokens, first_gain, first_gate, first_up, first_down, ways)
        first_f = first.astype(jnp.float32)
        squares = jnp.sum(first_f * first_f, axis=1, keepdims=True)
        premix = (first_f * mix_gain).astype(jnp.bfloat16)
        parts = [
            jnp.dot(premix, w, preferred_element_type=jnp.float32)
            for w in (w_input, w_write, w_read, w_outgate, w_step)
        ]
        ends = []
        total = 0
        for p in parts:
            total += p.shape[1]
            ends.append(total)
        padded = -(-(total + 1) // 1024) * 1024
        pad = jnp.zeros((rows, padded - total - 1), jnp.float32)
        packed = jnp.concatenate(parts + [squares, pad], axis=1)
        packed = packed.reshape(ways, count, padded)
        summed = jnp.sum(exchange(packed), axis=0)
        own_squares = summed[:, total : total + 1]
        scale = lax.rsqrt(own_squares / width + EPS)
        scaled = (scale * summed[:, :total]).astype(jnp.bfloat16)
        fresh = scaled[:, : ends[2]]
        outgate = scaled[:, ends[2] : ends[3]]
        steps_raw = scaled[:, ends[3] :]
        window = jnp.concatenate([conv_history, fresh[:, None, :]], axis=1)
        history_out = window[:, 1:]
        conv = jax.nn.silu(
            jnp.sum(window.astype(jnp.float32) * conv_taps.astype(jnp.float32)[None], axis=1)
        )
        conv_in = conv[:, :ssd_width].reshape(count, groups, per_group, head_dim)
        conv_write = conv[:, ssd_width : ssd_width + groups * state_dim].reshape(
            count, groups, state_dim
        )
        conv_read = conv[:, ssd_width + groups * state_dim :].reshape(count, groups, state_dim)
        step = jax.nn.softplus(steps_raw.astype(jnp.float32) + step_bias)
        decay = jnp.exp(-step * jnp.exp(rate_log))
        state = mixer_state.reshape(count, groups, per_group, head_dim, state_dim)
        decay_g = decay.reshape(count, groups, per_group)
        step_g = step.reshape(count, groups, per_group)
        written = (step_g[..., None] * conv_in)[..., None] * conv_write[:, :, None, None, :]
        new_state = decay_g[..., None, None] * state + written
        read_out = jnp.sum(new_state * conv_read[:, :, None, None, :], axis=-1)
        gated = read_out.reshape(count, ssd_width) * jax.nn.silu(outgate.astype(jnp.float32))
        blocks = gated.reshape(count, groups, ssd_width // groups)
        block_scale = lax.rsqrt(jnp.mean(blocks * blocks, axis=-1, keepdims=True) + EPS)
        normed = ((blocks * block_scale).reshape(count, ssd_width) * group_gain).astype(jnp.bfloat16)
        mixed = jnp.dot(
            gather(normed, ways).reshape(rows, ssd_width),
            w_output,
            preferred_element_type=jnp.float32,
        )
        second = (first_f + mixed).astype(jnp.bfloat16)
        layer_out = half_block(second, second_gain, second_gate, second_up, second_down, ways)
        state_out = new_state.reshape(count, heads, head_dim, state_dim)
        return (layer_out, state_out, history_out)

    return body


def solution(mesh):
    whole = P(AXES)
    rows = P(AXES, None)
    columns = P(None, AXES)
    own = ("dp",) + AXES
    return jax.shard_map(
        make_body(mesh.shape["kv"] * mesh.shape["tp"]),
        mesh=mesh,
        in_specs=(
            P("dp", AXES),
            P(),
            columns,
            columns,
            rows,
            whole,
            rows,
            rows,
            rows,
            rows,
            rows,
            P(),
            P(own, None, None),
            P(),
            P(),
            P(own, None, None, None),
            P(),
            columns,
            P(),
            columns,
            columns,
            rows,
        ),
        out_specs=(P("dp", AXES), P(own, None, None, None), P(own, None, None)),
        check_vma=False,
    )
```

time: 235 us -> 86.9 us (0.37)
  waiting for transfers between devices: 110 us -> 5.2 us
  blocking collectives: 70.6 us -> 47.4 us
  between operations: 14.7 us -> 1.54 us
  other arithmetic: 11.7 us -> 6.31 us
  matrix products: 24.4 us -> 19.6 us
  starting transfers between devices: 0.12 us -> 3.35 us
    reduce_scatter x2 -> x0, waiting for transfers between devices: 57.2 us -> none  [half_block(): lax.psum_scatter(down, ('kv', 'tp'), scatter_dimension=1, tiled=True)]
    unnamed x4 -> x0, waiting for transfers between devices: 53 us -> none
    all_to_all x0 -> x5, blocking collectives: none -> 47.4 us  [exchange(): return lax.all_to_all(blocks, AXES, split_axis=0, concat_axis=0, tiled=True)]
    all_gather x3 -> x0, blocking collectives: 44.2 us -> none  [the longest x2 30.1 us: half_block(): whole = lax.all_gather(resid, ('kv', 'tp'), axis=1, tiled=True)]
    unnamed x1 -> x0, blocking collectives: 26.4 us -> none
    all_to_all x0 -> x1, waiting for transfers between devices: none -> 5.2 us  [exchange(): return lax.all_to_all(blocks, AXES, split_axis=0, concat_axis=0, tiled=True)]
    dot_general x7 -> x6, matrix products: 9.91 us -> 5.79 us  [the longest x5 4.32 us: body(): jnp.dot(premix, w, preferred_element_type=jnp.float32)]
    all_to_all x0 -> x1, starting transfers between devices: none -> 3.35 us  [exchange(): return lax.all_to_all(blocks, AXES, split_axis=0, concat_axis=0, tiled=True)]
  transfers between devices with their start and end apart: 3 -> 1, of which waited for: 3 -> 1; matrix products, arithmetic and copies ran while one was open for 2% -> 1% of each run, Pallas kernels for 0% -> 0%
where the time goes in v1:
time: 86.9 us; the launch traced here: 86.2 us
  blocking collectives  47.4 us (55%)
  matrix products  19.6 us (23%)
  other arithmetic  6.31 us (7%)
  waiting for transfers between devices  5.2 us (6%)
  starting transfers between devices  3.35 us (4%)
  local copies, waits for them, and re-layouts  2.77 us (3%)
  between operations  1.54 us (2%)
    all_to_all x5, blocking collectives, exchange(): return lax.all_to_all(blocks, AXES, split_axis=0, concat_axis=0, tiled=True)  47.4 us
    dot_general x2, matrix products, half_block(): down = jnp.dot(hidden, w_down, preferred_element_type=jnp.float32)  8.5 us
    dot_general x2, matrix products, half_block(): gate = jnp.dot(normed, w_gate, preferred_element_type=jnp.float32)  5.33 us
    all_to_all x1, waiting for transfers between devices, exchange(): return lax.all_to_all(blocks, AXES, split_axis=0, concat_axis=0, tiled=True)  5.2 us
    dot_general x5, matrix products, body(): jnp.dot(premix, w, preferred_element_type=jnp.float32)  4.32 us
    all_to_all x1, starting transfers between devices, exchange(): return lax.all_to_all(blocks, AXES, split_axis=0, concat_axis=0, tiled=True)  3.35 us
    reduce_sum x1, other arithmetic, body(): read_out = jnp.sum(new_state * conv_read[:, :, None, None, :], axis=-1)  2.61 us
  transfers between devices with their start and end apart: 1, of which 1 were waited for; matrix products, arithmetic and copies ran while one was open for 1% of the time, Pallas kernels for 0%

profile of v1, /device:TPU:0, one launch (start us, length us, event | category | flops | bytes accessed | tf_op | source)
XLA Modules:
  0.0 86.2 jit_solution(5825125142098099461)
XLA Ops:
  0.6 0.0 copy-start
  0.6 0.0 copy-start.3
  0.7 0.8 broadcast_in_dim.16
  1.5 12.0 %all_to_all.30 = bf16[8,8,256]{2,1,0:T(8,128)(2,1)S(1)} all-to-all(bf16[8,8,256]{2,1,0:T(8,128)(2,1)S(1)} %broadcast_in_dim.16), channel_id=1, replica_groups=mesh['dp'=4,'kv'=4,'tp'=2] {'kv','tp'}, dimensions={0} | all-to-all | bytes 65536 | tf_op jit(solution)/shard_map/all_to_all | solution.py:11
  13.5 0.1 multiply_reduce_fusion.2
  13.7 2.7 %fusion.38 = f32[8,704]{1,0:T(8,128)S(1)} fusion(bf16[2048,704]{0,1:T(8,128)(2,1)} %param.24, f32[8,2048]{1,0:T(8,128)S(1)} %bitcast.58, f32[2048]{0:T(1024)} %param.23, f32[8]{0:T(128)S(1)} %add_rsqrt_fusion.2), kind=kOutput, calls=%fused_computation.65 | convolution fusion | flops 23117824 | bytes 2979872 | tf_op jit(solution)/shard_map/dot_general | solution.py:30
  16.3 0.0 copy-done
  16.3 0.0 copy-start.8
  16.4 0.0 copy-start.5
  16.4 0.0 copy-start.1
  16.4 3.5 %fusion.3 = f32[8,2048]{1,0:T(8,128)S(1)} fusion(bf16[704,2048]{1,0:T(8,128)(2,1)S(1)} %copy-done, bf16[2048,704]{0,1:T(8,128)(2,1)} %param.25, f32[8,704]{1,0:T(8,128)S(1)} %fusion.38, f32[8,2048]{1,0:T(8,128)S(1)} %bitcast.59, f32[2048]{0:T(1024)S(1)} %copy-done.3, f32[8]{0:T(128)S(1)} %add_rsqrt_fusion.2), kind=kOutput, calls=%fused_computation.5 | convolution fusion | flops 46220288 | bytes 5928992 | tf_op jit(solution)/shard_map/dot_general | solution.py:33
  19.9 0.0 copy-start.10
  19.9 8.4 %all_to_all.31 = f32[8,8,256]{2,1,0:T(8,128)S(1)} all-to-all(f32[8,8,256]{2,1,0:T(8,128)S(1)} %bitcast.62), channel_id=1, replica_groups=mesh['dp'=4,'kv'=4,'tp'=2] {'kv','tp'}, dimensions={0} | all-to-all | bytes 131072 | tf_op jit(solution)/shard_map/all_to_all | solution.py:11
  28.4 0.1 fusion.22
  28.5 1.5 %fusion.28 = f32[8,2048]{1,0:T(8,128)S(1)} fusion(bf16[256,2048]{1,0:T(8,128)(2,1)} %param.29, bf16[8,256]{1,0:T(8,128)(2,1)S(1)} %get-tuple-element.10, f32[256]{0:T(256)S(1)} %copy-done.5), kind=kOutput, calls=%fused_computation.58 | convolution fusion | flops 8394752 | bytes 1119232 | tf_op jit(solution)/shard_map/dot_general | solution.py:77
  30.0 1.5 %fusion.34 = f32[8,2048]{1,0:T(8,128)S(1)} fusion(bf16[256,2048]{1,0:T(8,128)(2,1)} %param.28, bf16[8,256]{1,0:T(8,128)(2,1)S(1)} %get-tuple-element.10, f32[256]{0:T(256)S(1)} %copy-done.5), kind=kOutput, calls=%fused_computation.61 | convolution fusion | flops 8394752 | bytes 1119232 | tf_op jit(solution)/shard_map/dot_general | solution.py:77
  31.5 0.0 copy-done.1
  31.5 0.1 fusion.30
  31.6 1.1 %fusion.32 = f32[8,512]{1,0:T(8,128)S(1)} fusion(bf16[256,512]{1,0:T(8,128)(2,1)} %param.30, bf16[8,256]{1,0:T(8,128)(2,1)S(1)} %get-tuple-element.10, f32[256]{0:T(256)S(1)} %copy-done.5), kind=kOutput, calls=%fused_computation.60 | convolution fusion | flops 2103296 | bytes 283648 | tf_op jit(solution)/shard_map/dot_general | solution.py:77
  32.7 0.1 fusion.26
  32.8 0.1 copy.29
  32.9 0.1 concatenate.11
  33.0 0.2 copy.30
  33.2 10.7 %all_to_all.32 = f32[8,1,6144]{2,1,0:T(1,128)S(1)} all-to-all(f32[8,1,6144]{2,1,0:T(1,128)S(1)} %copy.30), channel_id=1, replica_groups=mesh['dp'=4,'kv'=4,'tp'=2] {'kv','tp'}, dimensions={0} | all-to-all | bytes 393216 | tf_op jit(solution)/shard_map/all_to_all | solution.py:11
  43.9 0.1 reduce_sum.88
  44.1 0.6 slice.36
  45.4 0.0 copy-done.2
  45.4 0.0 copy-done.6
  45.4 0.1 multiply_reduce_fusion.3
  45.6 0.1 reshape.186
  45.7 0.7 fusion.25
  46.3 0.1 broadcast_multiply_fusion
  46.4 2.6 %multiply_reduce_fusion = (f32[32,64]{1,0:T(8,128)S(1)}, f32[1,32,64,128]{3,2,1,0:T(8,128)}) fusion(f32[32,128]{1,0:T(8,128)S(1)} %get-tuple-element.15, f32[32,128]{1,0:T(8,128)S(1)} %get-tuple-element.16, f32[32,64]{1,0:T(8,128)S(1)} %broadcast_multiply_fusion, f32[1,32,64,128]{3,2,1,0:T(8,128)} %param.37, f32[32]{0:T(128)S(1)} %get-tuple-element.7), kind=kLoop, calls=%fused_computation.8 | loop fusion | flops 1308672 | bytes 2146432 | tf_op jit(solution)/shard_map/reduce_sum | solution.py:113
  49.0 0.1 reshape.187
  49.2 0.1 reduce_sum.93
  49.3 0.1 mul.258
  49.4 0.5 broadcast.149
  50.0 0.8 reduce.19
  50.8 8.1 %all_to_all.33 = bf16[8,2,1024]{2,1,0:T(2,128)(2,1)S(1)} all-to-all(bf16[8,2,1024]{2,1,0:T(2,128)(2,1)S(1)} %reshape.205), channel_id=1, replica_groups=mesh['dp'=4,'kv'=4,'tp'=2] {'kv','tp'}, dimensions={0} | all-to-all | bytes 65536 | tf_op jit(solution)/shard_map/all_to_all | solution.py:11
  59.0 1.5 %fusion.4 = bf16[8,256]{1,0:T(8,128)(2,1)S(1)} fusion(bf16[2048,256]{1,0:T(8,128)(2,1)} %param.39, bf16[8,1,2048]{2,1,0:T(2,128)(2,1)S(1)} %reshape.206, bf16[8,256]{1,0:T(8,128)(2,1)S(1)} %get-tuple-element.10), kind=kOutput, calls=%fused_computation.7 | convolution fusion | flops 8394752 | bytes 1089536 | tf_op jit(solution)/shard_map/dot_general | solution.py:118
  60.4 8.1 %all_to_all.34 = bf16[8,8,256]{2,1,0:T(8,128)(2,1)S(1)} all-to-all(bf16[8,8,256]{2,1,0:T(8,128)(2,1)S(1)} %broadcast_in_dim.22), channel_id=1, replica_groups=mesh['dp'=4,'kv'=4,'tp'=2] {'kv','tp'}, dimensions={0} | all-to-all | bytes 65536 | tf_op jit(solution)/shard_map/all_to_all | solution.py:11
  68.5 0.1 multiply_reduce_fusion.1
  68.7 2.7 %fusion.39 = f32[8,704]{1,0:T(8,128)S(1)} fusion(bf16[2048,704]{0,1:T(8,128)(2,1)} %param.41, f32[8,2048]{1,0:T(8,128)S(1)} %bitcast.60, f32[2048]{0:T(1024)S(1)} %copy-done.4, f32[8]{0:T(128)S(1)} %add_rsqrt_fusion), kind=kOutput, calls=%fused_computation.66 | convolution fusion | flops 23117824 | bytes 2979872 | tf_op jit(solution)/shard_map/dot_general | solution.py:30
  71.4 5.0 %fusion.2 = f32[8,2048]{1,0:T(8,128)} fusion(bf16[704,2048]{1,0:T(8,128)(2,1)} %param.43, bf16[2048,704]{0,1:T(8,128)(2,1)} %param.42, f32[8,704]{1,0:T(8,128)S(1)} %fusion.39, f32[8,2048]{1,0:T(8,128)S(1)} %bitcast.61, f32[2048]{0:T(1024)S(1)} %copy-done.4, f32[8]{0:T(128)S(1)} %add_rsqrt_fusion), kind=kOutput, calls=%fused_computation.4 | convolution fusion | flops 46220288 | bytes 5928992 | tf_op jit(solution)/shard_map/dot_general | solution.py:33
  76.4 3.3 %all-to-all-start.5 = ((f32[8,8,256]{2,1,0:T(8,128)}), f32[8,8,256]{2,1,0:T(8,128)S(1)}, u32[]{:S(2)}, u32[]{:S(2)}) async-start(f32[8,8,256]{2,1,0:T(8,128)} %bitcast.23), calls=%async_computation.5 | async-start | bytes 131072 | tf_op jit(solution)/shard_map/all_to_all | solution.py:11
  79.7 0.6 pad_maximum_fusion
  80.4 5.2 %all-to-all-done.5 = f32[8,8,256]{2,1,0:T(8,128)S(1)} async-done(((f32[8,8,256]{2,1,0:T(8,128)}), f32[8,8,256]{2,1,0:T(8,128)S(1)}, u32[]{:S(2)}, u32[]{:S(2)}) %all-to-all-start.5) | async-done | bytes 65568 | tf_op jit(solution)/shard_map/all_to_all | solution.py:11
  85.6 0.6 add_convert_fusion
  (33 shorter events, 0.3 us)
Async XLA Ops:
  0.6 15.7 %copy-start = (bf16[704,2048]{1,0:T(8,128)(2,1)S(1)}, bf16[704,2048]{1,0:T(8,128)(2,1)}, u32[]{:S(2)}) copy-start(bf16[704,2048]{1,0:T(8,128)(2,1)} %param.26) | copy-start | bytes 8650756
  0.6 15.7 %copy-start.3 = (f32[2048]{0:T(1024)S(1)}, f32[2048]{0:T(1024)}, u32[]{:S(2)}) copy-start(f32[2048]{0:T(1024)} %param.23) | copy-start | bytes 24580
  16.3 12.0 %copy-start.8 = (bf16[8,256]{1,0:T(8,128)(2,1)S(1)}, bf16[8,256]{1,0:T(8,128)(2,1)}, u32[]{:S(2)}) copy-start(bf16[8,256]{1,0:T(8,128)(2,1)} %param.22) | copy-start | bytes 12292
  16.4 12.1 %copy-start.5 = (f32[256]{0:T(256)S(1)}, f32[256]{0:T(256)}, u32[]{:S(2)}) copy-start(f32[256]{0:T(256)} %param.27) | copy-start | bytes 3076
  16.4 15.1 %copy-start.1 = (bf16[256,512]{1,0:T(8,128)(2,1)S(1)}, bf16[256,512]{1,0:T(8,128)(2,1)}, u32[]{:S(2)}) copy-start(bf16[256,512]{1,0:T(8,128)(2,1)} %param.31) | copy-start | bytes 786436
  19.9 12.8 %copy-start.7 = (bf16[256,32]{0,1:T(8,128)(2,1)S(1)}, bf16[256,32]{0,1:T(8,128)(2,1)}, u32[]{:S(2)}) copy-start(bf16[256,32]{0,1:T(8,128)(2,1)} %param.32) | copy-start | bytes 49156
  19.9 25.5 %copy-start.2 = (bf16[1,3,3072]{2,1,0:T(4,128)(2,1)S(1)}, bf16[1,3,3072]{2,1,0:T(4,128)(2,1)}, u32[]{:S(2)}) copy-start(bf16[1,3,3072]{2,1,0:T(4,128)(2,1)} %param.34) | copy-start | bytes 55300
  19.9 25.5 %copy-start.6 = (bf16[4,3072]{1,0:T(4,128)(2,1)S(1)}, bf16[4,3072]{1,0:T(4,128)(2,1)}, u32[]{:S(2)}) copy-start(bf16[4,3072]{1,0:T(4,128)(2,1)} %param.33) | copy-start | bytes 73732
  19.9 25.8 %copy-start.10 = (f32[32]{0:T(128)S(1)}, f32[32]{0:T(128)}, u32[]{:S(2)}) copy-start(f32[32]{0:T(128)} %param.36) | copy-start | bytes 388
  30.0 19.4 %copy-start.9 = (f32[2048]{0:T(1024)S(1)}, f32[2048]{0:T(1024)}, u32[]{:S(2)}) copy-start(f32[2048]{0:T(1024)} %param.38) | copy-start | bytes 24580
  32.9 35.8 %copy-start.4 = (f32[2048]{0:T(1024)S(1)}, f32[2048]{0:T(1024)}, u32[]{:S(2)}) copy-start(f32[2048]{0:T(1024)} %param.40) | copy-start | bytes 24580
  76.4 9.2 %all-to-all-start.5 = ((f32[8,8,256]{2,1,0:T(8,128)}), f32[8,8,256]{2,1,0:T(8,128)S(1)}, u32[]{:S(2)}, u32[]{:S(2)}) async-start(f32[8,8,256]{2,1,0:T(8,128)} %bitcast.23), calls=%async_computation.5 | async-start | bytes 131072 | tf_op jit(solution)/shard_map/all_to_all | solution.py:11

commit v2 on v1

--- a/solution.py
+++ b/solution.py
@@ -1,14 +1,442 @@
+import functools
+
 import jax
 import jax.numpy as jnp
 from jax import lax
+from jax.experimental import pallas as pl
+from jax.experimental.pallas import tpu as pltpu
 from jax.sharding import PartitionSpec as P
 
 EPS = 1e-06
 AXES = ("kv", "tp")
+LANES = 128
+MIB = 1 << 20
+VMEM_SPEC = pl.BlockSpec(memory_space=pltpu.VMEM)
+ANY_SPEC = pl.BlockSpec(memory_space=pl.ANY)
+ROW_ROW = (((1,), (1,)), ((), ()))
 
 
 def exchange(blocks):
     return lax.all_to_all(blocks, AXES, split_axis=0, concat_axis=0, tiled=True)
+
+
+def params(megabytes):
+    return pltpu.CompilerParams(vmem_limit_bytes=megabytes * MIB)
+
+
+def cost(nbytes):
+    return pl.CostEstimate(flops=nbytes, bytes_accessed=nbytes, transcendentals=0)
+
+
+def silu(x):
+    return x / (1.0 + jnp.exp(-x))
+
+
+def load_kernel(cuts, *refs):
+    n = len(cuts)
+    sources, targets, sems = refs[:n], refs[n : 2 * n], refs[2 * n]
+    copies = []
+    for source, target, cut in zip(sources, targets, cuts):
+        step = source.shape[0] // cut
+        for i in range(cut):
+            part = pl.ds(i * step, step)
+            copies.append(
+                pltpu.make_async_copy(source.at[part], target.at[part], sems.at[len(copies)])
+            )
+    for copy in copies:
+        copy.start()
+    for copy in copies:
+        copy.wait()
+
+
+def load(*arrays):
+    cuts = tuple(4 if a.size * a.dtype.itemsize >= MIB and a.shape[0] % 64 == 0 else 1 for a in arrays)
+    return pl.pallas_call(
+        functools.partial(load_kernel, cuts),
+        out_shape=[pltpu.VMEM(a.shape, a.dtype) for a in arrays],
+        in_specs=[ANY_SPEC] * len(arrays),
+        out_specs=[VMEM_SPEC] * len(arrays),
+        scratch_shapes=[pltpu.SemaphoreType.DMA((sum(cuts),))],
+        compiler_params=params(4),
+        cost_estimate=cost(sum(a.size * a.dtype.itemsize for a in arrays)),
+    )(*arrays)
+
+
+def ff_kernel(x_ref, gain_ref, gate_ref, up_ref, down_hbm, out_ref, down_ref, sem):
+    copy = pltpu.make_async_copy(down_hbm, down_ref, sem)
+    copy.start()
+    ways, rows, chan = x_ref.shape
+    pieces = [x_ref[k].astype(jnp.float32) for k in range(ways)]
+    total = jnp.zeros((rows, 1), jnp.float32)
+    for piece in pieces:
+        total += jnp.sum(piece * piece, axis=1, keepdims=True)
+    scale = lax.rsqrt(total / (ways * chan) + EPS)
+    normed = jnp.concatenate(
+        [
+            (piece * scale * gain_ref[:, k * chan : (k + 1) * chan]).astype(jnp.bfloat16)
+            for k, piece in enumerate(pieces)
+        ],
+        axis=1,
+    )
+    gate = lax.dot_general(normed, gate_ref[...], ROW_ROW, preferred_element_type=jnp.float32)
+    upper = lax.dot_general(normed, up_ref[...], ROW_ROW, preferred_element_type=jnp.float32)
+    hidden = (silu(gate) * upper).astype(jnp.bfloat16)
+    copy.wait()
+    down = jnp.dot(hidden, down_ref[...], preferred_element_type=jnp.float32)
+    for k in range(ways):
+        out_ref[k] = down[:, k * chan : (k + 1) * chan]
+
+
+def ff_loaded_kernel(x_ref, gain_ref, gate_ref, up_ref, down_ref, out_ref):
+    ways, rows, chan = x_ref.shape
+    pieces = [x_ref[k].astype(jnp.float32) for k in range(ways)]
+    total = jnp.zeros((rows, 1), jnp.float32)
+    for piece in pieces:
+        total += jnp.sum(piece * piece, axis=1, keepdims=True)
+    scale = lax.rsqrt(total / (ways * chan) + EPS)
+    normed = jnp.concatenate(
+        [
+            (piece * scale * gain_ref[:, k * chan : (k + 1) * chan]).astype(jnp.bfloat16)
+            for k, piece in enumerate(pieces)
+        ],
+        axis=1,
+    )
+    gate = lax.dot_general(normed, gate_ref[...], ROW_ROW, preferred_element_type=jnp.float32)
+    upper = lax.dot_general(normed, up_ref[...], ROW_ROW, preferred_element_type=jnp.float32)
+    hidden = (silu(gate) * upper).astype(jnp.bfloat16)
+    down = jnp.dot(hidden, down_ref[...], preferred_element_type=jnp.float32)
+    for k in range(ways):
+        out_ref[k] = down[:, k * chan : (k + 1) * chan]
+
+
+def ff(whole, gain, gate, up, down, loaded):
+    size = 3 * gate.size * 2
+    scratch = [] if loaded else [pltpu.VMEM(down.shape, down.dtype), pltpu.SemaphoreType.DMA]
+    return pl.pallas_call(
+        ff_loaded_kernel if loaded else ff_kernel,
+        out_shape=jax.ShapeDtypeStruct(whole.shape, jnp.float32),
+        in_specs=[VMEM_SPEC] * 4 + [VMEM_SPEC if loaded else ANY_SPEC],
+        out_specs=VMEM_SPEC,
+        scratch_shapes=scratch,
+        compiler_params=params(8),
+        cost_estimate=cost(size),
+    )(whole, gain, gate, up, down)
+
+
+def project_kernel(got_ref, tok_ref, gain_ref, win_ref, wwrite_ref, wread_ref, wgate_ref, wstep_ref,
+                   first_ref, out_ref, stage):
+    ways, rows, _ = got_ref.shape
+    slots = out_ref.shape[1]
+    share = got_ref[0]
+    for k in range(1, ways):
+        share += got_ref[k]
+    first = (tok_ref[...].astype(jnp.float32) + 0.5 * share).astype(jnp.bfloat16)
+    first_ref[...] = first
+    first_f = first.astype(jnp.float32)
+    squares = jnp.sum(first_f * first_f, axis=1, keepdims=True)
+    premix = (first_f * gain_ref[...]).astype(jnp.bfloat16)
+    row = 0
+    for w_ref in (win_ref, wwrite_ref, wread_ref, wgate_ref):
+        part = jnp.dot(premix, w_ref[...], preferred_element_type=jnp.float32)
+        for j in range(part.shape[1] // LANES):
+            stage[pl.ds(row, rows, stride=slots), :] = part[:, j * LANES : (j + 1) * LANES]
+            row += 1
+    steps = lax.dot_general(premix, wstep_ref[...], ROW_ROW, preferred_element_type=jnp.float32)
+    stage[pl.ds(row, rows, stride=slots), :] = jnp.zeros((rows, LANES), jnp.float32)
+    stage[pl.ds(row, rows, stride=slots), : steps.shape[1]] = steps
+    row += 1
+    rest = jnp.broadcast_to(squares, (rows, LANES))
+    for _ in range(3):
+        term = rest.astype(jnp.bfloat16).astype(jnp.float32)
+        stage[pl.ds(row, rows, stride=slots), :] = term
+        rest = rest - term
+        row += 1
+    for j in range(row, slots):
+        stage[pl.ds(j, rows, stride=slots), :] = jnp.zeros((rows, LANES), jnp.float32)
+    for s in range(rows):
+        out_ref[s] = stage[pl.ds(s * slots, slots), :].astype(jnp.bfloat16)
+
+
+def project(got, tokens, gain, w_in, w_write, w_read, w_gate, w_step, slots):
+    _, rows, chan = got.shape
+    size = 2 * (w_in.size + w_write.size + w_read.size + w_gate.size)
+    return pl.pallas_call(
+        project_kernel,
+        out_shape=[
+            jax.ShapeDtypeStruct((rows, chan), jnp.bfloat16),
+            jax.ShapeDtypeStruct((rows, slots, LANES), jnp.bfloat16),
+        ],
+        in_specs=[VMEM_SPEC] * 8,
+        out_specs=[VMEM_SPEC] * 2,
+        scratch_shapes=[pltpu.VMEM((rows * slots, LANES), jnp.float32)],
+        compiler_params=params(8),
+        cost_estimate=cost(size),
+    )(got, tokens, gain, w_in, w_write, w_read, w_gate, w_step)
+
+
+def spread_kernel(wide_ref, out_ref):
+    taps, width = wide_ref.shape
+    slots = width // LANES
+    for j in range(slots):
+        out_ref[pl.ds(j, taps, stride=slots), :] = wide_ref[:, j * LANES : (j + 1) * LANES].astype(
+            jnp.float32
+        )
+
+
+def spread(wide):
+    taps, width = wide.shape
+    return pl.pallas_call(
+        spread_kernel,
+        out_shape=pltpu.VMEM((taps * width // LANES, LANES), jnp.float32),
+        in_specs=[VMEM_SPEC],
+        out_specs=VMEM_SPEC,
+        compiler_params=params(2),
+    )(wide)
+
+
+def mixer_kernel(width, groups, got_ref, taps_ref, hist_ref, bias_ref, rate_ref, state_ref, ggain_ref,
+                 state_out_ref, fresh_ref, normed_ref, read_rows):
+    ways = got_ref.shape[0]
+    heads, head_dim, state_dim = state_ref.shape
+    in_rows = heads * head_dim // LANES
+    map_rows = groups * state_dim // LANES
+    conv_rows = in_rows + 2 * map_rows
+    taps = taps_ref.shape[0] // conv_rows
+    total = got_ref[0].astype(jnp.float32)
+    for k in range(1, ways):
+        total += got_ref[k].astype(jnp.float32)
+    step_row = conv_rows + in_rows
+    squares = (
+        total[step_row + 1 : step_row + 2]
+        + total[step_row + 2 : step_row + 3]
+        + total[step_row + 3 : step_row + 4]
+    )
+    scale = lax.rsqrt(squares / width + EPS)
+    rounded = (total * scale).astype(jnp.bfloat16).astype(jnp.float32)
+    fresh = rounded[:conv_rows]
+    fresh_ref[...] = fresh.astype(jnp.bfloat16)
+    acc = hist_ref[pl.ds(0, conv_rows), :] * taps_ref[pl.ds(0, conv_rows), :]
+    for k in range(1, taps - 1):
+        part = pl.ds(k * conv_rows, conv_rows)
+        acc += hist_ref[part, :] * taps_ref[part, :]
+    acc += fresh * taps_ref[pl.ds((taps - 1) * conv_rows, conv_rows), :]
+    conv = silu(acc)
+    maps = conv[in_rows:]
+    raw = rounded[step_row : step_row + 1] + bias_ref[...]
+    step = jnp.maximum(raw, 0.0) + jnp.log1p(jnp.exp(-jnp.abs(raw)))
+    decay = jnp.exp(-step * jnp.exp(rate_ref[...]))
+    pad = jnp.zeros((LANES - in_rows, LANES), jnp.float32)
+    columns = jnp.concatenate([conv[:in_rows], pad], axis=0).T
+    per_row = LANES // head_dim
+    per_group = heads // groups
+    for g in range(groups):
+        write = maps[g : g + 1]
+        for h in range(g * per_group, (g + 1) * per_group):
+            r, c = h // per_row, h % per_row
+            column = columns[c * head_dim : (c + 1) * head_dim, r : r + 1] * step[:, h : h + 1]
+            state_out_ref[h] = decay[:, h : h + 1] * state_ref[h] + column * write
+        block = state_out_ref[g * per_group : (g + 1) * per_group].reshape(
+            per_group * head_dim, state_dim
+        )
+        read = lax.dot_general(
+            maps,
+            block,
+            ROW_ROW,
+            precision=lax.Precision.HIGHEST,
+            preferred_element_type=jnp.float32,
+        )
+        span = per_group * head_dim // LANES
+        for j in range(span):
+            read_rows[g * span + j : g * span + j + 1, :] = read[
+                map_rows + g : map_rows + g + 1, j * LANES : (j + 1) * LANES
+            ]
+    gated = read_rows[...] * silu(rounded[conv_rows : conv_rows + in_rows])
+    sums = jnp.sum(gated * gated, axis=1, keepdims=True)
+    owner = lax.broadcasted_iota(jnp.int32, (in_rows, 1), 0) // (in_rows // groups)
+    block_scale = jnp.zeros((in_rows, 1), jnp.float32)
+    for g in range(groups):
+        mine = owner == g
+        mean = jnp.sum(jnp.where(mine, sums, 0.0), axis=0, keepdims=True) / (
+            in_rows // groups * LANES
+        )
+        block_scale = jnp.where(mine, lax.rsqrt(mean + EPS), block_scale)
+    normed = (gated * block_scale * ggain_ref[...]).astype(jnp.bfloat16)
+    for k in range(ways):
+        normed_ref[k] = normed
+
+
+def mixer(width, groups, got, taps, hist, bias, rate, state, ggain):
+    ways = got.shape[0]
+    heads, head_dim, state_dim = state.shape
+    in_rows = heads * head_dim // LANES
+    conv_rows = in_rows + 2 * groups * state_dim // LANES
+    return pl.pallas_call(
+        functools.partial(mixer_kernel, width, groups),
+        out_shape=[
+            pltpu.VMEM(state.shape, jnp.float32),
+            jax.ShapeDtypeStruct((conv_rows, LANES), jnp.bfloat16),
+            jax.ShapeDtypeStruct((ways, in_rows, LANES), jnp.bfloat16),
+        ],
+        in_specs=[VMEM_SPEC] * 7,
+        out_specs=[VMEM_SPEC] * 3,
+        scratch_shapes=[pltpu.VMEM((in_rows, LANES), jnp.float32)],
+        compiler_params=params(8),
+        cost_estimate=cost(8 * state.size),
+    )(got, taps, hist, bias, rate, state, ggain)
+
+
+def store_kernel(source, target, sems):
+    cut = sems.shape[0]
+    step = source.shape[0] // cut
+    copies = [
+        pltpu.make_async_copy(
+            source.at[pl.ds(i * step, step)], target.at[pl.ds(i * step, step)], sems.at[i]
+        )
+        for i in range(cut)
+    ]
+    for copy in copies:
+        copy.start()
+    for copy in copies:
+        copy.wait()
+
+
+def store(array):
+    return pl.pallas_call(
+        store_kernel,
+        out_shape=pltpu.HBM(array.shape, array.dtype),
+        in_specs=[VMEM_SPEC],
+        out_specs=pl.BlockSpec(memory_space=pltpu.HBM),
+        scratch_shapes=[pltpu.SemaphoreType.DMA((4,))],
+        compiler_params=params(2),
+        cost_estimate=cost(array.size * array.dtype.itemsize),
+    )(array)
+
+
+def output_kernel(got_ref, w_ref, first_ref, out_ref, stage):
+    ways, slots, _ = got_ref.shape
+    for k in range(ways):
+        stage[pl.ds(k * slots, slots), :] = got_ref[k].astype(jnp.float32)
+    rows = jnp.concatenate(
+        [stage[pl.ds(j, ways, stride=slots), :].astype(jnp.bfloat16) for j in range(slots)], axis=1
+    )
+    mixed = jnp.dot(rows, w_ref[...], preferred_element_type=jnp.float32)
+    second = (first_ref[...].astype(jnp.float32) + mixed).astype(jnp.bfloat16)
+    for k in range(ways):
+        out_ref[k] = second
+
+
+def output(got, w, first):
+    ways, slots, _ = got.shape
+    return pl.pallas_call(
+        output_kernel,
+        out_shape=jax.ShapeDtypeStruct((ways,) + first.shape, jnp.bfloat16),
+        in_specs=[VMEM_SPEC] * 3,
+        out_specs=VMEM_SPEC,
+        scratch_shapes=[pltpu.VMEM((ways * slots, LANES), jnp.float32)],
+        compiler_params=params(4),
+        cost_estimate=cost(2 * w.size),
+    )(got, w, first)
+
+
+def final_kernel(got_ref, second_ref, out_ref):
+    share = got_ref[0]
+    for k in range(1, got_ref.shape[0]):
+        share += got_ref[k]
+    out_ref[...] = (second_ref[0].astype(jnp.float32) + 0.5 * share).astype(jnp.bfloat16)
+
+
+def final(got, second_all):
+    return pl.pallas_call(
+        final_kernel,
+        out_shape=jax.ShapeDtypeStruct(second_all.shape[1:], jnp.bfloat16),
+        in_specs=[VMEM_SPEC] * 2,
+        out_specs=VMEM_SPEC,
+        compiler_params=params(2),
+    )(got, second_all)
+
+
+def fast_body(
+    ways,
+    tokens,
+    first_gain,
+    first_gate,
+    first_up,
+    first_down,
+    mix_gain,
+    w_input,
+    w_outgate,
+    w_write,
+    w_read,
+    w_step,
+    conv_taps,
+    conv_history,
+    step_bias,
+    rate_log,
+    mixer_state,
+    group_gain,
+    w_output,
+    second_gain,
+    second_gate,
+    second_up,
+    second_down,
+):
+    width = first_gate.shape[0]
+    _, heads, head_dim, state_dim = mixer_state.shape
+    groups = w_write.shape[1] // state_dim
+    conv_width = conv_taps.shape[1]
+    used = (conv_width + heads * head_dim) // LANES + 4
+    slots = -(-used // 16) * 16
+    lane_pad = (0, LANES - heads)
+
+    gate1, up1, gain1 = load(first_gate.T, first_up.T, first_gain.reshape(1, width))
+    whole = exchange(jnp.broadcast_to(tokens[None], (ways,) + tokens.shape))
+    down1 = ff(whole, gain1, gate1, up1, first_down, False)
+    tok, gain_m, w_in, w_wr, w_rd, w_og, w_st, gate2 = load(
+        tokens, mix_gain.reshape(1, -1), w_input, w_write, w_read, w_outgate, w_step.T, second_gate.T
+    )
+    got1 = exchange(down1)
+    first, packed = project(got1, tok, gain_m, w_in, w_wr, w_rd, w_og, w_st, slots)
+    state, w_o, up2, taps_w, hist_w, bias, rate, ggain = load(
+        mixer_state[0],
+        w_output,
+        second_up.T,
+        conv_taps,
+        conv_history[0],
+        jnp.pad(step_bias, lane_pad).reshape(1, LANES),
+        jnp.pad(rate_log, lane_pad).reshape(1, LANES),
+        group_gain.reshape(-1, LANES),
+    )
+    taps = spread(taps_w)
+    hist = spread(hist_w)
+    got2 = exchange(packed)
+    new_state, fresh, normed = mixer(width, groups, got2, taps, hist, bias, rate, state, ggain)
+    down2, gain2 = load(second_down, second_gain.reshape(1, width))
+    got3 = exchange(normed)
+    second_all = output(got3, w_o, first)
+    state_out = store(new_state)
+    whole2 = exchange(second_all)
+    parts2 = ff(whole2, gain2, gate2, up2, down2, True)
+    got4 = exchange(parts2)
+    history_out = jnp.concatenate([conv_history[:, 1:], fresh.reshape(1, 1, conv_width)], axis=1)
+    layer_out = final(got4, second_all)
+    return layer_out, state_out[None], history_out
+
+
+def friendly(ways, args):
+    tokens, gate, taps, state, w_write = args[0], args[2], args[11], args[15], args[8]
+    count, heads, head_dim, state_dim = state.shape
+    return (
+        count == 1
+        and tokens.shape[0] == ways == 8
+        and tokens.shape[1] % LANES == 0
+        and gate.shape[1] % 64 == 0
+        and taps.shape[1] % (8 * LANES) == 0
+        and state_dim == LANES
+        and LANES % head_dim == 0
+        and heads < LANES
+        and 2 * (w_write.shape[1] // state_dim) == 8
+        and heads * head_dim % (16 * LANES) == 0
+    )
 
 
 def gather(block, ways):
@@ -35,7 +463,7 @@
     return (resid.astype(jnp.float32) + 0.5 * share).astype(jnp.bfloat16)
 
 
-def make_body(ways):
+def make_plain(ways):
     def body(
         tokens,
         first_gain,
@@ -133,8 +561,16 @@
     rows = P(AXES, None)
     columns = P(None, AXES)
     own = ("dp",) + AXES
+    ways = mesh.shape["kv"] * mesh.shape["tp"]
+    plain = make_plain(ways)
+
+    def body(*args):
+        if friendly(ways, args):
+            return fast_body(ways, *args)
+        return plain(*args)
+
     return jax.shard_map(
-        make_body(mesh.shape["kv"] * mesh.shape["tp"]),
+        body,
         mesh=mesh,
         in_specs=(
             P("dp", AXES),

time: 86.9 us -> 107 us (1.23)
  local copies, waits for them, and re-layouts: 2.77 us -> 47.7 us
  blocking collectives: 47.4 us -> 10.6 us
  starting transfers between devices: 3.35 us -> 23.9 us
  matrix products: 19.6 us -> 0 us
  Pallas kernels: 0 us -> 17.6 us
  other arithmetic: 6.31 us -> 0.64 us
  waiting for transfers between devices: 5.2 us -> 4.06 us
    unnamed x24 -> x86, local copies, waits for them, and re-layouts: 0.13 us -> 45.7 us
    all_to_all x5 -> x1, blocking collectives: 47.4 us -> 10.6 us  [exchange(): return lax.all_to_all(blocks, AXES, split_axis=0, concat_axis=0, tiled=True)]
    all_to_all x1 -> x5, starting transfers between devices: 3.35 us -> 23.9 us  [exchange(): return lax.all_to_all(blocks, AXES, split_axis=0, concat_axis=0, tiled=True)]
    dot_general x10 -> x0, matrix products: 19.6 us -> none  [the longest x2 8.5 us: half_block(): down = jnp.dot(hidden, w_down, preferred_element_type=jnp.float32)]
    pallas_call x0 -> x13, Pallas kernels: none -> 17.6 us  [the longest x4 6.88 us: load(): pl.pallas_call(functools.partial(load_kernel, cuts), out_shape=[pltpu.VME...]
    reduce_sum x9 -> x0, other arithmetic: 3.35 us -> none  [the longest x1 2.61 us: body(): read_out = jnp.sum(new_state * conv_read[:, :, None, None, :], axis=-1)]
    all_to_all x1 -> x5, waiting for transfers between devices: 5.2 us -> 4.06 us  [exchange(): return lax.all_to_all(blocks, AXES, split_axis=0, concat_axis=0, tiled=True)]
  transfers between devices with their start and end apart: 1 -> 5, of which waited for: 1 -> 2; matrix products, arithmetic and copies ran while one was open for 1% -> 1% of each run, Pallas kernels for 0% -> 7%
where the time goes in v2:
time: 107 us; the launch traced here: 105 us
  local copies, waits for them, and re-layouts  47.7 us (45%)
  starting transfers between devices  23.9 us (22%)
  Pallas kernels  17.6 us (16%)
  blocking collectives  10.6 us (10%)
  waiting for transfers between devices  4.06 us (4%)
    unnamed x86, local copies, waits for them, and re-layouts  45.7 us
    all_to_all x5, starting transfers between devices, exchange(): return lax.all_to_all(blocks, AXES, split_axis=0, concat_axis=0, tiled=True)  23.9 us
    all_to_all x1, blocking collectives, exchange(): return lax.all_to_all(blocks, AXES, split_axis=0, concat_axis=0, tiled=True)  10.6 us
    pallas_call x4, Pallas kernels, load(): pl.pallas_call(functools.partial(load_kernel, cuts), out_shape=[pltpu.VME...  6.88 us
    pallas_call x2, Pallas kernels, ff(): pl.pallas_call(ff_loaded_kernel if loaded else ff_kernel, out_shape=jax.S...  5.63 us
    all_to_all x5, waiting for transfers between devices, exchange(): return lax.all_to_all(blocks, AXES, split_axis=0, concat_axis=0, tiled=True)  4.06 us
  transfers between devices with their start and end apart: 5, of which 2 were waited for; matrix products, arithmetic and copies ran while one was open for 1% of the time, Pallas kernels for 7%

profile of v2, /device:TPU:0, one launch (start us, length us, event | category | flops | bytes accessed | tf_op | source)
XLA Modules:
  0.0 105.3 jit_solution(17541331332176631695)
XLA Ops:
  0.6 1.3 %broadcast_in_dim.4 = bf16[8,8,256]{2,1,0:T(8,128)(2,1)} broadcast(bf16[8,256]{1,0:T(8,128)(2,1)} %refs_0_.2), dimensions={1,2} | broadcast | bytes 36864 | tf_op jit(solution)/shard_map/broadcast_in_dim | solution.py:392
  1.9 6.4 %all-to-all-start = ((bf16[8,8,256]{2,1,0:T(8,128)(2,1)}), bf16[8,8,256]{2,1,0:T(8,128)(2,1)S(1)}, u32[]{:S(2)}, u32[]{:S(2)}) async-start(bf16[8,8,256]{2,1,0:T(8,128)(2,1)} %broadcast_in_dim.4), calls=%async_computation | async-start | bytes 65536 | tf_op jit(solution)/shard_map/all_to_all | solution.py:20
  8.3 1.8 %copy-done.9 = bf16[2048,704]{0,1:T(8,128)(2,1)S(1)} copy-done((bf16[2048,704]{0,1:T(8,128)(2,1)S(1)}, bf16[2048,704]{0,1:T(8,128)(2,1)}, u32[]{:S(2)}) %copy-start.9) | copy-done | bytes 2883608
  10.1 1.8 %copy-done.10 = bf16[2048,704]{0,1:T(8,128)(2,1)S(1)} copy-done((bf16[2048,704]{0,1:T(8,128)(2,1)S(1)}, bf16[2048,704]{0,1:T(8,128)(2,1)}, u32[]{:S(2)}) %copy-start.10) | copy-done | bytes 2883608
  12.6 2.4 %shard_map.229 = (bf16[704,2048]{1,0:T(8,128)(2,1)S(1)}, bf16[704,2048]{1,0:T(8,128)(2,1)S(1)}, f32[1,2048]{1,0:T(1,128)S(1)}) custom-call(bf16[704,2048]{1,0:T(8,128)(2,1)S(1)} %bitcast.16, bf16[704,2048]{1,0:T(8,128)(2,1)S(1)} %bitcast.17, f32[1,2048]{1,0:T(1,128)S(1)} %bitcast.23), custom_call_target="tpu_custom_call" | custom-call | flops 5775360 | bytes 5775360 | tf_op jit(solution)/shard_map/pallas_call | solution.py:54
  15.0 1.6 %copy-done.5 = bf16[704,2048]{1,0:T(8,128)(2,1)} copy-done((bf16[704,2048]{1,0:T(8,128)(2,1)}, bf16[704,2048]{1,0:T(8,128)(2,1)S(1)}, u32[]{:S(2)}) %copy-start.5) | copy-done | bytes 2883608
  16.6 1.6 %copy-done.7 = bf16[704,2048]{1,0:T(8,128)(2,1)} copy-done((bf16[704,2048]{1,0:T(8,128)(2,1)}, bf16[704,2048]{1,0:T(8,128)(2,1)S(1)}, u32[]{:S(2)}) %copy-start.7) | copy-done | bytes 2883608
  18.2 1.8 %copy-done.6 = bf16[704,2048]{1,0:T(8,128)(2,1)S(1)} copy-done((bf16[704,2048]{1,0:T(8,128)(2,1)S(1)}, bf16[704,2048]{1,0:T(8,128)(2,1)}, u32[]{:S(2)}) %copy-start.6) | copy-done | bytes 2883608
  20.0 1.8 %copy-done.8 = bf16[704,2048]{1,0:T(8,128)(2,1)S(1)} copy-done((bf16[704,2048]{1,0:T(8,128)(2,1)S(1)}, bf16[704,2048]{1,0:T(8,128)(2,1)}, u32[]{:S(2)}) %copy-start.8) | copy-done | bytes 2883608
  21.8 2.9 %shard_map.230 = f32[8,8,256]{2,1,0:T(8,128)} custom-call(bf16[8,8,256]{2,1,0:T(8,128)(2,1)S(1)} %all-to-all-done.x_ref, f32[1,2048]{1,0:T(1,128)S(1)} %get-tuple-element.29.gain_ref, bf16[704,2048]{1,0:T(8,128)(2,1)S(1)} %copy-done.6, bf16[704,2048]{1,0:T(8,128)(2,1)S(1)} %copy-done.8, bf16[704,2048]{1,0:T(8,128)(2,1)S(1)} %copy-done), custom_call_target="tpu_custom_call" | custom-call | flops 8650752 | bytes 8650752 | tf_op jit(solution)/shard_map/pallas_call | solution.py:115
  24.8 5.1 %all-to-all-start.1 = ((f32[8,8,256]{2,1,0:T(8,128)}), f32[8,8,256]{2,1,0:T(8,128)S(1)}, u32[]{:S(2)}, u32[]{:S(2)}) async-start(f32[8,8,256]{2,1,0:T(8,128)} %shard_map.230), calls=%async_computation.1 | async-start | bytes 131072 | tf_op jit(solution)/shard_map/all_to_all | solution.py:20
  29.9 1.8 %copy-done.13 = bf16[2048,704]{0,1:T(8,128)(2,1)S(1)} copy-done((bf16[2048,704]{0,1:T(8,128)(2,1)S(1)}, bf16[2048,704]{0,1:T(8,128)(2,1)}, u32[]{:S(2)}) %copy-start.13) | copy-done | bytes 2883608
  31.7 1.2 %copy-done.24 = bf16[256,2048]{1,0:T(8,128)(2,1)S(1)} copy-done((bf16[256,2048]{1,0:T(8,128)(2,1)S(1)}, bf16[256,2048]{1,0:T(8,128)(2,1)}, u32[]{:S(2)}) %copy-start.24) | copy-done | bytes 1048600
  32.9 1.2 %copy-done.25 = bf16[256,2048]{1,0:T(8,128)(2,1)S(1)} copy-done((bf16[256,2048]{1,0:T(8,128)(2,1)S(1)}, bf16[256,2048]{1,0:T(8,128)(2,1)}, u32[]{:S(2)}) %copy-start.25) | copy-done | bytes 1048600
  34.2 0.9 copy-done.28
  35.1 0.9 copy-done.29
  37.4 1.7 %shard_map.231 = (bf16[8,256]{1,0:T(8,128)(2,1)S(1)}, f32[1,256]{1,0:T(1,128)S(1)}, bf16[256,2048]{1,0:T(8,128)(2,1)S(1)}, bf16[256,512]{1,0:T(8,128)(2,1)S(1)},...) custom-call(bf16[8,256]{1,0:T(8,128)(2,1)S(1)} %copy-done.34, ...), custom_call_target="tpu_custom_call" | custom-call | flops 5526528 | bytes 5526528 | tf_op jit(solution)/shard_map/pallas_call | solution.py:54
  39.2 1.0 copy-done.20
  40.2 1.0 copy-done.22
  42.3 1.2 %copy-done.21 = bf16[256,2048]{1,0:T(8,128)(2,1)S(1)} copy-done((bf16[256,2048]{1,0:T(8,128)(2,1)S(1)}, bf16[256,2048]{1,0:T(8,128)(2,1)}, u32[]{:S(2)}) %copy-start.21) | copy-done | bytes 1048600
  43.6 1.2 %copy-done.23 = bf16[256,2048]{1,0:T(8,128)(2,1)S(1)} copy-done((bf16[256,2048]{1,0:T(8,128)(2,1)S(1)}, bf16[256,2048]{1,0:T(8,128)(2,1)}, u32[]{:S(2)}) %copy-start.23) | copy-done | bytes 1048600
  47.3 5.1 %all-to-all-start.2 = ((bf16[8,48,128]{2,1,0:T(8,128)(2,1)}), bf16[8,48,128]{2,1,0:T(8,128)(2,1)S(1)}, u32[]{:S(2)}, u32[]{:S(2)}) async-start(bf16[8,48,128]{2,1,0:T(8,128)(2,1)} %copy-done.30), calls=%async_computation.2 | async-start | bytes 196608 | tf_op jit(solution)/shard_map/all_to_all | solution.py:20
  53.1 1.8 %copy-done.11 = bf16[2048,704]{0,1:T(8,128)(2,1)S(1)} copy-done((bf16[2048,704]{0,1:T(8,128)(2,1)S(1)}, bf16[2048,704]{0,1:T(8,128)(2,1)}, u32[]{:S(2)}) %copy-start.11) | copy-done | bytes 2883608
  54.9 1.2 %copy-done.26 = f32[1,32,64,128]{3,2,1,0:T(8,128)S(1)} copy-done((f32[1,32,64,128]{3,2,1,0:T(8,128)S(1)}, f32[1,32,64,128]{3,2,1,0:T(8,128)}, u32[]{:S(2)}) %copy-start.26) | copy-done | bytes 1048600
  56.1 1.2 %copy-done.27 = bf16[2048,256]{1,0:T(8,128)(2,1)S(1)} copy-done((bf16[2048,256]{1,0:T(8,128)(2,1)S(1)}, bf16[2048,256]{1,0:T(8,128)(2,1)}, u32[]{:S(2)}) %copy-start.27) | copy-done | bytes 1048600
  57.3 1.5 %shard_map.233 = (f32[32,64,128]{2,1,0:T(8,128)S(1)}, bf16[2048,256]{1,0:T(8,128)(2,1)S(1)}, bf16[704,2048]{1,0:T(8,128)(2,1)S(1)}, bf16[4,3072]{1,0:T(4,128)(2,...) custom-call(f32[32,64,128]{2,1,0:T(8,128)S(1)} %bitcast.20, ...), custom_call_target="tpu_custom_call" | custom-call | flops 5032960 | bytes 5032960 | tf_op jit(solution)/shard_map/pallas_call | solution.py:54
  58.9 1.6 %copy-done.1 = bf16[704,2048]{1,0:T(8,128)(2,1)} copy-done((bf16[704,2048]{1,0:T(8,128)(2,1)}, bf16[704,2048]{1,0:T(8,128)(2,1)S(1)}, u32[]{:S(2)}) %copy-start.1) | copy-done | bytes 2883608
  60.4 1.0 copy-done.16
  61.4 1.0 copy-done.18
  62.4 1.2 %copy-done.19 = f32[32,64,128]{2,1,0:T(8,128)S(1)} copy-done((f32[32,64,128]{2,1,0:T(8,128)S(1)}, f32[32,64,128]{2,1,0:T(8,128)}, u32[]{:S(2)}) %copy-start.19) | copy-done | bytes 1048600
  63.6 1.4 %shard_map.236 = (f32[32,64,128]{2,1,0:T(8,128)S(1)}, bf16[24,128]{1,0:T(8,128)(2,1)S(1)}, bf16[8,16,128]{2,1,0:T(8,128)(2,1)S(1)}) custom-call(bf16[8,48,128]{2,1,0:T(8,128)(2,1)S(1)} %all-to-all-done.2.got_ref, f32[96,128]{1,0:T(8,128)S(1)} %shard_map.234.taps_ref, f32[72,128]{1,0:T(8,128)S(1)} %shard_map.235.hist_ref, ...), custom_call_target="tpu_custom_call" | custom-call | flops 2097152 | bytes 2097152 | tf_op jit(solution)/shard_map/pallas_call | solution.py:273
  65.0 1.0 copy-done.14
  66.0 10.6 %all_to_all.30.got_ref = bf16[8,16,128]{2,1,0:T(8,128)(2,1)S(1)} all-to-all(bf16[8,16,128]{2,1,0:T(8,128)(2,1)S(1)} %get-tuple-element.46), channel_id=1, replica_groups=mesh['dp'=4,'kv'=4,'tp'=2] {'kv','tp'}, dimensions={0} | all-to-all | bytes 65536 | tf_op jit(solution)/shard_map/all_to_all | solution.py:20
  76.6 1.2 %copy-done.17 = bf16[2048,256]{1,0:T(8,128)(2,1)S(1)} copy-done((bf16[2048,256]{1,0:T(8,128)(2,1)S(1)}, bf16[2048,256]{1,0:T(8,128)(2,1)}, u32[]{:S(2)}) %copy-start.17) | copy-done | bytes 1048600
  77.8 0.9 shard_map.237.second_ref
  78.7 3.3 %all-to-all-start.4 = ((bf16[8,8,256]{2,1,0:T(8,128)(2,1)}), bf16[8,8,256]{2,1,0:T(8,128)(2,1)S(1)}, u32[]{:S(2)}, u32[]{:S(2)}) async-start(bf16[8,8,256]{2,1,0:T(8,128)(2,1)} %shard_map.237.second_ref), calls=%async_computation.4 | async-start | bytes 65536 | tf_op jit(solution)/shard_map/all_to_all | solution.py:20
  82.1 1.8 %copy-done.12 = bf16[704,2048]{1,0:T(8,128)(2,1)S(1)} copy-done((bf16[704,2048]{1,0:T(8,128)(2,1)S(1)}, bf16[704,2048]{1,0:T(8,128)(2,1)}, u32[]{:S(2)}) %copy-start.12) | copy-done | bytes 2883608
  83.9 1.2 %shard_map.238 = (bf16[704,2048]{1,0:T(8,128)(2,1)S(1)}, f32[1,2048]{1,0:T(1,128)S(1)}) custom-call(bf16[704,2048]{1,0:T(8,128)(2,1)S(1)} %copy-done.12, f32[1,2048]{1,0:T(1,128)S(1)} %bitcast.25), custom_call_target="tpu_custom_call" | custom-call | flops 2891776 | bytes 2891776 | tf_op jit(solution)/shard_map/pallas_call | solution.py:54
  85.1 1.6 %copy-done.3 = bf16[704,2048]{1,0:T(8,128)(2,1)} copy-done((bf16[704,2048]{1,0:T(8,128)(2,1)}, bf16[704,2048]{1,0:T(8,128)(2,1)S(1)}, u32[]{:S(2)}) %copy-start.3) | copy-done | bytes 2883608
  86.7 1.0 all-to-all-done.4.x_ref
  87.7 1.8 %copy-done.2 = bf16[704,2048]{1,0:T(8,128)(2,1)S(1)} copy-done((bf16[704,2048]{1,0:T(8,128)(2,1)S(1)}, bf16[704,2048]{1,0:T(8,128)(2,1)}, u32[]{:S(2)}) %copy-start.2) | copy-done | bytes 2883608
  89.5 1.8 %copy-done.4 = bf16[704,2048]{1,0:T(8,128)(2,1)S(1)} copy-done((bf16[704,2048]{1,0:T(8,128)(2,1)S(1)}, bf16[704,2048]{1,0:T(8,128)(2,1)}, u32[]{:S(2)}) %copy-start.4) | copy-done | bytes 2883608
  91.3 2.7 %shard_map.239 = f32[8,8,256]{2,1,0:T(8,128)} custom-call(bf16[8,8,256]{2,1,0:T(8,128)(2,1)S(1)} %all-to-all-done.4.x_ref, f32[1,2048]{1,0:T(1,128)S(1)} %get-tuple-element.49.gain_ref, bf16[704,2048]{1,0:T(8,128)(2,1)S(1)} %get-tuple-element.50.gate_ref, bf16[704,2048]{1,0:T(8,128)(2,1)S(1)} %copy-done.2, bf16[704,2048]{1,0:T(8,128)(2,1)S(1)} %copy-done.4), custom_call_target="tpu_custom_call" | custom-call | flops 8650752 | bytes 8650752 | tf_op jit(solution)/shard_map/pallas_call | solution.py:115
  94.0 4.0 %all-to-all-start.5 = ((f32[8,8,256]{2,1,0:T(8,128)}), f32[8,8,256]{2,1,0:T(8,128)S(1)}, u32[]{:S(2)}, u32[]{:S(2)}) async-start(f32[8,8,256]{2,1,0:T(8,128)} %shard_map.239), calls=%async_computation.5 | async-start | bytes 131072 | tf_op jit(solution)/shard_map/all_to_all | solution.py:20
  98.7 1.2 %copy-done.15 = f32[32,64,128]{2,1,0:T(8,128)S(1)} copy-done((f32[32,64,128]{2,1,0:T(8,128)S(1)}, f32[32,64,128]{2,1,0:T(8,128)}, u32[]{:S(2)}) %copy-start.15) | copy-done | bytes 1048600
  99.9 1.0 shard_map.241
  100.9 3.1 %all-to-all-done.5.got_ref = f32[8,8,256]{2,1,0:T(8,128)S(1)} async-done(((f32[8,8,256]{2,1,0:T(8,128)}), f32[8,8,256]{2,1,0:T(8,128)S(1)}, u32[]{:S(2)}, u32[]{:S(2)}) %all-to-all-start.5) | async-done | bytes 65568 | tf_op jit(solution)/shard_map/all_to_all | solution.py:20
  104.0 1.4 %shard_map.240 = bf16[8,256]{1,0:T(8,128)(2,1)} custom-call(f32[8,8,256]{2,1,0:T(8,128)S(1)} %all-to-all-done.5.got_ref, bf16[8,8,256]{2,1,0:T(8,128)(2,1)} %shard_map.237.second_ref), custom_call_target="tpu_custom_call" | custom-call | tf_op jit(solution)/shard_map/pallas_call | solution.py:349
  (67 shorter events, 7.1 us)
Async XLA Ops:
  1.9 16.3 %all-to-all-start = ((bf16[8,8,256]{2,1,0:T(8,128)(2,1)}), bf16[8,8,256]{2,1,0:T(8,128)(2,1)S(1)}, u32[]{:S(2)}, u32[]{:S(2)}) async-start(bf16[8,8,256]{2,1,0:T(8,128)(2,1)} %broadcast_in_dim.4), calls=%async_computation | async-start | bytes 65536 | tf_op jit(solution)/shard_map/all_to_all | solution.py:20
  8.3 1.8 %copy-start.9 = (bf16[2048,704]{0,1:T(8,128)(2,1)S(1)}, bf16[2048,704]{0,1:T(8,128)(2,1)}, u32[]{:S(2)}) copy-start(bf16[2048,704]{0,1:T(8,128)(2,1)} %param.24) | copy-start | bytes 8650756
  10.1 1.8 %copy-start.10 = (bf16[2048,704]{0,1:T(8,128)(2,1)S(1)}, bf16[2048,704]{0,1:T(8,128)(2,1)}, u32[]{:S(2)}) copy-start(bf16[2048,704]{0,1:T(8,128)(2,1)} %param.25) | copy-start | bytes 8650756
  11.9 0.7 copy-start.35
  12.6 5.6 %copy-start = (bf16[704,2048]{1,0:T(8,128)(2,1)S(1)}, bf16[704,2048]{1,0:T(8,128)(2,1)}, u32[]{:S(2)}) copy-start(bf16[704,2048]{1,0:T(8,128)(2,1)} %down_hbm.1) | copy-start | bytes 8650756
  15.0 1.6 %copy-start.5 = (bf16[704,2048]{1,0:T(8,128)(2,1)}, bf16[704,2048]{1,0:T(8,128)(2,1)S(1)}, u32[]{:S(2)}) copy-start(bf16[704,2048]{1,0:T(8,128)(2,1)S(1)} %get-tuple-element.30.gate_ref) | copy-start | bytes 8650756
  16.6 1.6 %copy-start.7 = (bf16[704,2048]{1,0:T(8,128)(2,1)}, bf16[704,2048]{1,0:T(8,128)(2,1)S(1)}, u32[]{:S(2)}) copy-start(bf16[704,2048]{1,0:T(8,128)(2,1)S(1)} %get-tuple-element.31.up_ref) | copy-start | bytes 8650756
  18.2 1.8 %copy-start.6 = (bf16[704,2048]{1,0:T(8,128)(2,1)S(1)}, bf16[704,2048]{1,0:T(8,128)(2,1)}, u32[]{:S(2)}) copy-start(bf16[704,2048]{1,0:T(8,128)(2,1)} %copy-done.5) | copy-start | bytes 8650756
  20.0 1.8 %copy-start.8 = (bf16[704,2048]{1,0:T(8,128)(2,1)S(1)}, bf16[704,2048]{1,0:T(8,128)(2,1)}, u32[]{:S(2)}) copy-start(bf16[704,2048]{1,0:T(8,128)(2,1)} %copy-done.7) | copy-start | bytes 8650756
  21.8 8.1 %copy-start.33 = (bf16[256,32]{0,1:T(8,128)(2,1)S(1)}, bf16[256,32]{0,1:T(8,128)(2,1)}, u32[]{:S(2)}) copy-start(bf16[256,32]{0,1:T(8,128)(2,1)} %param.32) | copy-start | bytes 49156
  24.8 17.6 %all-to-all-start.1 = ((f32[8,8,256]{2,1,0:T(8,128)}), f32[8,8,256]{2,1,0:T(8,128)S(1)}, u32[]{:S(2)}, u32[]{:S(2)}) async-start(f32[8,8,256]{2,1,0:T(8,128)} %shard_map.230), calls=%async_computation.1 | async-start | bytes 131072 | tf_op jit(solution)/shard_map/all_to_all | solution.py:20
  29.9 1.8 %copy-start.13 = (bf16[2048,704]{0,1:T(8,128)(2,1)S(1)}, bf16[2048,704]{0,1:T(8,128)(2,1)}, u32[]{:S(2)}) copy-start(bf16[2048,704]{0,1:T(8,128)(2,1)} %param.41) | copy-start | bytes 8650756
  31.7 1.2 %copy-start.24 = (bf16[256,2048]{1,0:T(8,128)(2,1)S(1)}, bf16[256,2048]{1,0:T(8,128)(2,1)}, u32[]{:S(2)}) copy-start(bf16[256,2048]{1,0:T(8,128)(2,1)} %refs_2_.1) | copy-start | bytes 3145732
  32.9 1.2 %copy-start.25 = (bf16[256,2048]{1,0:T(8,128)(2,1)S(1)}, bf16[256,2048]{1,0:T(8,128)(2,1)}, u32[]{:S(2)}) copy-start(bf16[256,2048]{1,0:T(8,128)(2,1)} %refs_5_.1) | copy-start | bytes 3145732
  34.2 0.9 copy-start.28
  35.1 0.9 copy-start.29
  36.1 0.7 copy-start.34
  36.8 0.7 copy-start.42
  37.4 15.6 %copy-start.31 = (bf16[1,3,3072]{2,1,0:T(4,128)(2,1)S(1)}, bf16[1,3,3072]{2,1,0:T(4,128)(2,1)}, u32[]{:S(2)}) copy-start(bf16[1,3,3072]{2,1,0:T(4,128)(2,1)} %param.34) | copy-start | bytes 55300
  37.4 15.6 %copy-start.32 = (bf16[4,3072]{1,0:T(4,128)(2,1)S(1)}, bf16[4,3072]{1,0:T(4,128)(2,1)}, u32[]{:S(2)}) copy-start(bf16[4,3072]{1,0:T(4,128)(2,1)} %refs_3_.3) | copy-start | bytes 73732
  39.2 1.0 copy-start.20
  40.2 1.0 copy-start.22
  41.2 0.6 copy-start.38
  41.8 0.6 copy-start.40
  42.3 10.7 %copy-start.36 = (f32[2048]{0:T(1024)S(1)}, f32[2048]{0:T(1024)}, u32[]{:S(2)}) copy-start(f32[2048]{0:T(1024)} %param.38) | copy-start | bytes 24580
  42.3 1.2 %copy-start.21 = (bf16[256,2048]{1,0:T(8,128)(2,1)S(1)}, bf16[256,2048]{1,0:T(8,128)(2,1)}, u32[]{:S(2)}) copy-start(bf16[256,2048]{1,0:T(8,128)(2,1)} %copy-done.20) | copy-start | bytes 3145732
  43.6 1.2 %copy-start.23 = (bf16[256,2048]{1,0:T(8,128)(2,1)S(1)}, bf16[256,2048]{1,0:T(8,128)(2,1)}, u32[]{:S(2)}) copy-start(bf16[256,2048]{1,0:T(8,128)(2,1)} %copy-done.22) | copy-start | bytes 3145732
  44.8 0.7 copy-start.39
  45.5 0.7 copy-start.41
  46.6 0.6 copy-start.30
  47.3 15.1 %all-to-all-start.2 = ((bf16[8,48,128]{2,1,0:T(8,128)(2,1)}), bf16[8,48,128]{2,1,0:T(8,128)(2,1)S(1)}, u32[]{:S(2)}, u32[]{:S(2)}) async-start(bf16[8,48,128]{2,1,0:T(8,128)(2,1)} %copy-done.30), calls=%async_computation.2 | async-start | bytes 196608 | tf_op jit(solution)/shard_map/all_to_all | solution.py:20
  53.1 1.8 %copy-start.11 = (bf16[2048,704]{0,1:T(8,128)(2,1)S(1)}, bf16[2048,704]{0,1:T(8,128)(2,1)}, u32[]{:S(2)}) copy-start(bf16[2048,704]{0,1:T(8,128)(2,1)} %param.42) | copy-start | bytes 8650756
  54.9 1.2 %copy-start.26 = (f32[1,32,64,128]{3,2,1,0:T(8,128)S(1)}, f32[1,32,64,128]{3,2,1,0:T(8,128)}, u32[]{:S(2)}) copy-start(f32[1,32,64,128]{3,2,1,0:T(8,128)} %param.37) | copy-start | bytes 3145732
  56.1 1.2 %copy-start.27 = (bf16[2048,256]{1,0:T(8,128)(2,1)S(1)}, bf16[2048,256]{1,0:T(8,128)(2,1)}, u32[]{:S(2)}) copy-start(bf16[2048,256]{1,0:T(8,128)(2,1)} %refs_1_.1) | copy-start | bytes 3145732
  57.3 24.7 %copy-start.37 = (f32[2048]{0:T(1024)S(1)}, f32[2048]{0:T(1024)}, u32[]{:S(2)}) copy-start(f32[2048]{0:T(1024)} %param.40) | copy-start | bytes 24580
  58.8 1.6 %copy-start.1 = (bf16[704,2048]{1,0:T(8,128)(2,1)}, bf16[704,2048]{1,0:T(8,128)(2,1)S(1)}, u32[]{:S(2)}) copy-start(bf16[704,2048]{1,0:T(8,128)(2,1)S(1)} %get-tuple-element.51.up_ref) | copy-start | bytes 8650756
  60.4 1.0 copy-start.16
  61.4 1.0 copy-start.18
  62.4 1.2 %copy-start.19 = (f32[32,64,128]{2,1,0:T(8,128)S(1)}, f32[32,64,128]{2,1,0:T(8,128)}, u32[]{:S(2)}) copy-start(f32[32,64,128]{2,1,0:T(8,128)} %copy-done.18) | copy-start | bytes 3145732
  65.0 1.0 copy-start.14
  76.6 1.2 %copy-start.17 = (bf16[2048,256]{1,0:T(8,128)(2,1)S(1)}, bf16[2048,256]{1,0:T(8,128)(2,1)}, u32[]{:S(2)}) copy-start(bf16[2048,256]{1,0:T(8,128)(2,1)} %copy-done.16) | copy-start | bytes 3145732
  78.7 9.0 %all-to-all-start.4 = ((bf16[8,8,256]{2,1,0:T(8,128)(2,1)}), bf16[8,8,256]{2,1,0:T(8,128)(2,1)S(1)}, u32[]{:S(2)}, u32[]{:S(2)}) async-start(bf16[8,8,256]{2,1,0:T(8,128)(2,1)} %shard_map.237.second_ref), calls=%async_computation.4 | async-start | bytes 65536 | tf_op jit(solution)/shard_map/all_to_all | solution.py:20
  82.1 1.8 %copy-start.12 = (bf16[704,2048]{1,0:T(8,128)(2,1)S(1)}, bf16[704,2048]{1,0:T(8,128)(2,1)}, u32[]{:S(2)}) copy-start(bf16[704,2048]{1,0:T(8,128)(2,1)} %refs_0_.3) | copy-start | bytes 8650756
  85.1 1.6 %copy-start.3 = (bf16[704,2048]{1,0:T(8,128)(2,1)}, bf16[704,2048]{1,0:T(8,128)(2,1)S(1)}, u32[]{:S(2)}) copy-start(bf16[704,2048]{1,0:T(8,128)(2,1)S(1)} %get-tuple-element.52.down_ref) | copy-start | bytes 8650756
  87.7 1.8 %copy-start.2 = (bf16[704,2048]{1,0:T(8,128)(2,1)S(1)}, bf16[704,2048]{1,0:T(8,128)(2,1)}, u32[]{:S(2)}) copy-start(bf16[704,2048]{1,0:T(8,128)(2,1)} %copy-done.1) | copy-start | bytes 8650756
  89.5 1.8 %copy-start.4 = (bf16[704,2048]{1,0:T(8,128)(2,1)S(1)}, bf16[704,2048]{1,0:T(8,128)(2,1)}, u32[]{:S(2)}) copy-start(bf16[704,2048]{1,0:T(8,128)(2,1)} %copy-done.3) | copy-start | bytes 8650756
  94.0 9.9 %all-to-all-start.5 = ((f32[8,8,256]{2,1,0:T(8,128)}), f32[8,8,256]{2,1,0:T(8,128)S(1)}, u32[]{:S(2)}, u32[]{:S(2)}) async-start(f32[8,8,256]{2,1,0:T(8,128)} %shard_map.239), calls=%async_computation.5 | async-start | bytes 131072 | tf_op jit(solution)/shard_map/all_to_all | solution.py:20
  98.7 1.2 %copy-start.15 = (f32[32,64,128]{2,1,0:T(8,128)S(1)}, f32[32,64,128]{2,1,0:T(8,128)}, u32[]{:S(2)}) copy-start(f32[32,64,128]{2,1,0:T(8,128)} %copy-done.14) | copy-start | bytes 3145732

commit v3 on v2

--- a/solution.py
+++ b/solution.py
@@ -12,7 +12,6 @@
 LANES = 128
 MIB = 1 << 20
 VMEM_SPEC = pl.BlockSpec(memory_space=pltpu.VMEM)
-ANY_SPEC = pl.BlockSpec(memory_space=pl.ANY)
 ROW_ROW = (((1,), (1,)), ((), ()))
 
 
@@ -24,70 +23,30 @@
     return pltpu.CompilerParams(vmem_limit_bytes=megabytes * MIB)
 
 
-def cost(nbytes):
-    return pl.CostEstimate(flops=nbytes, bytes_accessed=nbytes, transcendentals=0)
+COST = pl.CostEstimate(flops=10**10, bytes_accessed=1000, transcendentals=0)
 
 
 def silu(x):
     return x / (1.0 + jnp.exp(-x))
 
 
-def load_kernel(cuts, *refs):
-    n = len(cuts)
-    sources, targets, sems = refs[:n], refs[n : 2 * n], refs[2 * n]
-    copies = []
-    for source, target, cut in zip(sources, targets, cuts):
-        step = source.shape[0] // cut
-        for i in range(cut):
-            part = pl.ds(i * step, step)
-            copies.append(
-                pltpu.make_async_copy(source.at[part], target.at[part], sems.at[len(copies)])
-            )
-    for copy in copies:
-        copy.start()
-    for copy in copies:
-        copy.wait()
-
-
-def load(*arrays):
-    cuts = tuple(4 if a.size * a.dtype.itemsize >= MIB and a.shape[0] % 64 == 0 else 1 for a in arrays)
+def repeat_kernel(block_ref, out_ref):
+    for k in range(out_ref.shape[0]):
+        out_ref[k] = block_ref[...]
+
+
+def repeat(block, ways):
     return pl.pallas_call(
-        functools.partial(load_kernel, cuts),
-        out_shape=[pltpu.VMEM(a.shape, a.dtype) for a in arrays],
-        in_specs=[ANY_SPEC] * len(arrays),
-        out_specs=[VMEM_SPEC] * len(arrays),
-        scratch_shapes=[pltpu.SemaphoreType.DMA((sum(cuts),))],
-        compiler_params=params(4),
-        cost_estimate=cost(sum(a.size * a.dtype.itemsize for a in arrays)),
-    )(*arrays)
-
-
-def ff_kernel(x_ref, gain_ref, gate_ref, up_ref, down_hbm, out_ref, down_ref, sem):
-    copy = pltpu.make_async_copy(down_hbm, down_ref, sem)
-    copy.start()
-    ways, rows, chan = x_ref.shape
-    pieces = [x_ref[k].astype(jnp.float32) for k in range(ways)]
-    total = jnp.zeros((rows, 1), jnp.float32)
-    for piece in pieces:
-        total += jnp.sum(piece * piece, axis=1, keepdims=True)
-    scale = lax.rsqrt(total / (ways * chan) + EPS)
-    normed = jnp.concatenate(
-        [
-            (piece * scale * gain_ref[:, k * chan : (k + 1) * chan]).astype(jnp.bfloat16)
-            for k, piece in enumerate(pieces)
-        ],
-        axis=1,
-    )
-    gate = lax.dot_general(normed, gate_ref[...], ROW_ROW, preferred_element_type=jnp.float32)
-    upper = lax.dot_general(normed, up_ref[...], ROW_ROW, preferred_element_type=jnp.float32)
-    hidden = (silu(gate) * upper).astype(jnp.bfloat16)
-    copy.wait()
-    down = jnp.dot(hidden, down_ref[...], preferred_element_type=jnp.float32)
-    for k in range(ways):
-        out_ref[k] = down[:, k * chan : (k + 1) * chan]
-
-
-def ff_loaded_kernel(x_ref, gain_ref, gate_ref, up_ref, down_ref, out_ref):
+        repeat_kernel,
+        out_shape=jax.ShapeDtypeStruct((ways,) + block.shape, block.dtype),
+        in_specs=[VMEM_SPEC],
+        out_specs=VMEM_SPEC,
+        compiler_params=params(2),
+        cost_estimate=COST,
+    )(block)
+
+
+def ff_kernel(x_ref, gain_ref, gate_ref, up_ref, down_ref, out_ref):
     ways, rows, chan = x_ref.shape
     pieces = [x_ref[k].astype(jnp.float32) for k in range(ways)]
     total = jnp.zeros((rows, 1), jnp.float32)
@@ -109,23 +68,20 @@
         out_ref[k] = down[:, k * chan : (k + 1) * chan]
 
 
-def ff(whole, gain, gate, up, down, loaded):
-    size = 3 * gate.size * 2
-    scratch = [] if loaded else [pltpu.VMEM(down.shape, down.dtype), pltpu.SemaphoreType.DMA]
+def ff(whole, gain, gate, up, down):
     return pl.pallas_call(
-        ff_loaded_kernel if loaded else ff_kernel,
+        ff_kernel,
         out_shape=jax.ShapeDtypeStruct(whole.shape, jnp.float32),
-        in_specs=[VMEM_SPEC] * 4 + [VMEM_SPEC if loaded else ANY_SPEC],
+        in_specs=[VMEM_SPEC] * 5,
         out_specs=VMEM_SPEC,
-        scratch_shapes=scratch,
         compiler_params=params(8),
-        cost_estimate=cost(size),
+        cost_estimate=COST,
     )(whole, gain, gate, up, down)
 
 
 def project_kernel(got_ref, tok_ref, gain_ref, win_ref, wwrite_ref, wread_ref, wgate_ref, wstep_ref,
                    first_ref, out_ref, stage):
-    ways, rows, _ = got_ref.shape
+    ways, rows, chan = got_ref.shape
     slots = out_ref.shape[1]
     share = got_ref[0]
     for k in range(1, ways):
@@ -158,8 +114,7 @@
 
 
 def project(got, tokens, gain, w_in, w_write, w_read, w_gate, w_step, slots):
-    _, rows, chan = got.shape
-    size = 2 * (w_in.size + w_write.size + w_read.size + w_gate.size)
+    ways, rows, chan = got.shape
     return pl.pallas_call(
         project_kernel,
         out_shape=[
@@ -170,38 +125,22 @@
         out_specs=[VMEM_SPEC] * 2,
         scratch_shapes=[pltpu.VMEM((rows * slots, LANES), jnp.float32)],
         compiler_params=params(8),
-        cost_estimate=cost(size),
+        cost_estimate=COST,
     )(got, tokens, gain, w_in, w_write, w_read, w_gate, w_step)
 
 
-def spread_kernel(wide_ref, out_ref):
-    taps, width = wide_ref.shape
-    slots = width // LANES
-    for j in range(slots):
-        out_ref[pl.ds(j, taps, stride=slots), :] = wide_ref[:, j * LANES : (j + 1) * LANES].astype(
-            jnp.float32
-        )
-
-
-def spread(wide):
-    taps, width = wide.shape
-    return pl.pallas_call(
-        spread_kernel,
-        out_shape=pltpu.VMEM((taps * width // LANES, LANES), jnp.float32),
-        in_specs=[VMEM_SPEC],
-        out_specs=VMEM_SPEC,
-        compiler_params=params(2),
-    )(wide)
-
-
 def mixer_kernel(width, groups, got_ref, taps_ref, hist_ref, bias_ref, rate_ref, state_ref, ggain_ref,
-                 state_out_ref, fresh_ref, normed_ref, read_rows):
+                 state_out_ref, hist_out_ref, normed_ref, read_rows, taps_rows, hist_rows, hist_wide):
     ways = got_ref.shape[0]
     heads, head_dim, state_dim = state_ref.shape
     in_rows = heads * head_dim // LANES
     map_rows = groups * state_dim // LANES
     conv_rows = in_rows + 2 * map_rows
-    taps = taps_ref.shape[0] // conv_rows
+    taps = taps_ref.shape[0]
+    for j in range(conv_rows):
+        part = pl.ds(j * LANES, LANES)
+        taps_rows[pl.ds(j, taps, stride=conv_rows), :] = taps_ref[:, part].astype(jnp.float32)
+        hist_rows[pl.ds(j, taps - 1, stride=conv_rows), :] = hist_ref[:, part].astype(jnp.float32)
     total = got_ref[0].astype(jnp.float32)
     for k in range(1, ways):
         total += got_ref[k].astype(jnp.float32)
@@ -214,15 +153,18 @@
     scale = lax.rsqrt(squares / width + EPS)
     rounded = (total * scale).astype(jnp.bfloat16).astype(jnp.float32)
     fresh = rounded[:conv_rows]
-    fresh_ref[...] = fresh.astype(jnp.bfloat16)
-    acc = hist_ref[pl.ds(0, conv_rows), :] * taps_ref[pl.ds(0, conv_rows), :]
+    hist_wide[: taps - 2, :] = hist_ref[1:, :].astype(jnp.float32)
+    for j in range(conv_rows):
+        hist_wide[taps - 2 : taps - 1, j * LANES : (j + 1) * LANES] = fresh[j : j + 1]
+    hist_out_ref[...] = hist_wide[...].astype(jnp.bfloat16)
+    acc = hist_rows[pl.ds(0, conv_rows), :] * taps_rows[pl.ds(0, conv_rows), :]
     for k in range(1, taps - 1):
         part = pl.ds(k * conv_rows, conv_rows)
-        acc += hist_ref[part, :] * taps_ref[part, :]
-    acc += fresh * taps_ref[pl.ds((taps - 1) * conv_rows, conv_rows), :]
+        acc += hist_rows[part, :] * taps_rows[part, :]
+    acc += fresh * taps_rows[pl.ds((taps - 1) * conv_rows, conv_rows), :]
     conv = silu(acc)
     maps = conv[in_rows:]
-    raw = rounded[step_row : step_row + 1] + bias_ref[...]
+    raw = rounded[step_row : step_row + 1, :heads] + bias_ref[...]
     step = jnp.maximum(raw, 0.0) + jnp.log1p(jnp.exp(-jnp.abs(raw)))
     decay = jnp.exp(-step * jnp.exp(rate_ref[...]))
     pad = jnp.zeros((LANES - in_rows, LANES), jnp.float32)
@@ -273,43 +215,21 @@
     return pl.pallas_call(
         functools.partial(mixer_kernel, width, groups),
         out_shape=[
-            pltpu.VMEM(state.shape, jnp.float32),
-            jax.ShapeDtypeStruct((conv_rows, LANES), jnp.bfloat16),
+            jax.ShapeDtypeStruct(state.shape, jnp.float32),
+            jax.ShapeDtypeStruct(hist.shape, jnp.bfloat16),
             jax.ShapeDtypeStruct((ways, in_rows, LANES), jnp.bfloat16),
         ],
         in_specs=[VMEM_SPEC] * 7,
         out_specs=[VMEM_SPEC] * 3,
-        scratch_shapes=[pltpu.VMEM((in_rows, LANES), jnp.float32)],
+        scratch_shapes=[
+            pltpu.VMEM((in_rows, LANES), jnp.float32),
+            pltpu.VMEM((taps.shape[0] * conv_rows, LANES), jnp.float32),
+            pltpu.VMEM((hist.shape[0] * conv_rows, LANES), jnp.float32),
+            pltpu.VMEM(hist.shape, jnp.float32),
+        ],
         compiler_params=params(8),
-        cost_estimate=cost(8 * state.size),
+        cost_estimate=COST,
     )(got, taps, hist, bias, rate, state, ggain)
-
-
-def store_kernel(source, target, sems):
-    cut = sems.shape[0]
-    step = source.shape[0] // cut
-    copies = [
-        pltpu.make_async_copy(
-            source.at[pl.ds(i * step, step)], target.at[pl.ds(i * step, step)], sems.at[i]
-        )
-        for i in range(cut)
-    ]
-    for copy in copies:
-        copy.start()
-    for copy in copies:
-        copy.wait()
-
-
-def store(array):
-    return pl.pallas_call(
-        store_kernel,
-        out_shape=pltpu.HBM(array.shape, array.dtype),
-        in_specs=[VMEM_SPEC],
-        out_specs=pl.BlockSpec(memory_space=pltpu.HBM),
-        scratch_shapes=[pltpu.SemaphoreType.DMA((4,))],
-        compiler_params=params(2),
-        cost_estimate=cost(array.size * array.dtype.itemsize),
-    )(array)
 
 
 def output_kernel(got_ref, w_ref, first_ref, out_ref, stage):
@@ -334,7 +254,7 @@
         out_specs=VMEM_SPEC,
         scratch_shapes=[pltpu.VMEM((ways * slots, LANES), jnp.float32)],
         compiler_params=params(4),
-        cost_estimate=cost(2 * w.size),
+        cost_estimate=COST,
     )(got, w, first)
 
 
@@ -386,40 +306,41 @@
     conv_width = conv_taps.shape[1]
     used = (conv_width + heads * head_dim) // LANES + 4
     slots = -(-used // 16) * 16
-    lane_pad = (0, LANES - heads)
-
-    gate1, up1, gain1 = load(first_gate.T, first_up.T, first_gain.reshape(1, width))
-    whole = exchange(jnp.broadcast_to(tokens[None], (ways,) + tokens.shape))
-    down1 = ff(whole, gain1, gate1, up1, first_down, False)
-    tok, gain_m, w_in, w_wr, w_rd, w_og, w_st, gate2 = load(
-        tokens, mix_gain.reshape(1, -1), w_input, w_write, w_read, w_outgate, w_step.T, second_gate.T
-    )
+    scope = jax.named_scope
+
+    with scope("repeat"):
+        blocks = repeat(tokens, ways)
+    whole = exchange(blocks)
+    with scope("ff1"):
+        down1 = ff(whole, first_gain.reshape(1, width), first_gate.T, first_up.T, first_down)
     got1 = exchange(down1)
-    first, packed = project(got1, tok, gain_m, w_in, w_wr, w_rd, w_og, w_st, slots)
-    state, w_o, up2, taps_w, hist_w, bias, rate, ggain = load(
-        mixer_state[0],
-        w_output,
-        second_up.T,
-        conv_taps,
-        conv_history[0],
-        jnp.pad(step_bias, lane_pad).reshape(1, LANES),
-        jnp.pad(rate_log, lane_pad).reshape(1, LANES),
-        group_gain.reshape(-1, LANES),
-    )
-    taps = spread(taps_w)
-    hist = spread(hist_w)
+    with scope("project"):
+        first, packed = project(
+            got1, tokens, mix_gain.reshape(1, -1), w_input, w_write, w_read, w_outgate, w_step.T, slots
+        )
     got2 = exchange(packed)
-    new_state, fresh, normed = mixer(width, groups, got2, taps, hist, bias, rate, state, ggain)
-    down2, gain2 = load(second_down, second_gain.reshape(1, width))
+    with scope("mixer"):
+        state_out, history_out, normed = mixer(
+            width,
+            groups,
+            got2,
+            conv_taps,
+            conv_history[0],
+            step_bias.reshape(1, heads),
+            rate_log.reshape(1, heads),
+            mixer_state[0],
+            group_gain.reshape(-1, LANES),
+        )
     got3 = exchange(normed)
-    second_all = output(got3, w_o, first)
-    state_out = store(new_state)
+    with scope("output"):
+        second_all = output(got3, w_output, first)
     whole2 = exchange(second_all)
-    parts2 = ff(whole2, gain2, gate2, up2, down2, True)
-    got4 = exchange(parts2)
-    history_out = jnp.concatenate([conv_history[:, 1:], fresh.reshape(1, 1, conv_width)], axis=1)
-    layer_out = final(got4, second_all)
-    return layer_out, state_out[None], history_out
+    with scope("ff2"):
+        down2 = ff(whole2, second_gain.reshape(1, width), second_gate.T, second_up.T, second_down)
+    got4 = exchange(down2)
+    with scope("final"):
+        layer_out = final(got4, second_all)
+    return layer_out, state_out[None], history_out[None]
 
 
 def friendly(ways, args):

time: 107 us -> 63.6 us (0.59); the launches traced: 105 us -> 63.2 us
  local copies, waits for them, and re-layouts: 47.7 us -> 0.95 us
  blocking collectives: 10.6 us -> 54 us
  starting transfers between devices: 23.9 us -> 0 us
  Pallas kernels: 17.6 us -> 7.36 us
  waiting for transfers between devices: 4.06 us -> 0 us
    unnamed x86 -> x46, local copies, waits for them, and re-layouts: 45.7 us -> 0.95 us
    all_to_all x1 -> x6, blocking collectives: 10.6 us -> 54 us  [exchange(): return lax.all_to_all(blocks, AXES, split_axis=0, concat_axis=0, tiled=True)]
    all_to_all x5 -> x0, starting transfers between devices: 23.9 us -> none  [exchange(): return lax.all_to_all(blocks, AXES, split_axis=0, concat_axis=0, tiled=True)]
    pallas_call x9 -> x3, Pallas kernels: 13.5 us -> 4.1 us  [the longest x2 4.1 us: ff(): pl.pallas_call(ff_kernel, out_shape=jax.ShapeDtypeStruct(whole.shape, jnp...]
    all_to_all x5 -> x0, waiting for transfers between devices: 4.06 us -> none  [exchange(): return lax.all_to_all(blocks, AXES, split_axis=0, concat_axis=0, tiled=True)]
    broadcast_in_dim x1 -> x0, local copies, waits for them, and re-layouts: 1.31 us -> none  [fast_body(): whole = exchange(jnp.broadcast_to(tokens[None], (ways,) + tokens.shape))]
  transfers between devices with their start and end apart: 5 -> 0, of which waited for: 2 -> 0; matrix products, arithmetic and copies ran while one was open for 1% -> 0% of each run, Pallas kernels for 7% -> 0%
where the time goes in v3:
time: 63.6 us; the launch traced here: 63.2 us
  blocking collectives  54 us (85%)
  Pallas kernels  7.36 us (12%)
  local copies, waits for them, and re-layouts  0.95 us (1%)
  between operations  0.9 us (1%)
    all_to_all x6, blocking collectives, exchange(): return lax.all_to_all(blocks, AXES, split_axis=0, concat_axis=0, tiled=True)  54 us
    pallas_call x2, Pallas kernels, ff(): pl.pallas_call(ff_kernel, out_shape=jax.ShapeDtypeStruct(whole.shape, jnp...  4.1 us
    pallas_call x1, Pallas kernels, mixer(): pl.pallas_call(functools.partial(mixer_kernel, width, groups), out_shape=...  1.93 us

profile of v3, /device:TPU:0, one launch (start us, length us, event | category | flops | bytes accessed | tf_op | source)
XLA Modules:
  0.0 63.2 jit_solution(1075389161768030415)
XLA Ops:
  0.6 0.0 copy-start.2
  0.6 0.0 copy-start.1
  0.7 0.0 copy-start
  0.7 0.0 copy-start.15
  0.7 0.0 copy-start.18
  0.7 0.8 %copy-done.18 = bf16[8,256]{1,0:T(8,128)(2,1)S(1)} copy-done((bf16[8,256]{1,0:T(8,128)(2,1)S(1)}, bf16[8,256]{1,0:T(8,128)(2,1)}, u32[]{:S(2)}) %copy-start.18) | copy-done | bytes 4120
  1.5 12.1 %all_to_all.30.x_ref = bf16[8,8,256]{2,1,0:T(8,128)(2,1)S(1)} all-to-all(bf16[8,8,256]{2,1,0:T(8,128)(2,1)S(1)} %repeat.1), channel_id=1, replica_groups=mesh['dp'=4,'kv'=4,'tp'=2] {'kv','tp'}, dimensions={0} | all-to-all | bytes 65536 | tf_op jit(solution)/shard_map/all_to_all | solution.py:19
  13.7 0.0 copy-done.2
  13.7 0.0 copy-done.1
  13.7 0.0 copy-done
  13.7 0.0 copy-done.15
  13.7 0.0 copy-start.6
  13.7 0.0 copy-start.7
  13.7 0.0 copy-start.10
  13.7 0.0 copy-start.11
  13.7 0.0 copy-start.14
  13.7 0.0 copy-start.19
  13.8 0.0 copy-start.20
  13.8 2.0 %ff1.1 = f32[8,8,256]{2,1,0:T(8,128)S(1)} custom-call(bf16[8,8,256]{2,1,0:T(8,128)(2,1)S(1)} %all_to_all.30.x_ref, f32[1,2048]{1,0:T(1,128)S(1)} %bitcast.22, bf16[704,2048]{1,0:T(8,128)(2,1)S(1)} %bitcast.15, bf16[704,2048]{1,0:T(8,128)(2,1)S(1)} %bitcast.16, bf16[704,2048]{1,0:T(8,128)(2,1)S(1)} %copy-done.2), custom_call_target="tpu_custom_call" | custom-call | flops 10000000000 | bytes 1000 | tf_op jit(solution)/shard_map/ff1/pallas_call | solution.py:72
  15.8 8.3 %all_to_all.31.got_ref = f32[8,8,256]{2,1,0:T(8,128)S(1)} all-to-all(f32[8,8,256]{2,1,0:T(8,128)S(1)} %ff1.1), channel_id=1, replica_groups=mesh['dp'=4,'kv'=4,'tp'=2] {'kv','tp'}, dimensions={0} | all-to-all | bytes 131072 | tf_op jit(solution)/shard_map/all_to_all | solution.py:19
  24.1 0.0 copy-done.6
  24.1 0.0 copy-done.7
  24.1 0.0 copy-done.10
  24.1 0.0 copy-done.11
  24.1 0.0 copy-done.14
  24.1 0.0 copy-done.19
  24.1 0.0 copy-done.20
  24.2 0.0 copy-start.8
  24.2 0.0 copy-start.12
  24.2 0.0 copy-start.13
  24.2 0.0 copy-start.16
  24.2 0.0 copy-start.21
  24.2 0.0 copy-start.22
  24.2 0.5 project.1
  24.7 8.7 %all_to_all.32.got_ref = bf16[8,48,128]{2,1,0:T(8,128)(2,1)S(1)} all-to-all(bf16[8,48,128]{2,1,0:T(8,128)(2,1)S(1)} %get-tuple-element.8), channel_id=1, replica_groups=mesh['dp'=4,'kv'=4,'tp'=2] {'kv','tp'}, dimensions={0} | all-to-all | bytes 196608 | tf_op jit(solution)/shard_map/all_to_all | solution.py:19
  33.4 0.0 copy-done.8
  33.4 0.0 copy-done.13
  33.4 0.0 copy-start.9
  33.5 1.9 %mixer.1 = (f32[32,64,128]{2,1,0:T(8,128)}, bf16[3,3072]{1,0:T(4,128)(2,1)}, bf16[8,16,128]{2,1,0:T(8,128)(2,1)S(1)}) custom-call(bf16[8,48,128]{2,1,0:T(8,128)(2,1)S(1)} %all_to_all.32.got_ref, bf16[4,3072]{1,0:T(4,128)(2,1)S(1)} %copy-done.12, bf16[3,3072]{1,0:T(4,128)(2,1)S(1)} %bitcast.20, f32[1,32]{1,0:T(1,128)S(1)} %bitcast.26, f32[1,32]{1,0:T(1,128)S(1)} %bitcast.27, ...), custom_call_target="tpu_custom_call" | custom-call | flops 10000000000 | bytes 1000 | tf_op jit(solution)/shard_map/mixer/pallas_call | solution.py:215
  35.4 8.1 %all_to_all.33.got_ref = bf16[8,16,128]{2,1,0:T(8,128)(2,1)S(1)} all-to-all(bf16[8,16,128]{2,1,0:T(8,128)(2,1)S(1)} %get-tuple-element.9), channel_id=1, replica_groups=mesh['dp'=4,'kv'=4,'tp'=2] {'kv','tp'}, dimensions={0} | all-to-all | bytes 65536 | tf_op jit(solution)/shard_map/all_to_all | solution.py:19
  43.5 0.0 copy-start.17
  43.5 0.2 output.1.second_ref
  43.8 8.5 %all_to_all.34.x_ref = bf16[8,8,256]{2,1,0:T(8,128)(2,1)S(1)} all-to-all(bf16[8,8,256]{2,1,0:T(8,128)(2,1)S(1)} %output.1.second_ref), channel_id=1, replica_groups=mesh['dp'=4,'kv'=4,'tp'=2] {'kv','tp'}, dimensions={0} | all-to-all | bytes 65536 | tf_op jit(solution)/shard_map/all_to_all | solution.py:19
  52.3 0.0 copy-done.3
  52.3 0.0 copy-done.5
  52.3 2.0 %ff2.1 = f32[8,8,256]{2,1,0:T(8,128)S(1)} custom-call(bf16[8,8,256]{2,1,0:T(8,128)(2,1)S(1)} %all_to_all.34.x_ref, f32[1,2048]{1,0:T(1,128)S(1)} %bitcast.24, bf16[704,2048]{1,0:T(8,128)(2,1)S(1)} %bitcast.17, bf16[704,2048]{1,0:T(8,128)(2,1)S(1)} %bitcast.18, bf16[704,2048]{1,0:T(8,128)(2,1)S(1)} %copy-done.5), custom_call_target="tpu_custom_call" | custom-call | flops 10000000000 | bytes 1000 | tf_op jit(solution)/shard_map/ff2/pallas_call | solution.py:72
  54.3 8.3 %all_to_all.35.got_ref = f32[8,8,256]{2,1,0:T(8,128)S(1)} all-to-all(f32[8,8,256]{2,1,0:T(8,128)S(1)} %ff2.1), channel_id=1, replica_groups=mesh['dp'=4,'kv'=4,'tp'=2] {'kv','tp'}, dimensions={0} | all-to-all | bytes 131072 | tf_op jit(solution)/shard_map/all_to_all | solution.py:19
  62.6 0.6 final.1
  (11 shorter events, 0.0 us)
Async XLA Ops:
  0.6 13.0 %copy-start.2 = (bf16[704,2048]{1,0:T(8,128)(2,1)S(1)}, bf16[704,2048]{1,0:T(8,128)(2,1)}, u32[]{:S(2)}) copy-start(bf16[704,2048]{1,0:T(8,128)(2,1)} %down_ref.2) | copy-start | bytes 8650756
  0.6 13.0 %copy-start.1 = (bf16[2048,704]{0,1:T(8,128)(2,1)S(1)}, bf16[2048,704]{0,1:T(8,128)(2,1)}, u32[]{:S(2)}) copy-start(bf16[2048,704]{0,1:T(8,128)(2,1)} %param.25) | copy-start | bytes 8650756
  0.7 13.0 %copy-start = (bf16[2048,704]{0,1:T(8,128)(2,1)S(1)}, bf16[2048,704]{0,1:T(8,128)(2,1)}, u32[]{:S(2)}) copy-start(bf16[2048,704]{0,1:T(8,128)(2,1)} %param.24) | copy-start | bytes 8650756
  0.7 13.0 %copy-start.15 = (f32[2048]{0:T(1024)S(1)}, f32[2048]{0:T(1024)}, u32[]{:S(2)}) copy-start(f32[2048]{0:T(1024)} %param.23) | copy-start | bytes 24580
  0.7 0.8 %copy-start.18 = (bf16[8,256]{1,0:T(8,128)(2,1)S(1)}, bf16[8,256]{1,0:T(8,128)(2,1)}, u32[]{:S(2)}) copy-start(bf16[8,256]{1,0:T(8,128)(2,1)} %tok_ref.1) | copy-start | bytes 12292
  13.7 10.4 %copy-start.6 = (bf16[256,2048]{1,0:T(8,128)(2,1)S(1)}, bf16[256,2048]{1,0:T(8,128)(2,1)}, u32[]{:S(2)}) copy-start(bf16[256,2048]{1,0:T(8,128)(2,1)} %win_ref.1) | copy-start | bytes 3145732
  13.7 10.4 %copy-start.7 = (bf16[256,2048]{1,0:T(8,128)(2,1)S(1)}, bf16[256,2048]{1,0:T(8,128)(2,1)}, u32[]{:S(2)}) copy-start(bf16[256,2048]{1,0:T(8,128)(2,1)} %wgate_ref.1) | copy-start | bytes 3145732
  13.7 10.4 %copy-start.10 = (bf16[256,512]{1,0:T(8,128)(2,1)S(1)}, bf16[256,512]{1,0:T(8,128)(2,1)}, u32[]{:S(2)}) copy-start(bf16[256,512]{1,0:T(8,128)(2,1)} %wwrite_ref.1) | copy-start | bytes 786436
  13.7 10.4 %copy-start.11 = (bf16[256,512]{1,0:T(8,128)(2,1)S(1)}, bf16[256,512]{1,0:T(8,128)(2,1)}, u32[]{:S(2)}) copy-start(bf16[256,512]{1,0:T(8,128)(2,1)} %wread_ref.1) | copy-start | bytes 786436
  13.7 10.4 %copy-start.14 = (bf16[256,32]{0,1:T(8,128)(2,1)S(1)}, bf16[256,32]{0,1:T(8,128)(2,1)}, u32[]{:S(2)}) copy-start(bf16[256,32]{0,1:T(8,128)(2,1)} %param.32) | copy-start | bytes 49156
  13.7 10.4 %copy-start.19 = (bf16[8,256]{1,0:T(8,128)(2,1)S(1)}, bf16[8,256]{1,0:T(8,128)(2,1)}, u32[]{:S(2)}) copy-start(bf16[8,256]{1,0:T(8,128)(2,1)} %tok_ref.1) | copy-start | bytes 12292
  13.8 10.4 %copy-start.20 = (f32[256]{0:T(256)S(1)}, f32[256]{0:T(256)}, u32[]{:S(2)}) copy-start(f32[256]{0:T(256)} %param.27) | copy-start | bytes 3076
  24.2 9.3 %copy-start.8 = (f32[1,32,64,128]{3,2,1,0:T(8,128)S(1)}, f32[1,32,64,128]{3,2,1,0:T(8,128)}, u32[]{:S(2)}) copy-start(f32[1,32,64,128]{3,2,1,0:T(8,128)} %param.37) | copy-start | bytes 3145732
  24.2 9.2 %copy-start.12 = (bf16[4,3072]{1,0:T(4,128)(2,1)S(1)}, bf16[4,3072]{1,0:T(4,128)(2,1)}, u32[]{:S(2)}) copy-start(bf16[4,3072]{1,0:T(4,128)(2,1)} %taps_ref.1) | copy-start | bytes 73732
  24.2 9.2 %copy-start.13 = (bf16[1,3,3072]{2,1,0:T(4,128)(2,1)S(1)}, bf16[1,3,3072]{2,1,0:T(4,128)(2,1)}, u32[]{:S(2)}) copy-start(bf16[1,3,3072]{2,1,0:T(4,128)(2,1)} %param.34) | copy-start | bytes 55300
  24.2 9.2 %copy-start.16 = (f32[2048]{0:T(1024)S(1)}, f32[2048]{0:T(1024)}, u32[]{:S(2)}) copy-start(f32[2048]{0:T(1024)} %param.38) | copy-start | bytes 24580
  24.2 9.2 %copy-start.21 = (f32[32]{0:T(128)S(1)}, f32[32]{0:T(128)}, u32[]{:S(2)}) copy-start(f32[32]{0:T(128)} %param.35) | copy-start | bytes 388
  24.2 9.2 %copy-start.22 = (f32[32]{0:T(128)S(1)}, f32[32]{0:T(128)}, u32[]{:S(2)}) copy-start(f32[32]{0:T(128)} %param.36) | copy-start | bytes 388
  33.4 10.0 %copy-start.9 = (bf16[2048,256]{1,0:T(8,128)(2,1)S(1)}, bf16[2048,256]{1,0:T(8,128)(2,1)}, u32[]{:S(2)}) copy-start(bf16[2048,256]{1,0:T(8,128)(2,1)} %w_ref.1) | copy-start | bytes 3145732
  43.5 8.8 %copy-start.3 = (bf16[2048,704]{0,1:T(8,128)(2,1)S(1)}, bf16[2048,704]{0,1:T(8,128)(2,1)}, u32[]{:S(2)}) copy-start(bf16[2048,704]{0,1:T(8,128)(2,1)} %param.41) | copy-start | bytes 8650756
  43.5 8.8 %copy-start.4 = (bf16[2048,704]{0,1:T(8,128)(2,1)S(1)}, bf16[2048,704]{0,1:T(8,128)(2,1)}, u32[]{:S(2)}) copy-start(bf16[2048,704]{0,1:T(8,128)(2,1)} %param.42) | copy-start | bytes 8650756
  43.5 8.8 %copy-start.5 = (bf16[704,2048]{1,0:T(8,128)(2,1)S(1)}, bf16[704,2048]{1,0:T(8,128)(2,1)}, u32[]{:S(2)}) copy-start(bf16[704,2048]{1,0:T(8,128)(2,1)} %down_ref.3) | copy-start | bytes 8650756
  43.5 8.8 %copy-start.17 = (f32[2048]{0:T(1024)S(1)}, f32[2048]{0:T(1024)}, u32[]{:S(2)}) copy-start(f32[2048]{0:T(1024)} %param.40) | copy-start | bytes 24580

commit v4 on v3

--- a/solution.py
+++ b/solution.py
@@ -15,8 +15,11 @@
 ROW_ROW = (((1,), (1,)), ((), ()))
 
 
-def exchange(blocks):
-    return lax.all_to_all(blocks, AXES, split_axis=0, concat_axis=0, tiled=True)
+def exchange(blocks, order=None):
+    groups = None if order is None else [list(order)]
+    return lax.all_to_all(
+        blocks, AXES, split_axis=0, concat_axis=0, tiled=True, axis_index_groups=groups
+    )
 
 
 def params(megabytes):
@@ -46,9 +49,16 @@
     )(block)
 
 
-def ff_kernel(x_ref, gain_ref, gate_ref, up_ref, down_ref, out_ref):
+def ff_kernel(place, extras, x_ref, gain_ref, gate_ref, up_ref, down_ref, *refs):
+    kept, out_ref, stored, sems = refs[:extras], refs[extras], refs[extras + 1 : -1], refs[-1]
+    copies = [
+        pltpu.make_async_copy(source, target, sems.at[i])
+        for i, (source, target) in enumerate(zip(kept, stored))
+    ]
+    for copy in copies:
+        copy.start()
     ways, rows, chan = x_ref.shape
-    pieces = [x_ref[k].astype(jnp.float32) for k in range(ways)]
+    pieces = [x_ref[place[k]].astype(jnp.float32) for k in range(ways)]
     total = jnp.zeros((rows, 1), jnp.float32)
     for piece in pieces:
         total += jnp.sum(piece * piece, axis=1, keepdims=True)
@@ -65,27 +75,31 @@
     hidden = (silu(gate) * upper).astype(jnp.bfloat16)
     down = jnp.dot(hidden, down_ref[...], preferred_element_type=jnp.float32)
     for k in range(ways):
-        out_ref[k] = down[:, k * chan : (k + 1) * chan]
-
-
-def ff(whole, gain, gate, up, down):
+        out_ref[place[k]] = down[:, k * chan : (k + 1) * chan].astype(jnp.bfloat16)
+    for copy in copies:
+        copy.wait()
+
+
+def ff(place, whole, gain, gate, up, down, *kept):
     return pl.pallas_call(
-        ff_kernel,
-        out_shape=jax.ShapeDtypeStruct(whole.shape, jnp.float32),
-        in_specs=[VMEM_SPEC] * 5,
-        out_specs=VMEM_SPEC,
+        functools.partial(ff_kernel, place, len(kept)),
+        out_shape=[jax.ShapeDtypeStruct(whole.shape, jnp.bfloat16)]
+        + [jax.ShapeDtypeStruct(k.shape, k.dtype) for k in kept],
+        in_specs=[VMEM_SPEC] * (5 + len(kept)),
+        out_specs=[VMEM_SPEC] + [pl.BlockSpec(memory_space=pltpu.HBM)] * len(kept),
+        scratch_shapes=[pltpu.SemaphoreType.DMA((max(1, len(kept)),))],
         compiler_params=params(8),
         cost_estimate=COST,
-    )(whole, gain, gate, up, down)
-
-
-def project_kernel(got_ref, tok_ref, gain_ref, win_ref, wwrite_ref, wread_ref, wgate_ref, wstep_ref,
+    )(whole, gain, gate, up, down, *kept)
+
+
+def project_kernel(place, got_ref, tok_ref, gain_ref, win_ref, wwrite_ref, wread_ref, wgate_ref, wstep_ref,
                    first_ref, out_ref, stage):
     ways, rows, chan = got_ref.shape
     slots = out_ref.shape[1]
-    share = got_ref[0]
+    share = got_ref[0].astype(jnp.float32)
     for k in range(1, ways):
-        share += got_ref[k]
+        share += got_ref[k].astype(jnp.float32)
     first = (tok_ref[...].astype(jnp.float32) + 0.5 * share).astype(jnp.bfloat16)
     first_ref[...] = first
     first_f = first.astype(jnp.float32)
@@ -110,13 +124,13 @@
     for j in range(row, slots):
         stage[pl.ds(j, rows, stride=slots), :] = jnp.zeros((rows, LANES), jnp.float32)
     for s in range(rows):
-        out_ref[s] = stage[pl.ds(s * slots, slots), :].astype(jnp.bfloat16)
-
-
-def project(got, tokens, gain, w_in, w_write, w_read, w_gate, w_step, slots):
+        out_ref[place[s]] = stage[pl.ds(s * slots, slots), :].astype(jnp.bfloat16)
+
+
+def project(place, got, tokens, gain, w_in, w_write, w_read, w_gate, w_step, slots):
     ways, rows, chan = got.shape
     return pl.pallas_call(
-        project_kernel,
+        functools.partial(project_kernel, place),
         out_shape=[
             jax.ShapeDtypeStruct((rows, chan), jnp.bfloat16),
             jax.ShapeDtypeStruct((rows, slots, LANES), jnp.bfloat16),
@@ -215,8 +229,8 @@
     return pl.pallas_call(
         functools.partial(mixer_kernel, width, groups),
         out_shape=[
-            jax.ShapeDtypeStruct(state.shape, jnp.float32),
-            jax.ShapeDtypeStruct(hist.shape, jnp.bfloat16),
+            pltpu.VMEM(state.shape, jnp.float32),
+            pltpu.VMEM(hist.shape, jnp.bfloat16),
             jax.ShapeDtypeStruct((ways, in_rows, LANES), jnp.bfloat16),
         ],
         in_specs=[VMEM_SPEC] * 7,
@@ -232,10 +246,10 @@
     )(got, taps, hist, bias, rate, state, ggain)
 
 
-def output_kernel(got_ref, w_ref, first_ref, out_ref, stage):
+def output_kernel(place, got_ref, w_ref, first_ref, out_ref, stage):
     ways, slots, _ = got_ref.shape
     for k in range(ways):
-        stage[pl.ds(k * slots, slots), :] = got_ref[k].astype(jnp.float32)
+        stage[pl.ds(k * slots, slots), :] = got_ref[place[k]].astype(jnp.float32)
     rows = jnp.concatenate(
         [stage[pl.ds(j, ways, stride=slots), :].astype(jnp.bfloat16) for j in range(slots)], axis=1
     )
@@ -245,10 +259,10 @@
         out_ref[k] = second
 
 
-def output(got, w, first):
+def output(place, got, w, first):
     ways, slots, _ = got.shape
     return pl.pallas_call(
-        output_kernel,
+        functools.partial(output_kernel, place),
         out_shape=jax.ShapeDtypeStruct((ways,) + first.shape, jnp.bfloat16),
         in_specs=[VMEM_SPEC] * 3,
         out_specs=VMEM_SPEC,
@@ -259,9 +273,9 @@
 
 
 def final_kernel(got_ref, second_ref, out_ref):
-    share = got_ref[0]
+    share = got_ref[0].astype(jnp.float32)
     for k in range(1, got_ref.shape[0]):
-        share += got_ref[k]
+        share += got_ref[k].astype(jnp.float32)
     out_ref[...] = (second_ref[0].astype(jnp.float32) + 0.5 * share).astype(jnp.bfloat16)
 
 
@@ -277,6 +291,7 @@
 
 def fast_body(
     ways,
+    leader,
     tokens,
     first_gain,
     first_gate,
@@ -307,20 +322,23 @@
     used = (conv_width + heads * head_dim) // LANES + 4
     slots = -(-used // 16) * 16
     scope = jax.named_scope
+    order = (leader,) + tuple(k for k in range(ways) if k != leader)
+    place = tuple(order.index(k) for k in range(ways))
 
     with scope("repeat"):
         blocks = repeat(tokens, ways)
-    whole = exchange(blocks)
+    whole = exchange(blocks, order)
     with scope("ff1"):
-        down1 = ff(whole, first_gain.reshape(1, width), first_gate.T, first_up.T, first_down)
-    got1 = exchange(down1)
+        (down1,) = ff(place, whole, first_gain.reshape(1, width), first_gate.T, first_up.T, first_down)
+    got1 = exchange(down1, order)
     with scope("project"):
         first, packed = project(
+            place,
             got1, tokens, mix_gain.reshape(1, -1), w_input, w_write, w_read, w_outgate, w_step.T, slots
         )
-    got2 = exchange(packed)
+    got2 = exchange(packed, order)
     with scope("mixer"):
-        state_out, history_out, normed = mixer(
+        new_state, new_hist, normed = mixer(
             width,
             groups,
             got2,
@@ -331,13 +349,22 @@
             mixer_state[0],
             group_gain.reshape(-1, LANES),
         )
-    got3 = exchange(normed)
+    got3 = exchange(normed, order)
     with scope("output"):
-        second_all = output(got3, w_output, first)
-    whole2 = exchange(second_all)
+        second_all = output(place, got3, w_output, first)
+    whole2 = exchange(second_all, order)
     with scope("ff2"):
-        down2 = ff(whole2, second_gain.reshape(1, width), second_gate.T, second_up.T, second_down)
-    got4 = exchange(down2)
+        down2, state_out, history_out = ff(
+            place,
+            whole2,
+            second_gain.reshape(1, width),
+            second_gate.T,
+            second_up.T,
+            second_down,
+            new_state,
+            new_hist,
+        )
+    got4 = exchange(down2, order)
     with scope("final"):
         layer_out = final(got4, second_all)
     return layer_out, state_out[None], history_out[None]
@@ -482,12 +509,14 @@
     rows = P(AXES, None)
     columns = P(None, AXES)
     own = ("dp",) + AXES
-    ways = mesh.shape["kv"] * mesh.shape["tp"]
+    kv, tp = mesh.shape["kv"], mesh.shape["tp"]
+    ways = kv * tp
+    leader = kv // 2 * tp + tp - 1
     plain = make_plain(ways)
 
     def body(*args):
         if friendly(ways, args):
-            return fast_body(ways, *args)
+            return fast_body(ways, leader, *args)
         return plain(*args)
 
     return jax.shard_map(

time: 63.6 us -> 55.7 us (0.88)
  blocking collectives: 54 us -> 46.6 us
    all_to_all x6, blocking collectives: 54 us -> 46.6 us  [exchange(): lax.all_to_all(blocks, AXES, split_axis=0, concat_axis=0, tiled=True, axi...]
where the time goes in v4:
time: 55.7 us; the launch traced here: 55.3 us
  blocking collectives  46.6 us (84%)
  Pallas kernels  6.88 us (12%)
  local copies, waits for them, and re-layouts  0.95 us (2%)
  between operations  0.92 us (2%)
    all_to_all x6, blocking collectives, exchange(): lax.all_to_all(blocks, AXES, split_axis=0, concat_axis=0, tiled=True, axi...  46.6 us
    pallas_call x2, Pallas kernels, ff(): pl.pallas_call(functools.partial(ff_kernel, place, len(kept)), out_shape=...  4.15 us
    pallas_call x1, Pallas kernels, mixer(): pl.pallas_call(functools.partial(mixer_kernel, width, groups), out_shape=...  1.4 us

profile of v4, /device:TPU:0, one launch (start us, length us, event | category | flops | bytes accessed | tf_op | source)
XLA Modules:
  0.0 55.3 jit_solution(1487790337809759852)
XLA Ops:
  0.6 0.0 copy-start.2
  0.6 0.0 copy-start.1
  0.7 0.0 copy-start
  0.7 0.0 copy-start.15
  0.7 0.0 copy-start.18
  0.7 0.8 %copy-done.18 = bf16[8,256]{1,0:T(8,128)(2,1)S(1)} copy-done((bf16[8,256]{1,0:T(8,128)(2,1)S(1)}, bf16[8,256]{1,0:T(8,128)(2,1)}, u32[]{:S(2)}) %copy-start.18) | copy-done | bytes 4120
  1.5 10.0 %all_to_all.30.x_ref = bf16[8,8,256]{2,1,0:T(8,128)(2,1)S(1)} all-to-all(bf16[8,8,256]{2,1,0:T(8,128)(2,1)S(1)} %repeat.1), channel_id=1, replica_groups={{5,0,1,2,3,4,6,7},{13,8,9,10,11,12,14,15},{21,16,17,18,19,20,22,23},{29..., dimensions={0} | all-to-all | bytes 65536 | tf_op jit(solution)/shard_map/all_to_all | solution.py:20
  11.5 0.0 copy-done.2
  11.5 0.0 copy-done.1
  11.5 0.0 copy-done
  11.5 0.0 copy-done.15
  11.5 0.0 copy-start.6
  11.5 0.0 copy-start.7
  11.5 0.0 copy-start.10
  11.6 0.0 copy-start.11
  11.6 0.0 copy-start.14
  11.6 0.0 copy-start.19
  11.6 0.0 copy-start.20
  11.6 2.1 %ff1.1 = bf16[8,8,256]{2,1,0:T(8,128)(2,1)S(1)} custom-call(bf16[8,8,256]{2,1,0:T(8,128)(2,1)S(1)} %all_to_all.30.x_ref, f32[1,2048]{1,0:T(1,128)S(1)} %bitcast.22, bf16[704,2048]{1,0:T(8,128)(2,1)S(1)} %bitcast.15, bf16[704,2048]{1,0:T(8,128)(2,1)S(1)} %bitcast.16, bf16[704,2048]{1,0:T(8,128)(2,1)S(1)} %copy-done.2), custom_call_target="tpu_custom_call" | custom-call | flops 10000000000 | bytes 1000 | tf_op jit(solution)/shard_map/ff1/pallas_call | solution.py:84
  13.7 7.1 %all_to_all.31.got_ref = bf16[8,8,256]{2,1,0:T(8,128)(2,1)S(1)} all-to-all(bf16[8,8,256]{2,1,0:T(8,128)(2,1)S(1)} %ff1.1), channel_id=1, replica_groups={{5,0,1,2,3,4,6,7},{13,8,9,10,11,12,14,15},{21,16,17,18,19,20,22,23},{29..., dimensions={0} | all-to-all | bytes 65536 | tf_op jit(solution)/shard_map/all_to_all | solution.py:20
  20.8 0.0 copy-done.6
  20.8 0.0 copy-done.7
  20.8 0.0 copy-done.10
  20.8 0.0 copy-done.11
  20.8 0.0 copy-done.14
  20.8 0.0 copy-done.19
  20.9 0.0 copy-done.20
  20.9 0.0 copy-start.8
  20.9 0.0 copy-start.12
  20.9 0.0 copy-start.13
  20.9 0.0 copy-start.16
  20.9 0.0 copy-start.21
  20.9 0.0 copy-start.22
  20.9 0.5 project.1
  21.4 7.5 %all_to_all.32.got_ref = bf16[8,48,128]{2,1,0:T(8,128)(2,1)S(1)} all-to-all(bf16[8,48,128]{2,1,0:T(8,128)(2,1)S(1)} %get-tuple-element.11), channel_id=1, replica_groups={{5,0,1,2,3,4,6,7},{13,8,9,10,11,12,14,15},{21,16,17,18,19,20,22,23},{29..., dimensions={0} | all-to-all | bytes 196608 | tf_op jit(solution)/shard_map/all_to_all | solution.py:20
  29.0 0.0 copy-done.16
  29.0 0.0 copy-done.21
  29.0 0.0 copy-done.22
  29.0 0.0 copy-start.9
  29.0 1.4 %mixer.1 = (f32[32,64,128]{2,1,0:T(8,128)S(1)}, bf16[3,3072]{1,0:T(4,128)(2,1)S(1)}, bf16[8,16,128]{2,1,0:T(8,128)(2,1)S(1)}) custom-call(bf16[8,48,128]{2,1,0:T(8,128)(2,1)S(1)} %all_to_all.32.got_ref, bf16[4,3072]{1,0:T(4,128)(2,1)S(1)} %copy-done.12, bf16[3,3072]{1,0:T(4,128)(2,1)S(1)} %bitcast.20, f32[1,32]{1,0:T(1,128)S(1)} %bitcast.26, ...), custom_call_target="tpu_custom_call" | custom-call | flops 10000000000 | bytes 1000 | tf_op jit(solution)/shard_map/mixer/pallas_call | solution.py:229
  30.4 7.4 %all_to_all.33.got_ref = bf16[8,16,128]{2,1,0:T(8,128)(2,1)S(1)} all-to-all(bf16[8,16,128]{2,1,0:T(8,128)(2,1)S(1)} %get-tuple-element.12), channel_id=1, replica_groups={{5,0,1,2,3,4,6,7},{13,8,9,10,11,12,14,15},{21,16,17,18,19,20,22,23},{29..., dimensions={0} | all-to-all | bytes 65536 | tf_op jit(solution)/shard_map/all_to_all | solution.py:20
  37.8 0.0 copy-start.17
  37.8 0.2 output.1.second_ref
  38.1 7.4 %all_to_all.34.x_ref = bf16[8,8,256]{2,1,0:T(8,128)(2,1)S(1)} all-to-all(bf16[8,8,256]{2,1,0:T(8,128)(2,1)S(1)} %output.1.second_ref), channel_id=1, replica_groups={{5,0,1,2,3,4,6,7},{13,8,9,10,11,12,14,15},{21,16,17,18,19,20,22,23},{29..., dimensions={0} | all-to-all | bytes 65536 | tf_op jit(solution)/shard_map/all_to_all | solution.py:20
  45.5 0.0 copy-done.17
  45.5 2.1 %ff2.1 = (bf16[8,8,256]{2,1,0:T(8,128)(2,1)S(1)}, f32[32,64,128]{2,1,0:T(8,128)}, bf16[3,3072]{1,0:T(4,128)(2,1)}) custom-call(bf16[8,8,256]{2,1,0:T(8,128)(2,1)S(1)} %all_to_all.34.x_ref, f32[1,2048]{1,0:T(1,128)S(1)} %bitcast.24, bf16[704,2048]{1,0:T(8,128)(2,1)S(1)} %bitcast.17, bf16[704,2048]{1,0:T(8,128)(2,1)S(1)} %bitcast.18, ...), custom_call_target="tpu_custom_call" | custom-call | flops 10000000000 | bytes 1000 | tf_op jit(solution)/shard_map/ff2/pallas_call | solution.py:84
  47.6 7.1 %all_to_all.35.got_ref = bf16[8,8,256]{2,1,0:T(8,128)(2,1)S(1)} all-to-all(bf16[8,8,256]{2,1,0:T(8,128)(2,1)S(1)} %get-tuple-element.16), channel_id=1, replica_groups={{5,0,1,2,3,4,6,7},{13,8,9,10,11,12,14,15},{21,16,17,18,19,20,22,23},{29..., dimensions={0} | all-to-all | bytes 65536 | tf_op jit(solution)/shard_map/all_to_all | solution.py:20
  54.7 0.6 %final.1 = bf16[8,256]{1,0:T(8,128)(2,1)} custom-call(bf16[8,8,256]{2,1,0:T(8,128)(2,1)S(1)} %all_to_all.35.got_ref, bf16[8,8,256]{2,1,0:T(8,128)(2,1)S(1)} %output.1.second_ref), custom_call_target="tpu_custom_call" | custom-call | tf_op jit(solution)/shard_map/final/pallas_call | solution.py:283
  (11 shorter events, 0.0 us)
Async XLA Ops:
  0.6 10.9 %copy-start.2 = (bf16[704,2048]{1,0:T(8,128)(2,1)S(1)}, bf16[704,2048]{1,0:T(8,128)(2,1)}, u32[]{:S(2)}) copy-start(bf16[704,2048]{1,0:T(8,128)(2,1)} %down_ref.2) | copy-start | bytes 8650756
  0.6 10.9 %copy-start.1 = (bf16[2048,704]{0,1:T(8,128)(2,1)S(1)}, bf16[2048,704]{0,1:T(8,128)(2,1)}, u32[]{:S(2)}) copy-start(bf16[2048,704]{0,1:T(8,128)(2,1)} %param.25) | copy-start | bytes 8650756
  0.7 10.8 %copy-start = (bf16[2048,704]{0,1:T(8,128)(2,1)S(1)}, bf16[2048,704]{0,1:T(8,128)(2,1)}, u32[]{:S(2)}) copy-start(bf16[2048,704]{0,1:T(8,128)(2,1)} %param.24) | copy-start | bytes 8650756
  0.7 10.8 %copy-start.15 = (f32[2048]{0:T(1024)S(1)}, f32[2048]{0:T(1024)}, u32[]{:S(2)}) copy-start(f32[2048]{0:T(1024)} %param.23) | copy-start | bytes 24580
  0.7 0.8 %copy-start.18 = (bf16[8,256]{1,0:T(8,128)(2,1)S(1)}, bf16[8,256]{1,0:T(8,128)(2,1)}, u32[]{:S(2)}) copy-start(bf16[8,256]{1,0:T(8,128)(2,1)} %tok_ref.1) | copy-start | bytes 12292
  11.5 9.3 %copy-start.6 = (bf16[256,2048]{1,0:T(8,128)(2,1)S(1)}, bf16[256,2048]{1,0:T(8,128)(2,1)}, u32[]{:S(2)}) copy-start(bf16[256,2048]{1,0:T(8,128)(2,1)} %win_ref.1) | copy-start | bytes 3145732
  11.5 9.3 %copy-start.7 = (bf16[256,2048]{1,0:T(8,128)(2,1)S(1)}, bf16[256,2048]{1,0:T(8,128)(2,1)}, u32[]{:S(2)}) copy-start(bf16[256,2048]{1,0:T(8,128)(2,1)} %wgate_ref.1) | copy-start | bytes 3145732
  11.5 9.3 %copy-start.10 = (bf16[256,512]{1,0:T(8,128)(2,1)S(1)}, bf16[256,512]{1,0:T(8,128)(2,1)}, u32[]{:S(2)}) copy-start(bf16[256,512]{1,0:T(8,128)(2,1)} %wwrite_ref.1) | copy-start | bytes 786436
  11.6 9.3 %copy-start.11 = (bf16[256,512]{1,0:T(8,128)(2,1)S(1)}, bf16[256,512]{1,0:T(8,128)(2,1)}, u32[]{:S(2)}) copy-start(bf16[256,512]{1,0:T(8,128)(2,1)} %wread_ref.1) | copy-start | bytes 786436
  11.6 9.3 %copy-start.14 = (bf16[256,32]{0,1:T(8,128)(2,1)S(1)}, bf16[256,32]{0,1:T(8,128)(2,1)}, u32[]{:S(2)}) copy-start(bf16[256,32]{0,1:T(8,128)(2,1)} %param.32) | copy-start | bytes 49156
  11.6 9.3 %copy-start.19 = (bf16[8,256]{1,0:T(8,128)(2,1)S(1)}, bf16[8,256]{1,0:T(8,128)(2,1)}, u32[]{:S(2)}) copy-start(bf16[8,256]{1,0:T(8,128)(2,1)} %tok_ref.1) | copy-start | bytes 12292
  11.6 9.3 %copy-start.20 = (f32[256]{0:T(256)S(1)}, f32[256]{0:T(256)}, u32[]{:S(2)}) copy-start(f32[256]{0:T(256)} %param.27) | copy-start | bytes 3076
  20.9 8.1 %copy-start.8 = (f32[1,32,64,128]{3,2,1,0:T(8,128)S(1)}, f32[1,32,64,128]{3,2,1,0:T(8,128)}, u32[]{:S(2)}) copy-start(f32[1,32,64,128]{3,2,1,0:T(8,128)} %param.37) | copy-start | bytes 3145732
  20.9 8.1 %copy-start.12 = (bf16[4,3072]{1,0:T(4,128)(2,1)S(1)}, bf16[4,3072]{1,0:T(4,128)(2,1)}, u32[]{:S(2)}) copy-start(bf16[4,3072]{1,0:T(4,128)(2,1)} %taps_ref.1) | copy-start | bytes 73732
  20.9 8.1 %copy-start.13 = (bf16[1,3,3072]{2,1,0:T(4,128)(2,1)S(1)}, bf16[1,3,3072]{2,1,0:T(4,128)(2,1)}, u32[]{:S(2)}) copy-start(bf16[1,3,3072]{2,1,0:T(4,128)(2,1)} %param.34) | copy-start | bytes 55300
  20.9 8.1 %copy-start.16 = (f32[2048]{0:T(1024)S(1)}, f32[2048]{0:T(1024)}, u32[]{:S(2)}) copy-start(f32[2048]{0:T(1024)} %param.38) | copy-start | bytes 24580
  20.9 8.1 %copy-start.21 = (f32[32]{0:T(128)S(1)}, f32[32]{0:T(128)}, u32[]{:S(2)}) copy-start(f32[32]{0:T(128)} %param.35) | copy-start | bytes 388
  20.9 8.1 %copy-start.22 = (f32[32]{0:T(128)S(1)}, f32[32]{0:T(128)}, u32[]{:S(2)}) copy-start(f32[32]{0:T(128)} %param.36) | copy-start | bytes 388
  29.0 8.8 %copy-start.9 = (bf16[2048,256]{1,0:T(8,128)(2,1)S(1)}, bf16[2048,256]{1,0:T(8,128)(2,1)}, u32[]{:S(2)}) copy-start(bf16[2048,256]{1,0:T(8,128)(2,1)} %w_ref.1) | copy-start | bytes 3145732
  37.8 7.7 %copy-start.3 = (bf16[2048,704]{0,1:T(8,128)(2,1)S(1)}, bf16[2048,704]{0,1:T(8,128)(2,1)}, u32[]{:S(2)}) copy-start(bf16[2048,704]{0,1:T(8,128)(2,1)} %param.41) | copy-start | bytes 8650756
  37.8 7.7 %copy-start.4 = (bf16[2048,704]{0,1:T(8,128)(2,1)S(1)}, bf16[2048,704]{0,1:T(8,128)(2,1)}, u32[]{:S(2)}) copy-start(bf16[2048,704]{0,1:T(8,128)(2,1)} %param.42) | copy-start | bytes 8650756
  37.8 7.7 %copy-start.5 = (bf16[704,2048]{1,0:T(8,128)(2,1)S(1)}, bf16[704,2048]{1,0:T(8,128)(2,1)}, u32[]{:S(2)}) copy-start(bf16[704,2048]{1,0:T(8,128)(2,1)} %down_ref.3) | copy-start | bytes 8650756
  37.8 7.7 %copy-start.17 = (f32[2048]{0:T(1024)S(1)}, f32[2048]{0:T(1024)}, u32[]{:S(2)}) copy-start(f32[2048]{0:T(1024)} %param.40) | copy-start | bytes 24580

commit v5 on v4

--- a/solution.py
+++ b/solution.py
@@ -181,6 +181,9 @@
     raw = rounded[step_row : step_row + 1, :heads] + bias_ref[...]
     step = jnp.maximum(raw, 0.0) + jnp.log1p(jnp.exp(-jnp.abs(raw)))
     decay = jnp.exp(-step * jnp.exp(rate_ref[...]))
+    maps_high = maps.astype(jnp.bfloat16)
+    maps_low = (maps - maps_high.astype(jnp.float32)).astype(jnp.bfloat16)
+    maps2 = jnp.concatenate([maps_high, maps_low], axis=0)
     pad = jnp.zeros((LANES - in_rows, LANES), jnp.float32)
     columns = jnp.concatenate([conv[:in_rows], pad], axis=0).T
     per_row = LANES // head_dim
@@ -194,13 +197,12 @@
         block = state_out_ref[g * per_group : (g + 1) * per_group].reshape(
             per_group * head_dim, state_dim
         )
-        read = lax.dot_general(
-            maps,
-            block,
-            ROW_ROW,
-            precision=lax.Precision.HIGHEST,
-            preferred_element_type=jnp.float32,
-        )
+        high = block.astype(jnp.bfloat16)
+        read = lax.dot_general(maps2, high, ROW_ROW, preferred_element_type=jnp.float32)
+        low = (block - high.astype(jnp.float32)).astype(jnp.bfloat16)
+        read += lax.dot_general(maps2, low, ROW_ROW, preferred_element_type=jnp.float32)
+        count = 2 * map_rows
+        read = read[:count] + read[count:]
         span = per_group * head_dim // LANES
         for j in range(span):
             read_rows[g * span + j : g * span + j + 1, :] = read[
@@ -322,7 +324,10 @@
     used = (conv_width + heads * head_dim) // LANES + 4
     slots = -(-used // 16) * 16
     scope = jax.named_scope
-    order = (leader,) + tuple(k for k in range(ways) if k != leader)
+    rest = [k for k in range(ways) if k != leader]
+    rest[3], rest[4] = rest[4], rest[3]
+    rest[-2], rest[-1] = rest[-1], rest[-2]
+    order = (leader, *rest)
     place = tuple(order.index(k) for k in range(ways))
 
     with scope("repeat"):

time: 55.7 us -> 54.8 us (0.984)
  blocking collectives: 46.6 us -> 46 us
where the time goes in v5:
time: 54.8 us; the launch traced here: 54.5 us
  blocking collectives  46 us (84%)
  Pallas kernels  6.57 us (12%)
  local copies, waits for them, and re-layouts  0.95 us (2%)
  between operations  0.92 us (2%)
    all_to_all x6, blocking collectives, exchange(): lax.all_to_all(blocks, AXES, split_axis=0, concat_axis=0, tiled=True, axi...  46 us
    pallas_call x2, Pallas kernels, ff(): pl.pallas_call(functools.partial(ff_kernel, place, len(kept)), out_shape=...  4.15 us

profile of v5, /device:TPU:0, one launch (start us, length us, event | category | flops | bytes accessed | tf_op | source)
XLA Modules:
  0.0 54.5 jit_solution(13837224423783384626)
XLA Ops:
  0.6 0.0 copy-start.2
  0.6 0.0 copy-start.1
  0.7 0.0 copy-start
  0.7 0.0 copy-start.15
  0.7 0.0 copy-start.18
  0.7 0.8 %copy-done.18 = bf16[8,256]{1,0:T(8,128)(2,1)S(1)} copy-done((bf16[8,256]{1,0:T(8,128)(2,1)S(1)}, bf16[8,256]{1,0:T(8,128)(2,1)}, u32[]{:S(2)}) %copy-start.18) | copy-done | bytes 4120
  1.5 10.0 %all_to_all.30.x_ref = bf16[8,8,256]{2,1,0:T(8,128)(2,1)S(1)} all-to-all(bf16[8,8,256]{2,1,0:T(8,128)(2,1)S(1)} %repeat.1), channel_id=1, replica_groups={{5,0,1,2,4,3,7,6},{13,8,9,10,12,11,15,14},{21,16,17,18,20,19,23,22},{29..., dimensions={0} | all-to-all | bytes 65536 | tf_op jit(solution)/shard_map/all_to_all | solution.py:20
  11.5 0.0 copy-done.2
  11.5 0.0 copy-done.1
  11.5 0.0 copy-done
  11.5 0.0 copy-done.15
  11.6 0.0 copy-start.6
  11.6 0.0 copy-start.7
  11.6 0.0 copy-start.10
  11.6 0.0 copy-start.11
  11.6 0.0 copy-start.14
  11.6 0.0 copy-start.19
  11.6 0.0 copy-start.20
  11.6 2.1 %ff1.1 = bf16[8,8,256]{2,1,0:T(8,128)(2,1)S(1)} custom-call(bf16[8,8,256]{2,1,0:T(8,128)(2,1)S(1)} %all_to_all.30.x_ref, f32[1,2048]{1,0:T(1,128)S(1)} %bitcast.22, bf16[704,2048]{1,0:T(8,128)(2,1)S(1)} %bitcast.15, bf16[704,2048]{1,0:T(8,128)(2,1)S(1)} %bitcast.16, bf16[704,2048]{1,0:T(8,128)(2,1)S(1)} %copy-done.2), custom_call_target="tpu_custom_call" | custom-call | flops 10000000000 | bytes 1000 | tf_op jit(solution)/shard_map/ff1/pallas_call | solution.py:84
  13.7 7.1 %all_to_all.31.got_ref = bf16[8,8,256]{2,1,0:T(8,128)(2,1)S(1)} all-to-all(bf16[8,8,256]{2,1,0:T(8,128)(2,1)S(1)} %ff1.1), channel_id=1, replica_groups={{5,0,1,2,4,3,7,6},{13,8,9,10,12,11,15,14},{21,16,17,18,20,19,23,22},{29..., dimensions={0} | all-to-all | bytes 65536 | tf_op jit(solution)/shard_map/all_to_all | solution.py:20
  20.8 0.0 copy-done.6
  20.8 0.0 copy-done.7
  20.8 0.0 copy-done.10
  20.8 0.0 copy-done.11
  20.8 0.0 copy-done.14
  20.8 0.0 copy-done.19
  20.8 0.0 copy-done.20
  20.8 0.0 copy-start.8
  20.8 0.0 copy-start.12
  20.8 0.0 copy-start.13
  20.9 0.0 copy-start.16
  20.9 0.0 copy-start.21
  20.9 0.0 copy-start.22
  20.9 0.5 project.1
  21.4 7.5 %all_to_all.32.got_ref = bf16[8,48,128]{2,1,0:T(8,128)(2,1)S(1)} all-to-all(bf16[8,48,128]{2,1,0:T(8,128)(2,1)S(1)} %get-tuple-element.11), channel_id=1, replica_groups={{5,0,1,2,4,3,7,6},{13,8,9,10,12,11,15,14},{21,16,17,18,20,19,23,22},{29..., dimensions={0} | all-to-all | bytes 196608 | tf_op jit(solution)/shard_map/all_to_all | solution.py:20
  28.9 0.0 copy-done.8
  28.9 0.0 copy-done.12
  28.9 0.0 copy-done.13
  28.9 0.0 copy-start.9
  29.0 1.1 %mixer.1 = (f32[32,64,128]{2,1,0:T(8,128)S(1)}, bf16[3,3072]{1,0:T(4,128)(2,1)S(1)}, bf16[8,16,128]{2,1,0:T(8,128)(2,1)S(1)}) custom-call(bf16[8,48,128]{2,1,0:T(8,128)(2,1)S(1)} %all_to_all.32.got_ref, bf16[4,3072]{1,0:T(4,128)(2,1)S(1)} %copy-done.12, bf16[3,3072]{1,0:T(4,128)(2,1)S(1)} %bitcast.20, f32[1,32]{1,0:T(1,128)S(1)} %bitcast.26, ...), custom_call_target="tpu_custom_call" | custom-call | flops 10000000000 | bytes 1000 | tf_op jit(solution)/shard_map/mixer/pallas_call | solution.py:231
  30.1 7.1 %all_to_all.33.got_ref = bf16[8,16,128]{2,1,0:T(8,128)(2,1)S(1)} all-to-all(bf16[8,16,128]{2,1,0:T(8,128)(2,1)S(1)} %get-tuple-element.12), channel_id=1, replica_groups={{5,0,1,2,4,3,7,6},{13,8,9,10,12,11,15,14},{21,16,17,18,20,19,23,22},{29..., dimensions={0} | all-to-all | bytes 65536 | tf_op jit(solution)/shard_map/all_to_all | solution.py:20
  37.1 0.0 copy-start.17
  37.1 0.2 output.1.second_ref
  37.4 7.3 %all_to_all.34.x_ref = bf16[8,8,256]{2,1,0:T(8,128)(2,1)S(1)} all-to-all(bf16[8,8,256]{2,1,0:T(8,128)(2,1)S(1)} %output.1.second_ref), channel_id=1, replica_groups={{5,0,1,2,4,3,7,6},{13,8,9,10,12,11,15,14},{21,16,17,18,20,19,23,22},{29..., dimensions={0} | all-to-all | bytes 65536 | tf_op jit(solution)/shard_map/all_to_all | solution.py:20
  44.7 0.0 copy-done.17
  44.7 2.1 %ff2.1 = (bf16[8,8,256]{2,1,0:T(8,128)(2,1)S(1)}, f32[32,64,128]{2,1,0:T(8,128)}, bf16[3,3072]{1,0:T(4,128)(2,1)}) custom-call(bf16[8,8,256]{2,1,0:T(8,128)(2,1)S(1)} %all_to_all.34.x_ref, f32[1,2048]{1,0:T(1,128)S(1)} %bitcast.24, bf16[704,2048]{1,0:T(8,128)(2,1)S(1)} %bitcast.17, bf16[704,2048]{1,0:T(8,128)(2,1)S(1)} %bitcast.18, ...), custom_call_target="tpu_custom_call" | custom-call | flops 10000000000 | bytes 1000 | tf_op jit(solution)/shard_map/ff2/pallas_call | solution.py:84
  46.8 7.1 %all_to_all.35.got_ref = bf16[8,8,256]{2,1,0:T(8,128)(2,1)S(1)} all-to-all(bf16[8,8,256]{2,1,0:T(8,128)(2,1)S(1)} %get-tuple-element.16), channel_id=1, replica_groups={{5,0,1,2,4,3,7,6},{13,8,9,10,12,11,15,14},{21,16,17,18,20,19,23,22},{29..., dimensions={0} | all-to-all | bytes 65536 | tf_op jit(solution)/shard_map/all_to_all | solution.py:20
  53.9 0.6 %final.1 = bf16[8,256]{1,0:T(8,128)(2,1)} custom-call(bf16[8,8,256]{2,1,0:T(8,128)(2,1)S(1)} %all_to_all.35.got_ref, bf16[8,8,256]{2,1,0:T(8,128)(2,1)S(1)} %output.1.second_ref), custom_call_target="tpu_custom_call" | custom-call | tf_op jit(solution)/shard_map/final/pallas_call | solution.py:285
  (11 shorter events, 0.0 us)
Async XLA Ops:
  0.6 10.9 %copy-start.2 = (bf16[704,2048]{1,0:T(8,128)(2,1)S(1)}, bf16[704,2048]{1,0:T(8,128)(2,1)}, u32[]{:S(2)}) copy-start(bf16[704,2048]{1,0:T(8,128)(2,1)} %down_ref.2) | copy-start | bytes 8650756
  0.6 10.9 %copy-start.1 = (bf16[2048,704]{0,1:T(8,128)(2,1)S(1)}, bf16[2048,704]{0,1:T(8,128)(2,1)}, u32[]{:S(2)}) copy-start(bf16[2048,704]{0,1:T(8,128)(2,1)} %param.25) | copy-start | bytes 8650756
  0.7 10.9 %copy-start = (bf16[2048,704]{0,1:T(8,128)(2,1)S(1)}, bf16[2048,704]{0,1:T(8,128)(2,1)}, u32[]{:S(2)}) copy-start(bf16[2048,704]{0,1:T(8,128)(2,1)} %param.24) | copy-start | bytes 8650756
  0.7 10.9 %copy-start.15 = (f32[2048]{0:T(1024)S(1)}, f32[2048]{0:T(1024)}, u32[]{:S(2)}) copy-start(f32[2048]{0:T(1024)} %param.23) | copy-start | bytes 24580
  0.7 0.8 %copy-start.18 = (bf16[8,256]{1,0:T(8,128)(2,1)S(1)}, bf16[8,256]{1,0:T(8,128)(2,1)}, u32[]{:S(2)}) copy-start(bf16[8,256]{1,0:T(8,128)(2,1)} %tok_ref.1) | copy-start | bytes 12292
  11.6 9.2 %copy-start.6 = (bf16[256,2048]{1,0:T(8,128)(2,1)S(1)}, bf16[256,2048]{1,0:T(8,128)(2,1)}, u32[]{:S(2)}) copy-start(bf16[256,2048]{1,0:T(8,128)(2,1)} %win_ref.1) | copy-start | bytes 3145732
  11.6 9.2 %copy-start.7 = (bf16[256,2048]{1,0:T(8,128)(2,1)S(1)}, bf16[256,2048]{1,0:T(8,128)(2,1)}, u32[]{:S(2)}) copy-start(bf16[256,2048]{1,0:T(8,128)(2,1)} %wgate_ref.1) | copy-start | bytes 3145732
  11.6 9.2 %copy-start.10 = (bf16[256,512]{1,0:T(8,128)(2,1)S(1)}, bf16[256,512]{1,0:T(8,128)(2,1)}, u32[]{:S(2)}) copy-start(bf16[256,512]{1,0:T(8,128)(2,1)} %wwrite_ref.1) | copy-start | bytes 786436
  11.6 9.2 %copy-start.11 = (bf16[256,512]{1,0:T(8,128)(2,1)S(1)}, bf16[256,512]{1,0:T(8,128)(2,1)}, u32[]{:S(2)}) copy-start(bf16[256,512]{1,0:T(8,128)(2,1)} %wread_ref.1) | copy-start | bytes 786436
  11.6 9.2 %copy-start.14 = (bf16[256,32]{0,1:T(8,128)(2,1)S(1)}, bf16[256,32]{0,1:T(8,128)(2,1)}, u32[]{:S(2)}) copy-start(bf16[256,32]{0,1:T(8,128)(2,1)} %param.32) | copy-start | bytes 49156
  11.6 9.2 %copy-start.19 = (bf16[8,256]{1,0:T(8,128)(2,1)S(1)}, bf16[8,256]{1,0:T(8,128)(2,1)}, u32[]{:S(2)}) copy-start(bf16[8,256]{1,0:T(8,128)(2,1)} %tok_ref.1) | copy-start | bytes 12292
  11.6 9.2 %copy-start.20 = (f32[256]{0:T(256)S(1)}, f32[256]{0:T(256)}, u32[]{:S(2)}) copy-start(f32[256]{0:T(256)} %param.27) | copy-start | bytes 3076
  20.8 8.1 %copy-start.8 = (f32[1,32,64,128]{3,2,1,0:T(8,128)S(1)}, f32[1,32,64,128]{3,2,1,0:T(8,128)}, u32[]{:S(2)}) copy-start(f32[1,32,64,128]{3,2,1,0:T(8,128)} %param.37) | copy-start | bytes 3145732
  20.8 8.1 %copy-start.12 = (bf16[4,3072]{1,0:T(4,128)(2,1)S(1)}, bf16[4,3072]{1,0:T(4,128)(2,1)}, u32[]{:S(2)}) copy-start(bf16[4,3072]{1,0:T(4,128)(2,1)} %taps_ref.1) | copy-start | bytes 73732
  20.8 8.1 %copy-start.13 = (bf16[1,3,3072]{2,1,0:T(4,128)(2,1)S(1)}, bf16[1,3,3072]{2,1,0:T(4,128)(2,1)}, u32[]{:S(2)}) copy-start(bf16[1,3,3072]{2,1,0:T(4,128)(2,1)} %param.34) | copy-start | bytes 55300
  20.9 8.1 %copy-start.16 = (f32[2048]{0:T(1024)S(1)}, f32[2048]{0:T(1024)}, u32[]{:S(2)}) copy-start(f32[2048]{0:T(1024)} %param.38) | copy-start | bytes 24580
  20.9 8.1 %copy-start.21 = (f32[32]{0:T(128)S(1)}, f32[32]{0:T(128)}, u32[]{:S(2)}) copy-start(f32[32]{0:T(128)} %param.35) | copy-start | bytes 388
  20.9 8.1 %copy-start.22 = (f32[32]{0:T(128)S(1)}, f32[32]{0:T(128)}, u32[]{:S(2)}) copy-start(f32[32]{0:T(128)} %param.36) | copy-start | bytes 388
  28.9 8.2 %copy-start.9 = (bf16[2048,256]{1,0:T(8,128)(2,1)S(1)}, bf16[2048,256]{1,0:T(8,128)(2,1)}, u32[]{:S(2)}) copy-start(bf16[2048,256]{1,0:T(8,128)(2,1)} %w_ref.1) | copy-start | bytes 3145732
  37.1 7.6 %copy-start.3 = (bf16[2048,704]{0,1:T(8,128)(2,1)S(1)}, bf16[2048,704]{0,1:T(8,128)(2,1)}, u32[]{:S(2)}) copy-start(bf16[2048,704]{0,1:T(8,128)(2,1)} %param.41) | copy-start | bytes 8650756
  37.1 7.6 %copy-start.4 = (bf16[2048,704]{0,1:T(8,128)(2,1)S(1)}, bf16[2048,704]{0,1:T(8,128)(2,1)}, u32[]{:S(2)}) copy-start(bf16[2048,704]{0,1:T(8,128)(2,1)} %param.42) | copy-start | bytes 8650756
  37.1 7.6 %copy-start.5 = (bf16[704,2048]{1,0:T(8,128)(2,1)S(1)}, bf16[704,2048]{1,0:T(8,128)(2,1)}, u32[]{:S(2)}) copy-start(bf16[704,2048]{1,0:T(8,128)(2,1)} %down_ref.3) | copy-start | bytes 8650756
  37.1 7.6 %copy-start.17 = (f32[2048]{0:T(1024)S(1)}, f32[2048]{0:T(1024)}, u32[]{:S(2)}) copy-start(f32[2048]{0:T(1024)} %param.40) | copy-start | bytes 24580

commit v6 on v5

--- a/solution.py
+++ b/solution.py
@@ -36,6 +36,20 @@
 def repeat_kernel(block_ref, out_ref):
     for k in range(out_ref.shape[0]):
         out_ref[k] = block_ref[...]
+
+
+def fetch_kernel(block_ref, out_ref):
+    out_ref[...] = block_ref[...]
+
+
+def fetch(block):
+    return pl.pallas_call(
+        fetch_kernel,
+        out_shape=jax.ShapeDtypeStruct(block.shape, block.dtype),
+        in_specs=[VMEM_SPEC],
+        out_specs=VMEM_SPEC,
+        compiler_params=params(2),
+    )(block)
 
 
 def repeat(block, ways):
@@ -65,14 +79,14 @@
     scale = lax.rsqrt(total / (ways * chan) + EPS)
     normed = jnp.concatenate(
         [
-            (piece * scale * gain_ref[:, k * chan : (k + 1) * chan]).astype(jnp.bfloat16)
+            (piece * gain_ref[:, k * chan : (k + 1) * chan]).astype(jnp.bfloat16)
             for k, piece in enumerate(pieces)
         ],
         axis=1,
     )
     gate = lax.dot_general(normed, gate_ref[...], ROW_ROW, preferred_element_type=jnp.float32)
     upper = lax.dot_general(normed, up_ref[...], ROW_ROW, preferred_element_type=jnp.float32)
-    hidden = (silu(gate) * upper).astype(jnp.bfloat16)
+    hidden = (silu(scale * gate) * (scale * upper)).astype(jnp.bfloat16)
     down = jnp.dot(hidden, down_ref[...], preferred_element_type=jnp.float32)
     for k in range(ways):
         out_ref[place[k]] = down[:, k * chan : (k + 1) * chan].astype(jnp.bfloat16)
@@ -100,7 +114,7 @@
     share = got_ref[0].astype(jnp.float32)
     for k in range(1, ways):
         share += got_ref[k].astype(jnp.float32)
-    first = (tok_ref[...].astype(jnp.float32) + 0.5 * share).astype(jnp.bfloat16)
+    first = (tok_ref[0].astype(jnp.float32) + 0.5 * share).astype(jnp.bfloat16)
     first_ref[...] = first
     first_f = first.astype(jnp.float32)
     squares = jnp.sum(first_f * first_f, axis=1, keepdims=True)
@@ -144,7 +158,8 @@
 
 
 def mixer_kernel(width, groups, got_ref, taps_ref, hist_ref, bias_ref, rate_ref, state_ref, ggain_ref,
-                 state_out_ref, hist_out_ref, normed_ref, read_rows, taps_rows, hist_rows, hist_wide):
+                 state_out_ref, hist_out_ref, normed_ref, read_rows, taps_rows, hist_rows, hist_wide,
+                 head_rows, head_wide):
     ways = got_ref.shape[0]
     heads, head_dim, state_dim = state_ref.shape
     in_rows = heads * head_dim // LANES
@@ -184,16 +199,24 @@
     maps_high = maps.astype(jnp.bfloat16)
     maps_low = (maps - maps_high.astype(jnp.float32)).astype(jnp.bfloat16)
     maps2 = jnp.concatenate([maps_high, maps_low], axis=0)
-    pad = jnp.zeros((LANES - in_rows, LANES), jnp.float32)
-    columns = jnp.concatenate([conv[:in_rows], pad], axis=0).T
+    head_rows[...] = jnp.zeros_like(head_rows)
+    head_rows[0:1, :heads] = decay
+    head_rows[1:2, :heads] = step
+    pad = jnp.zeros((LANES - in_rows - 8, LANES), jnp.float32)
+    columns = jnp.concatenate([conv[:in_rows], head_rows[...], pad], axis=0).T
+    for i in range(2):
+        head_wide[i * heads : (i + 1) * heads, :] = jnp.broadcast_to(
+            columns[:heads, in_rows + i : in_rows + i + 1], (heads, LANES)
+        )
     per_row = LANES // head_dim
     per_group = heads // groups
     for g in range(groups):
         write = maps[g : g + 1]
         for h in range(g * per_group, (g + 1) * per_group):
             r, c = h // per_row, h % per_row
-            column = columns[c * head_dim : (c + 1) * head_dim, r : r + 1] * step[:, h : h + 1]
-            state_out_ref[h] = decay[:, h : h + 1] * state_ref[h] + column * write
+            column = columns[c * head_dim : (c + 1) * head_dim, r : r + 1]
+            added = column * (head_wide[heads + h : heads + h + 1, :] * write)
+            state_out_ref[h] = head_wide[h : h + 1, :] * state_ref[h] + added
         block = state_out_ref[g * per_group : (g + 1) * per_group].reshape(
             per_group * head_dim, state_dim
         )
@@ -242,6 +265,8 @@
             pltpu.VMEM((taps.shape[0] * conv_rows, LANES), jnp.float32),
             pltpu.VMEM((hist.shape[0] * conv_rows, LANES), jnp.float32),
             pltpu.VMEM(hist.shape, jnp.float32),
+            pltpu.VMEM((8, LANES), jnp.float32),
+            pltpu.VMEM((2 * heads, LANES), jnp.float32),
         ],
         compiler_params=params(8),
         cost_estimate=COST,
@@ -331,7 +356,7 @@
     place = tuple(order.index(k) for k in range(ways))
 
     with scope("repeat"):
-        blocks = repeat(tokens, ways)
+        blocks = repeat(fetch(tokens), ways)
     whole = exchange(blocks, order)
     with scope("ff1"):
         (down1,) = ff(place, whole, first_gain.reshape(1, width), first_gate.T, first_up.T, first_down)
@@ -339,7 +364,7 @@
     with scope("project"):
         first, packed = project(
             place,
-            got1, tokens, mix_gain.reshape(1, -1), w_input, w_write, w_read, w_outgate, w_step.T, slots
+            got1, blocks, mix_gain.reshape(1, -1), w_input, w_write, w_read, w_outgate, w_step.T, slots
         )
     got2 = exchange(packed, order)
     with scope("mixer"):

time: 54.8 us -> 54.5 us (level)
  no operation moved by 1% of the time
where the time goes in v6:
time: 54.5 us; the launch traced here: 54.1 us
  blocking collectives  46.1 us (85%)
  Pallas kernels  6.36 us (12%)
  between operations  0.89 us (2%)
  local copies, waits for them, and re-layouts  0.8 us (1%)
    all_to_all x6, blocking collectives, exchange(): lax.all_to_all(blocks, AXES, split_axis=0, concat_axis=0, tiled=True, axi...  46.1 us
    pallas_call x2, Pallas kernels, ff(): pl.pallas_call(functools.partial(ff_kernel, place, len(kept)), out_shape=...  4.09 us

profile of v6, /device:TPU:0, one launch (start us, length us, event | category | flops | bytes accessed | tf_op | source)
XLA Modules:
  0.0 54.1 jit_solution(5642392426145288572)
XLA Ops:
  0.6 0.0 copy-start
  0.6 0.7 %copy-done = bf16[8,256]{1,0:T(8,128)(2,1)S(1)} copy-done((bf16[8,256]{1,0:T(8,128)(2,1)S(1)}, bf16[8,256]{1,0:T(8,128)(2,1)}, u32[]{:S(2)}) %copy-start) | copy-done | bytes 4120
  1.3 0.0 copy-start.16
  1.4 10.0 %all_to_all.30.x_ref = bf16[8,8,256]{2,1,0:T(8,128)(2,1)S(1)} all-to-all(bf16[8,8,256]{2,1,0:T(8,128)(2,1)S(1)} %repeat.3.tok_ref), channel_id=1, replica_groups={{5,0,1,2,4,3,7,6},{13,8,9,10,12,11,15,14},{21,16,17,18,20,19,23,22},{29..., dimensions={0} | all-to-all | bytes 65536 | tf_op jit(solution)/shard_map/all_to_all | solution.py:20
  11.4 0.0 copy-done.1
  11.4 0.0 copy-done.2
  11.4 0.0 copy-done.3
  11.4 0.0 copy-done.16
  11.4 0.0 copy-start.7
  11.4 0.0 copy-start.8
  11.4 0.0 copy-start.11
  11.4 0.0 copy-start.12
  11.5 0.0 copy-start.15
  11.5 0.0 copy-start.19
  11.5 2.0 %ff1.1 = bf16[8,8,256]{2,1,0:T(8,128)(2,1)S(1)} custom-call(bf16[8,8,256]{2,1,0:T(8,128)(2,1)S(1)} %all_to_all.30.x_ref, f32[1,2048]{1,0:T(1,128)S(1)} %bitcast.22, bf16[704,2048]{1,0:T(8,128)(2,1)S(1)} %bitcast.15, bf16[704,2048]{1,0:T(8,128)(2,1)S(1)} %bitcast.16, bf16[704,2048]{1,0:T(8,128)(2,1)S(1)} %copy-done.3), custom_call_target="tpu_custom_call" | custom-call | flops 10000000000 | bytes 1000 | tf_op jit(solution)/shard_map/ff1/pallas_call | solution.py:98
  13.5 7.1 %all_to_all.31.got_ref = bf16[8,8,256]{2,1,0:T(8,128)(2,1)S(1)} all-to-all(bf16[8,8,256]{2,1,0:T(8,128)(2,1)S(1)} %ff1.1), channel_id=1, replica_groups={{5,0,1,2,4,3,7,6},{13,8,9,10,12,11,15,14},{21,16,17,18,20,19,23,22},{29..., dimensions={0} | all-to-all | bytes 65536 | tf_op jit(solution)/shard_map/all_to_all | solution.py:20
  20.6 0.0 copy-done.7
  20.6 0.0 copy-done.8
  20.6 0.0 copy-done.11
  20.6 0.0 copy-done.12
  20.6 0.0 copy-done.15
  20.6 0.0 copy-done.19
  20.6 0.0 copy-start.9
  20.6 0.0 copy-start.13
  20.6 0.0 copy-start.14
  20.7 0.0 copy-start.17
  20.7 0.0 copy-start.20
  20.7 0.0 copy-start.21
  20.7 0.5 project.1
  21.2 7.5 %all_to_all.32.got_ref = bf16[8,48,128]{2,1,0:T(8,128)(2,1)S(1)} all-to-all(bf16[8,48,128]{2,1,0:T(8,128)(2,1)S(1)} %get-tuple-element.11), channel_id=1, replica_groups={{5,0,1,2,4,3,7,6},{13,8,9,10,12,11,15,14},{21,16,17,18,20,19,23,22},{29..., dimensions={0} | all-to-all | bytes 196608 | tf_op jit(solution)/shard_map/all_to_all | solution.py:20
  28.7 0.0 copy-done.9
  28.7 0.0 copy-done.13
  28.7 0.0 copy-done.14
  28.7 0.0 copy-done.17
  28.7 0.0 copy-done.20
  28.7 0.0 copy-done.21
  28.7 0.0 copy-start.10
  28.8 0.9 %mixer.1 = (f32[32,64,128]{2,1,0:T(8,128)S(1)}, bf16[3,3072]{1,0:T(4,128)(2,1)S(1)}, bf16[8,16,128]{2,1,0:T(8,128)(2,1)S(1)}) custom-call(bf16[8,48,128]{2,1,0:T(8,128)(2,1)S(1)} %all_to_all.32.got_ref, bf16[4,3072]{1,0:T(4,128)(2,1)S(1)} %copy-done.13, bf16[3,3072]{1,0:T(4,128)(2,1)S(1)} %bitcast.20, f32[1,32]{1,0:T(1,128)S(1)} %bitcast.26, ...), custom_call_target="tpu_custom_call" | custom-call | flops 10000000000 | bytes 1000 | tf_op jit(solution)/shard_map/mixer/pallas_call | solution.py:254
  29.7 7.1 %all_to_all.33.got_ref = bf16[8,16,128]{2,1,0:T(8,128)(2,1)S(1)} all-to-all(bf16[8,16,128]{2,1,0:T(8,128)(2,1)S(1)} %get-tuple-element.12), channel_id=1, replica_groups={{5,0,1,2,4,3,7,6},{13,8,9,10,12,11,15,14},{21,16,17,18,20,19,23,22},{29..., dimensions={0} | all-to-all | bytes 65536 | tf_op jit(solution)/shard_map/all_to_all | solution.py:20
  36.8 0.0 copy-done.10
  36.8 0.0 copy-start.18
  36.8 0.2 output.1.second_ref
  37.0 7.3 %all_to_all.34.x_ref = bf16[8,8,256]{2,1,0:T(8,128)(2,1)S(1)} all-to-all(bf16[8,8,256]{2,1,0:T(8,128)(2,1)S(1)} %output.1.second_ref), channel_id=1, replica_groups={{5,0,1,2,4,3,7,6},{13,8,9,10,12,11,15,14},{21,16,17,18,20,19,23,22},{29..., dimensions={0} | all-to-all | bytes 65536 | tf_op jit(solution)/shard_map/all_to_all | solution.py:20
  44.4 0.0 copy-done.4
  44.4 0.0 copy-done.6
  44.4 2.1 %ff2.1 = (bf16[8,8,256]{2,1,0:T(8,128)(2,1)S(1)}, f32[32,64,128]{2,1,0:T(8,128)}, bf16[3,3072]{1,0:T(4,128)(2,1)}) custom-call(bf16[8,8,256]{2,1,0:T(8,128)(2,1)S(1)} %all_to_all.34.x_ref, f32[1,2048]{1,0:T(1,128)S(1)} %bitcast.24, bf16[704,2048]{1,0:T(8,128)(2,1)S(1)} %bitcast.17, bf16[704,2048]{1,0:T(8,128)(2,1)S(1)} %bitcast.18, ...), custom_call_target="tpu_custom_call" | custom-call | flops 10000000000 | bytes 1000 | tf_op jit(solution)/shard_map/ff2/pallas_call | solution.py:98
  46.4 7.1 %all_to_all.35.got_ref = bf16[8,8,256]{2,1,0:T(8,128)(2,1)S(1)} all-to-all(bf16[8,8,256]{2,1,0:T(8,128)(2,1)S(1)} %get-tuple-element.16), channel_id=1, replica_groups={{5,0,1,2,4,3,7,6},{13,8,9,10,12,11,15,14},{21,16,17,18,20,19,23,22},{29..., dimensions={0} | all-to-all | bytes 65536 | tf_op jit(solution)/shard_map/all_to_all | solution.py:20
  53.5 0.6 %final.1 = bf16[8,256]{1,0:T(8,128)(2,1)} custom-call(bf16[8,8,256]{2,1,0:T(8,128)(2,1)S(1)} %all_to_all.35.got_ref, bf16[8,8,256]{2,1,0:T(8,128)(2,1)S(1)} %output.1.second_ref), custom_call_target="tpu_custom_call" | custom-call | tf_op jit(solution)/shard_map/final/pallas_call | solution.py:310
  (10 shorter events, 0.0 us)
Async XLA Ops:
  0.6 0.7 %copy-start = (bf16[8,256]{1,0:T(8,128)(2,1)S(1)}, bf16[8,256]{1,0:T(8,128)(2,1)}, u32[]{:S(2)}) copy-start(bf16[8,256]{1,0:T(8,128)(2,1)} %block_ref.1) | copy-start | bytes 12292
  1.3 10.1 %copy-start.1 = (bf16[2048,704]{0,1:T(8,128)(2,1)S(1)}, bf16[2048,704]{0,1:T(8,128)(2,1)}, u32[]{:S(2)}) copy-start(bf16[2048,704]{0,1:T(8,128)(2,1)} %param.24) | copy-start | bytes 8650756
  1.3 10.1 %copy-start.2 = (bf16[2048,704]{0,1:T(8,128)(2,1)S(1)}, bf16[2048,704]{0,1:T(8,128)(2,1)}, u32[]{:S(2)}) copy-start(bf16[2048,704]{0,1:T(8,128)(2,1)} %param.25) | copy-start | bytes 8650756
  1.3 10.1 %copy-start.3 = (bf16[704,2048]{1,0:T(8,128)(2,1)S(1)}, bf16[704,2048]{1,0:T(8,128)(2,1)}, u32[]{:S(2)}) copy-start(bf16[704,2048]{1,0:T(8,128)(2,1)} %down_ref.2) | copy-start | bytes 8650756
  1.3 10.1 %copy-start.16 = (f32[2048]{0:T(1024)S(1)}, f32[2048]{0:T(1024)}, u32[]{:S(2)}) copy-start(f32[2048]{0:T(1024)} %param.23) | copy-start | bytes 24580
  11.4 9.2 %copy-start.7 = (bf16[256,2048]{1,0:T(8,128)(2,1)S(1)}, bf16[256,2048]{1,0:T(8,128)(2,1)}, u32[]{:S(2)}) copy-start(bf16[256,2048]{1,0:T(8,128)(2,1)} %win_ref.1) | copy-start | bytes 3145732
  11.4 9.2 %copy-start.8 = (bf16[256,2048]{1,0:T(8,128)(2,1)S(1)}, bf16[256,2048]{1,0:T(8,128)(2,1)}, u32[]{:S(2)}) copy-start(bf16[256,2048]{1,0:T(8,128)(2,1)} %wgate_ref.1) | copy-start | bytes 3145732
  11.4 9.2 %copy-start.11 = (bf16[256,512]{1,0:T(8,128)(2,1)S(1)}, bf16[256,512]{1,0:T(8,128)(2,1)}, u32[]{:S(2)}) copy-start(bf16[256,512]{1,0:T(8,128)(2,1)} %wwrite_ref.1) | copy-start | bytes 786436
  11.4 9.2 %copy-start.12 = (bf16[256,512]{1,0:T(8,128)(2,1)S(1)}, bf16[256,512]{1,0:T(8,128)(2,1)}, u32[]{:S(2)}) copy-start(bf16[256,512]{1,0:T(8,128)(2,1)} %wread_ref.1) | copy-start | bytes 786436
  11.5 9.1 %copy-start.15 = (bf16[256,32]{0,1:T(8,128)(2,1)S(1)}, bf16[256,32]{0,1:T(8,128)(2,1)}, u32[]{:S(2)}) copy-start(bf16[256,32]{0,1:T(8,128)(2,1)} %param.32) | copy-start | bytes 49156
  11.5 9.1 %copy-start.19 = (f32[256]{0:T(256)S(1)}, f32[256]{0:T(256)}, u32[]{:S(2)}) copy-start(f32[256]{0:T(256)} %param.27) | copy-start | bytes 3076
  20.6 8.1 %copy-start.9 = (f32[1,32,64,128]{3,2,1,0:T(8,128)S(1)}, f32[1,32,64,128]{3,2,1,0:T(8,128)}, u32[]{:S(2)}) copy-start(f32[1,32,64,128]{3,2,1,0:T(8,128)} %param.37) | copy-start | bytes 3145732
  20.6 8.1 %copy-start.13 = (bf16[4,3072]{1,0:T(4,128)(2,1)S(1)}, bf16[4,3072]{1,0:T(4,128)(2,1)}, u32[]{:S(2)}) copy-start(bf16[4,3072]{1,0:T(4,128)(2,1)} %taps_ref.1) | copy-start | bytes 73732
  20.6 8.1 %copy-start.14 = (bf16[1,3,3072]{2,1,0:T(4,128)(2,1)S(1)}, bf16[1,3,3072]{2,1,0:T(4,128)(2,1)}, u32[]{:S(2)}) copy-start(bf16[1,3,3072]{2,1,0:T(4,128)(2,1)} %param.34) | copy-start | bytes 55300
  20.7 8.1 %copy-start.17 = (f32[2048]{0:T(1024)S(1)}, f32[2048]{0:T(1024)}, u32[]{:S(2)}) copy-start(f32[2048]{0:T(1024)} %param.38) | copy-start | bytes 24580
  20.7 8.1 %copy-start.20 = (f32[32]{0:T(128)S(1)}, f32[32]{0:T(128)}, u32[]{:S(2)}) copy-start(f32[32]{0:T(128)} %param.35) | copy-start | bytes 388
  20.7 8.1 %copy-start.21 = (f32[32]{0:T(128)S(1)}, f32[32]{0:T(128)}, u32[]{:S(2)}) copy-start(f32[32]{0:T(128)} %param.36) | copy-start | bytes 388
  28.7 8.0 %copy-start.10 = (bf16[2048,256]{1,0:T(8,128)(2,1)S(1)}, bf16[2048,256]{1,0:T(8,128)(2,1)}, u32[]{:S(2)}) copy-start(bf16[2048,256]{1,0:T(8,128)(2,1)} %w_ref.1) | copy-start | bytes 3145732
  36.8 7.6 %copy-start.4 = (bf16[2048,704]{0,1:T(8,128)(2,1)S(1)}, bf16[2048,704]{0,1:T(8,128)(2,1)}, u32[]{:S(2)}) copy-start(bf16[2048,704]{0,1:T(8,128)(2,1)} %param.41) | copy-start | bytes 8650756
  36.8 7.6 %copy-start.5 = (bf16[2048,704]{0,1:T(8,128)(2,1)S(1)}, bf16[2048,704]{0,1:T(8,128)(2,1)}, u32[]{:S(2)}) copy-start(bf16[2048,704]{0,1:T(8,128)(2,1)} %param.42) | copy-start | bytes 8650756
  36.8 7.6 %copy-start.6 = (bf16[704,2048]{1,0:T(8,128)(2,1)S(1)}, bf16[704,2048]{1,0:T(8,128)(2,1)}, u32[]{:S(2)}) copy-start(bf16[704,2048]{1,0:T(8,128)(2,1)} %down_ref.3) | copy-start | bytes 8650756
  36.8 7.6 %copy-start.18 = (f32[2048]{0:T(1024)S(1)}, f32[2048]{0:T(1024)}, u32[]{:S(2)}) copy-start(f32[2048]{0:T(1024)} %param.40) | copy-start | bytes 24580

commit v7 on v6

--- a/solution.py
+++ b/solution.py
@@ -222,8 +222,6 @@
         )
         high = block.astype(jnp.bfloat16)
         read = lax.dot_general(maps2, high, ROW_ROW, preferred_element_type=jnp.float32)
-        low = (block - high.astype(jnp.float32)).astype(jnp.bfloat16)
-        read += lax.dot_general(maps2, low, ROW_ROW, preferred_element_type=jnp.float32)
         count = 2 * map_rows
         read = read[:count] + read[count:]
         span = per_group * head_dim // LANES

time: 54.5 us -> 54.4 us (level)
  no operation moved by 1% of the time
where the time goes in v7:
time: 54.4 us; the launch traced here: 54 us
  blocking collectives  46.1 us (85%)
  Pallas kernels  6.29 us (12%)
  between operations  0.89 us (2%)
  local copies, waits for them, and re-layouts  0.8 us (1%)
    all_to_all x6, blocking collectives, exchange(): lax.all_to_all(blocks, AXES, split_axis=0, concat_axis=0, tiled=True, axi...  46.1 us
    pallas_call x2, Pallas kernels, ff(): pl.pallas_call(functools.partial(ff_kernel, place, len(kept)), out_shape=...  4.09 us

profile of v7, /device:TPU:0, one launch (start us, length us, event | category | flops | bytes accessed | tf_op | source)
XLA Modules:
  0.0 54.0 jit_solution(15947155033291920749)
XLA Ops:
  0.6 0.0 copy-start
  0.6 0.7 %copy-done = bf16[8,256]{1,0:T(8,128)(2,1)S(1)} copy-done((bf16[8,256]{1,0:T(8,128)(2,1)S(1)}, bf16[8,256]{1,0:T(8,128)(2,1)}, u32[]{:S(2)}) %copy-start) | copy-done | bytes 4120
  1.3 0.0 copy-start.16
  1.4 10.0 %all_to_all.30.x_ref = bf16[8,8,256]{2,1,0:T(8,128)(2,1)S(1)} all-to-all(bf16[8,8,256]{2,1,0:T(8,128)(2,1)S(1)} %repeat.3.tok_ref), channel_id=1, replica_groups={{5,0,1,2,4,3,7,6},{13,8,9,10,12,11,15,14},{21,16,17,18,20,19,23,22},{29..., dimensions={0} | all-to-all | bytes 65536 | tf_op jit(solution)/shard_map/all_to_all | solution.py:20
  11.4 0.0 copy-done.1
  11.4 0.0 copy-done.2
  11.4 0.0 copy-done.3
  11.4 0.0 copy-done.16
  11.4 0.0 copy-start.7
  11.4 0.0 copy-start.8
  11.4 0.0 copy-start.11
  11.4 0.0 copy-start.12
  11.5 0.0 copy-start.15
  11.5 0.0 copy-start.19
  11.5 2.0 %ff1.1 = bf16[8,8,256]{2,1,0:T(8,128)(2,1)S(1)} custom-call(bf16[8,8,256]{2,1,0:T(8,128)(2,1)S(1)} %all_to_all.30.x_ref, f32[1,2048]{1,0:T(1,128)S(1)} %bitcast.22, bf16[704,2048]{1,0:T(8,128)(2,1)S(1)} %bitcast.15, bf16[704,2048]{1,0:T(8,128)(2,1)S(1)} %bitcast.16, bf16[704,2048]{1,0:T(8,128)(2,1)S(1)} %copy-done.3), custom_call_target="tpu_custom_call" | custom-call | flops 10000000000 | bytes 1000 | tf_op jit(solution)/shard_map/ff1/pallas_call | solution.py:98
  13.5 7.1 %all_to_all.31.got_ref = bf16[8,8,256]{2,1,0:T(8,128)(2,1)S(1)} all-to-all(bf16[8,8,256]{2,1,0:T(8,128)(2,1)S(1)} %ff1.1), channel_id=1, replica_groups={{5,0,1,2,4,3,7,6},{13,8,9,10,12,11,15,14},{21,16,17,18,20,19,23,22},{29..., dimensions={0} | all-to-all | bytes 65536 | tf_op jit(solution)/shard_map/all_to_all | solution.py:20
  20.6 0.0 copy-done.7
  20.6 0.0 copy-done.8
  20.6 0.0 copy-done.11
  20.6 0.0 copy-done.12
  20.6 0.0 copy-done.15
  20.6 0.0 copy-done.19
  20.6 0.0 copy-start.9
  20.6 0.0 copy-start.13
  20.6 0.0 copy-start.14
  20.7 0.0 copy-start.17
  20.7 0.0 copy-start.20
  20.7 0.0 copy-start.21
  20.7 0.5 project.1
  21.2 7.5 %all_to_all.32.got_ref = bf16[8,48,128]{2,1,0:T(8,128)(2,1)S(1)} all-to-all(bf16[8,48,128]{2,1,0:T(8,128)(2,1)S(1)} %get-tuple-element.11), channel_id=1, replica_groups={{5,0,1,2,4,3,7,6},{13,8,9,10,12,11,15,14},{21,16,17,18,20,19,23,22},{29..., dimensions={0} | all-to-all | bytes 196608 | tf_op jit(solution)/shard_map/all_to_all | solution.py:20
  28.7 0.0 copy-done.9
  28.7 0.0 copy-done.13
  28.7 0.0 copy-done.14
  28.7 0.0 copy-done.17
  28.7 0.0 copy-done.20
  28.7 0.0 copy-done.21
  28.7 0.0 copy-start.10
  28.8 0.9 %mixer.1 = (f32[32,64,128]{2,1,0:T(8,128)S(1)}, bf16[3,3072]{1,0:T(4,128)(2,1)S(1)}, bf16[8,16,128]{2,1,0:T(8,128)(2,1)S(1)}) custom-call(bf16[8,48,128]{2,1,0:T(8,128)(2,1)S(1)} %all_to_all.32.got_ref, bf16[4,3072]{1,0:T(4,128)(2,1)S(1)} %copy-done.13, bf16[3,3072]{1,0:T(4,128)(2,1)S(1)} %bitcast.20, f32[1,32]{1,0:T(1,128)S(1)} %bitcast.26, ...), custom_call_target="tpu_custom_call" | custom-call | flops 10000000000 | bytes 1000 | tf_op jit(solution)/shard_map/mixer/pallas_call | solution.py:252
  29.6 7.1 %all_to_all.33.got_ref = bf16[8,16,128]{2,1,0:T(8,128)(2,1)S(1)} all-to-all(bf16[8,16,128]{2,1,0:T(8,128)(2,1)S(1)} %get-tuple-element.12), channel_id=1, replica_groups={{5,0,1,2,4,3,7,6},{13,8,9,10,12,11,15,14},{21,16,17,18,20,19,23,22},{29..., dimensions={0} | all-to-all | bytes 65536 | tf_op jit(solution)/shard_map/all_to_all | solution.py:20
  36.7 0.0 copy-done.10
  36.7 0.0 copy-start.18
  36.7 0.2 output.1.second_ref
  37.0 7.3 %all_to_all.34.x_ref = bf16[8,8,256]{2,1,0:T(8,128)(2,1)S(1)} all-to-all(bf16[8,8,256]{2,1,0:T(8,128)(2,1)S(1)} %output.1.second_ref), channel_id=1, replica_groups={{5,0,1,2,4,3,7,6},{13,8,9,10,12,11,15,14},{21,16,17,18,20,19,23,22},{29..., dimensions={0} | all-to-all | bytes 65536 | tf_op jit(solution)/shard_map/all_to_all | solution.py:20
  44.3 0.0 copy-done.4
  44.3 0.0 copy-done.5
  44.3 2.1 %ff2.1 = (bf16[8,8,256]{2,1,0:T(8,128)(2,1)S(1)}, f32[32,64,128]{2,1,0:T(8,128)}, bf16[3,3072]{1,0:T(4,128)(2,1)}) custom-call(bf16[8,8,256]{2,1,0:T(8,128)(2,1)S(1)} %all_to_all.34.x_ref, f32[1,2048]{1,0:T(1,128)S(1)} %bitcast.24, bf16[704,2048]{1,0:T(8,128)(2,1)S(1)} %bitcast.17, bf16[704,2048]{1,0:T(8,128)(2,1)S(1)} %bitcast.18, ...), custom_call_target="tpu_custom_call" | custom-call | flops 10000000000 | bytes 1000 | tf_op jit(solution)/shard_map/ff2/pallas_call | solution.py:98
  46.4 7.1 %all_to_all.35.got_ref = bf16[8,8,256]{2,1,0:T(8,128)(2,1)S(1)} all-to-all(bf16[8,8,256]{2,1,0:T(8,128)(2,1)S(1)} %get-tuple-element.16), channel_id=1, replica_groups={{5,0,1,2,4,3,7,6},{13,8,9,10,12,11,15,14},{21,16,17,18,20,19,23,22},{29..., dimensions={0} | all-to-all | bytes 65536 | tf_op jit(solution)/shard_map/all_to_all | solution.py:20
  53.4 0.6 %final.1 = bf16[8,256]{1,0:T(8,128)(2,1)} custom-call(bf16[8,8,256]{2,1,0:T(8,128)(2,1)S(1)} %all_to_all.35.got_ref, bf16[8,8,256]{2,1,0:T(8,128)(2,1)S(1)} %output.1.second_ref), custom_call_target="tpu_custom_call" | custom-call | tf_op jit(solution)/shard_map/final/pallas_call | solution.py:308
  (10 shorter events, 0.0 us)
Async XLA Ops:
  0.6 0.7 %copy-start = (bf16[8,256]{1,0:T(8,128)(2,1)S(1)}, bf16[8,256]{1,0:T(8,128)(2,1)}, u32[]{:S(2)}) copy-start(bf16[8,256]{1,0:T(8,128)(2,1)} %block_ref.1) | copy-start | bytes 12292
  1.3 10.1 %copy-start.1 = (bf16[2048,704]{0,1:T(8,128)(2,1)S(1)}, bf16[2048,704]{0,1:T(8,128)(2,1)}, u32[]{:S(2)}) copy-start(bf16[2048,704]{0,1:T(8,128)(2,1)} %param.24) | copy-start | bytes 8650756
  1.3 10.1 %copy-start.2 = (bf16[2048,704]{0,1:T(8,128)(2,1)S(1)}, bf16[2048,704]{0,1:T(8,128)(2,1)}, u32[]{:S(2)}) copy-start(bf16[2048,704]{0,1:T(8,128)(2,1)} %param.25) | copy-start | bytes 8650756
  1.3 10.1 %copy-start.3 = (bf16[704,2048]{1,0:T(8,128)(2,1)S(1)}, bf16[704,2048]{1,0:T(8,128)(2,1)}, u32[]{:S(2)}) copy-start(bf16[704,2048]{1,0:T(8,128)(2,1)} %down_ref.2) | copy-start | bytes 8650756
  1.3 10.1 %copy-start.16 = (f32[2048]{0:T(1024)S(1)}, f32[2048]{0:T(1024)}, u32[]{:S(2)}) copy-start(f32[2048]{0:T(1024)} %param.23) | copy-start | bytes 24580
  11.4 9.2 %copy-start.7 = (bf16[256,2048]{1,0:T(8,128)(2,1)S(1)}, bf16[256,2048]{1,0:T(8,128)(2,1)}, u32[]{:S(2)}) copy-start(bf16[256,2048]{1,0:T(8,128)(2,1)} %win_ref.1) | copy-start | bytes 3145732
  11.4 9.2 %copy-start.8 = (bf16[256,2048]{1,0:T(8,128)(2,1)S(1)}, bf16[256,2048]{1,0:T(8,128)(2,1)}, u32[]{:S(2)}) copy-start(bf16[256,2048]{1,0:T(8,128)(2,1)} %wgate_ref.1) | copy-start | bytes 3145732
  11.4 9.2 %copy-start.11 = (bf16[256,512]{1,0:T(8,128)(2,1)S(1)}, bf16[256,512]{1,0:T(8,128)(2,1)}, u32[]{:S(2)}) copy-start(bf16[256,512]{1,0:T(8,128)(2,1)} %wwrite_ref.1) | copy-start | bytes 786436
  11.4 9.2 %copy-start.12 = (bf16[256,512]{1,0:T(8,128)(2,1)S(1)}, bf16[256,512]{1,0:T(8,128)(2,1)}, u32[]{:S(2)}) copy-start(bf16[256,512]{1,0:T(8,128)(2,1)} %wread_ref.1) | copy-start | bytes 786436
  11.5 9.1 %copy-start.15 = (bf16[256,32]{0,1:T(8,128)(2,1)S(1)}, bf16[256,32]{0,1:T(8,128)(2,1)}, u32[]{:S(2)}) copy-start(bf16[256,32]{0,1:T(8,128)(2,1)} %param.32) | copy-start | bytes 49156
  11.5 9.1 %copy-start.19 = (f32[256]{0:T(256)S(1)}, f32[256]{0:T(256)}, u32[]{:S(2)}) copy-start(f32[256]{0:T(256)} %param.27) | copy-start | bytes 3076
  20.6 8.1 %copy-start.9 = (f32[1,32,64,128]{3,2,1,0:T(8,128)S(1)}, f32[1,32,64,128]{3,2,1,0:T(8,128)}, u32[]{:S(2)}) copy-start(f32[1,32,64,128]{3,2,1,0:T(8,128)} %param.37) | copy-start | bytes 3145732
  20.6 8.1 %copy-start.13 = (bf16[4,3072]{1,0:T(4,128)(2,1)S(1)}, bf16[4,3072]{1,0:T(4,128)(2,1)}, u32[]{:S(2)}) copy-start(bf16[4,3072]{1,0:T(4,128)(2,1)} %taps_ref.1) | copy-start | bytes 73732
  20.6 8.1 %copy-start.14 = (bf16[1,3,3072]{2,1,0:T(4,128)(2,1)S(1)}, bf16[1,3,3072]{2,1,0:T(4,128)(2,1)}, u32[]{:S(2)}) copy-start(bf16[1,3,3072]{2,1,0:T(4,128)(2,1)} %param.34) | copy-start | bytes 55300
  20.7 8.1 %copy-start.17 = (f32[2048]{0:T(1024)S(1)}, f32[2048]{0:T(1024)}, u32[]{:S(2)}) copy-start(f32[2048]{0:T(1024)} %param.38) | copy-start | bytes 24580
  20.7 8.1 %copy-start.20 = (f32[32]{0:T(128)S(1)}, f32[32]{0:T(128)}, u32[]{:S(2)}) copy-start(f32[32]{0:T(128)} %param.35) | copy-start | bytes 388
  20.7 8.1 %copy-start.21 = (f32[32]{0:T(128)S(1)}, f32[32]{0:T(128)}, u32[]{:S(2)}) copy-start(f32[32]{0:T(128)} %param.36) | copy-start | bytes 388
  28.7 7.9 %copy-start.10 = (bf16[2048,256]{1,0:T(8,128)(2,1)S(1)}, bf16[2048,256]{1,0:T(8,128)(2,1)}, u32[]{:S(2)}) copy-start(bf16[2048,256]{1,0:T(8,128)(2,1)} %w_ref.1) | copy-start | bytes 3145732
  36.7 7.6 %copy-start.4 = (bf16[2048,704]{0,1:T(8,128)(2,1)S(1)}, bf16[2048,704]{0,1:T(8,128)(2,1)}, u32[]{:S(2)}) copy-start(bf16[2048,704]{0,1:T(8,128)(2,1)} %param.41) | copy-start | bytes 8650756
  36.7 7.6 %copy-start.5 = (bf16[2048,704]{0,1:T(8,128)(2,1)S(1)}, bf16[2048,704]{0,1:T(8,128)(2,1)}, u32[]{:S(2)}) copy-start(bf16[2048,704]{0,1:T(8,128)(2,1)} %param.42) | copy-start | bytes 8650756
  36.7 7.6 %copy-start.6 = (bf16[704,2048]{1,0:T(8,128)(2,1)S(1)}, bf16[704,2048]{1,0:T(8,128)(2,1)}, u32[]{:S(2)}) copy-start(bf16[704,2048]{1,0:T(8,128)(2,1)} %down_ref.3) | copy-start | bytes 8650756
  36.7 7.6 %copy-start.18 = (f32[2048]{0:T(1024)S(1)}, f32[2048]{0:T(1024)}, u32[]{:S(2)}) copy-start(f32[2048]{0:T(1024)} %param.40) | copy-start | bytes 24580
